TPU v7x, 32 devices: a whole 2x2x4 slice. The times are simulated.
32 devices in a mesh: ep: 4 (over y, x), tp: 8 (over z, core).
Axes of the slice: x: 2, y: 2, z: 4, core: 2. Of those that a mesh axis runs over, the one named last changes fastest.
Arguments:
- resid: bfloat16 [512, 2048], P('ep'), may hold values from -6 to 6
- norm1_gain: float32 [2048], replicated, may hold values from 0.1 to 1.9
- w_query: bfloat16 [2048, 2048], P('ep', 'tp'), may hold values from -0.125 to 0.125
- w_key: bfloat16 [2048, 2048], P('ep', 'tp'), may hold values from -0.125 to 0.125
- w_value: bfloat16 [2048, 2048], P('ep', 'tp'), may hold values from -0.125 to 0.125
- w_outgate: bfloat16 [2048, 2048], P('ep', 'tp'), may hold values from -0.125 to 0.125
- w_igate: bfloat16 [2048, 32], replicated, may hold values from -0.125 to 0.125
- w_fgate: bfloat16 [2048, 32], replicated, may hold values from -0.125 to 0.125
- forget_bias: float32 [32], replicated, may hold values from 0 to 4
- head_gain: float32 [2048], P('tp'), may hold values from 0.1 to 1.9
- w_out: bfloat16 [2048, 2048], P('tp'), may hold values from -0.125 to 0.125
- state_matrix: float32 [512, 32, 64, 64], P('ep', 'tp'), may hold values from -4 to 4
- state_norm: float32 [512, 32, 64], P('ep', 'tp'), may hold values from -8 to 8
- state_max: float32 [512, 32], P('ep', 'tp'), may hold values from -1 to 2
- norm2_gain: float32 [2048], replicated, may hold values from 0.1 to 1.9
- group_router: bfloat16 [2048, 4], replicated, may hold values from -0.125 to 0.125
- expert_router: bfloat16 [2048, 8], replicated, may hold values from -0.125 to 0.125
- expert_ids: int32 [512, 2], P('ep'), may hold values from 0 to 7, all different within a row; in each aligned block of 128 rows (0 to 127, 128 to 255, ...) at most 48 rows name the same one
- exp_gate: bfloat16 [8, 2048, 1024], P('ep', None, 'tp'), may hold values from -0.125 to 0.125
- exp_up: bfloat16 [8, 2048, 1024], P('ep', None, 'tp'), may hold values from -0.125 to 0.125
- exp_down: bfloat16 [8, 1024, 2048], P('ep', 'tp'), may hold values from -0.1875 to 0.1875
Outputs:
- mixed: bfloat16 [512, 2048], P('ep', 'tp')
- new_matrix: float32 [512, 32, 64, 64], P('ep', 'tp')
- new_normer: float32 [512, 32, 64], P('ep', 'tp')
- new_max: float32 [512, 32], P('ep', 'tp')
Inputs may be any that keep to these rules, and one draw needn't show every extreme that they name: `expert_ids`: A token's 2 experts differ. Among the 128 tokens of one index of ep (aligned blocks of rows) no expert is named more than 48 times, and in some block one expert is named exactly 48 times.
All inputs are finite; a program needn't handle non-finite values.
Results may differ from a plain program's by a relative error of at most 0.014.
Values may be sent and summed in bfloat16 or wider, within the bound.
No kernel may reach another device: no remote copies, remote signals or barrier semaphores. Data moves between devices by JAX's collectives and lax.ppermute only.
A program may use at most 128 MiB of HBM per device.

v0:
```python
import functools

import jax
import jax.numpy as jnp
from jax import lax
from jax.experimental import pallas as pl
from jax.experimental.pallas import tpu as pltpu
from jax.sharding import PartitionSpec as P


EPSILON = 1e-06
CORES = 2
VMEM = pltpu.MemorySpace.VMEM
F32, BF16 = jnp.float32, jnp.bfloat16


def ep_send(value, step):
    count = lax.axis_size("ep")
    return lax.ppermute(value, "ep", [(i, i ^ step) for i in range(count)])


def chip_send(value, step):
    count = lax.axis_size("tp")
    return lax.ppermute(value, "tp", [(i, i ^ (CORES * step)) for i in range(count)])


def core_send(value):
    count = lax.axis_size("tp")
    return lax.ppermute(value, "tp", [(i, i ^ 1) for i in range(count)])


def dot(lhs, rhs, lhs_dim, rhs_dim):
    return lax.dot_general(
        lhs, rhs, (((lhs_dim,), (rhs_dim,)), ((), ())), preferred_element_type=F32
    )


def call(kernel, outs, *args, far=(), unread=(), far_out=(), scratch=(), limit=8):
    args = [
        pltpu.with_memory_space_constraint(value, pltpu.MemorySpace.HBM) if i in far else value
        for i, value in enumerate(args)
    ]
    return pl.pallas_call(
        kernel,
        out_shape=[jax.ShapeDtypeStruct(shape, dtype) for shape, dtype in outs],
        in_specs=[
            pl.BlockSpec(memory_space=pl.ANY if i in far or i in unread else VMEM)
            for i in range(len(args))
        ],
        out_specs=[
            pl.BlockSpec(memory_space=pl.ANY if i in far_out else VMEM) for i in range(len(outs))
        ],
        scratch_shapes=list(scratch),
        compiler_params=pltpu.CompilerParams(vmem_limit_bytes=limit << 20),
    )(*args)


def block_cols(step, core, cols):
    chip = (lax.axis_index("tp") // CORES) ^ step
    return pl.ds(pl.multiple_of((chip * CORES + core) * cols, cols), cols)


def norm_kernel(steps, depth, cols, resid_ref, gain_ref, normed_ref, own_ref, *refs):
    block_refs, (rows_ref, row_ref, sems) = refs[:-3], refs[-3:]
    copies = [
        pltpu.make_async_copy(resid_ref, rows_ref, sems.at[0]),
        pltpu.make_async_copy(gain_ref, row_ref, sems.at[1]),
    ]
    for copy in copies:
        copy.start()
    for copy in copies:
        copy.wait()
    width = rows_ref.shape[1]
    wide = rows_ref[...].astype(F32)
    factor = lax.rsqrt(jnp.sum(wide * wide, axis=1, keepdims=True) / width + EPSILON)
    normed_ref[...] = (wide * factor * row_ref[...]).astype(BF16)
    for step, block_ref in zip(steps, block_refs):
        start = pl.multiple_of((lax.axis_index("ep") ^ step) * depth, depth)
        block_ref[...] = normed_ref[:, pl.ds(start, depth)]
    start = pl.multiple_of(lax.axis_index("tp") * cols, cols)
    own_ref[...] = rows_ref[:, pl.ds(start, cols)].astype(F32)


def gates_kernel(heads, count, normed_ref, *refs):
    gate_args, refs = refs[:4], refs[4:]
    sources, outs, refs = refs[:count], refs[count : 2 * count], refs[2 * count :]
    gates_ref, new_max_ref = refs[:2]
    igate_ref, fgate_ref, bias_ref, max_ref, both_ref, sems = refs[2:]
    targets = (igate_ref, fgate_ref, bias_ref, max_ref) + tuple(outs)
    copies = [
        pltpu.make_async_copy(source, target, sems.at[i])
        for i, (source, target) in enumerate(zip(tuple(gate_args) + tuple(sources), targets))
    ]
    for copy in copies:
        copy.start()
    for copy in copies[:4]:
        copy.wait()
    all_heads = igate_ref.shape[0]
    square = (all_heads, all_heads)
    diagonal = lax.broadcasted_iota(jnp.int32, square, 0) == lax.broadcasted_iota(
        jnp.int32, square, 1
    )
    bias = jnp.sum(jnp.where(diagonal, bias_ref[...], 0.0), axis=1, keepdims=True)
    both_ref[:all_heads] = dot(igate_ref[...], normed_ref[...], 1, 1)
    both_ref[all_heads:] = dot(fgate_ref[...], normed_ref[...], 1, 1) + bias
    start = lax.axis_index("tp") * heads
    in_gate = both_ref[pl.ds(start, heads)]
    forget = both_ref[pl.ds(all_heads + start, heads)]
    log_forget = jnp.minimum(forget, 0.0) - jnp.log1p(jnp.exp(-jnp.abs(forget)))
    running = log_forget + max_ref[...]
    new_max = jnp.maximum(running, in_gate)
    new_max_ref[...] = new_max
    gates_ref[:heads] = jnp.exp(running - new_max)
    gates_ref[heads:] = jnp.exp(in_gate - new_max)
    for copy in copies[4:]:
        copy.wait()


def stage_kernel(skip, count, chips, cols, *refs):
    w_ref, refs = refs[skip], refs[skip + 1 :]
    sources, outs = refs[:count], refs[count : 2 * count]
    keep_ref, away_ref, sems = refs[2 * count :]
    core = lax.axis_index("tp") % CORES
    pairs = list(zip(sources, outs))
    for out_ref, target in ((away_ref, 1 - core), (keep_ref, core)):
        for k in range(chips):
            at = pl.ds(k * cols, cols)
            pairs.append((w_ref.at[:, block_cols(k, target, cols)], out_ref.at[:, at]))
    copies = [
        pltpu.make_async_copy(source, target, sems.at[i])
        for i, (source, target) in enumerate(pairs)
    ]
    for copy in copies:
        copy.start()
    for copy in copies:
        copy.wait()


def swap_kernel(count, experts, after_ref, ids_ref, *refs):
    sources, outs = refs[:count], refs[count:-3]
    picks_ref, at_ref, sems = refs[-3:]
    core = lax.axis_index("tp") % CORES
    copies = []
    for i, source in enumerate(sources):
        for j, index in enumerate((core, 1 - core)):
            at = 2 * i + j
            copies.append(pltpu.make_async_copy(source.at[index], outs[at], sems.at[at]))
    for copy in copies:
        copy.start()
    topk, rows = ids_ref.shape
    slots = picks_ref.shape[0]
    local = sources[0].shape[0]
    capacity = slots // (experts // local)
    expert_iota = lax.broadcasted_iota(jnp.int32, (experts, rows), 0)
    hots = [(expert_iota == ids_ref[j : j + 1, :]).astype(F32) for j in range(topk)]
    before = lax.broadcasted_iota(jnp.int32, (rows, rows), 0) < lax.broadcasted_iota(
        jnp.int32, (rows, rows), 1
    )
    total = functools.reduce(lambda x, y: x + y, hots)
    earlier = dot(total.astype(BF16), before.astype(F32).astype(BF16), 1, 0)
    slot_iota = lax.broadcasted_iota(jnp.int32, (slots, rows), 0)
    picked = jnp.zeros((slots, rows), F32)
    for j in range(topk):
        ids = ids_ref[j : j + 1, :]
        slot = jnp.sum(earlier * hots[j], axis=0, keepdims=True).astype(jnp.int32)
        place = lax.shift_right_logical(ids, local.bit_length() - 1) ^ lax.axis_index("ep")
        at = jnp.where((ids & (local - 1)) == core, place * capacity + slot, -1)
        at_ref[j : j + 1, :] = at
        picked = picked + (slot_iota == at).astype(F32)
    picks_ref[...] = picked.astype(BF16)
    for copy in copies:
        copy.wait()


def update_kernel(heads, size, after_ref, matrix_ref, key_ref, value_ref, gates_ref, *refs):
    out_ref, done_ref, slots_ref, sems = refs
    copies = []
    for h in range(heads):
        slot = h % 2
        if h >= 2:
            copies[h - 2].wait()
        carried = gates_ref[h : h + 1, :]
        keys = key_ref[h] * gates_ref[heads + h : heads + h + 1, :]
        values = value_ref[h]
        for d in range(size):
            slots_ref[slot, d] = carried * matrix_ref[h, d] + keys[d : d + 1, :] * values
        copies.append(pltpu.make_async_copy(slots_ref.at[slot], out_ref.at[h], sems.at[slot]))
        copies[h].start()
    for copy in copies[-2:]:
        copy.wait()
    done_ref[...] = jnp.zeros_like(done_ref)


def project_kernel(x_ref, *refs):
    weights, out_ref = refs[:-1], refs[-1]
    cols = weights[0].shape[1]
    for i, w_ref in enumerate(weights):
        out_ref[:, i * cols : (i + 1) * cols] = jnp.dot(
            x_ref[...], w_ref[...], preferred_element_type=F32
        ).astype(out_ref.dtype)


def cell_kernel(heads, size, received, *refs):
    own_ref = refs[0]
    got_refs = refs[1 : 1 + received]
    gates_ref, matrix_ref, normer_ref, gain_ref = refs[1 + received : 5 + received]
    head_ref, key_ref, value_ref, norm_ref, turned_ref = refs[-5:]
    total = own_ref[...]
    for ref in got_refs:
        total = total + ref[...].astype(F32)
    turned_ref[...] = total.astype(BF16).astype(F32).T
    span = heads * size
    outs = []
    for h in range(heads):
        carried = gates_ref[h : h + 1, :]
        fresh = gates_ref[heads + h : heads + h + 1, :]
        scaled = turned_ref[h * size : (h + 1) * size, :] * size ** (-0.5)
        keys = turned_ref[span + h * size : span + (h + 1) * size, :]
        values = turned_ref[2 * span + h * size : 2 * span + (h + 1) * size, :]
        outgate = turned_ref[3 * span + h * size : 3 * span + (h + 1) * size, :]
        normer = normer_ref[h]
        readout = scaled[0:1, :] * matrix_ref[h, 0]
        for d in range(1, size):
            readout = readout + scaled[d : d + 1, :] * matrix_ref[h, d]
        score = jnp.sum(scaled * keys, axis=0, keepdims=True) * fresh
        numer = carried * readout + score * values
        denom = carried * jnp.sum(scaled * normer, axis=0, keepdims=True) + score
        cell = numer / jnp.maximum(jnp.abs(denom), 1.0)
        cell = cell * lax.rsqrt(jnp.mean(cell * cell, axis=0, keepdims=True) + EPSILON)
        outs.append(cell * jax.nn.sigmoid(outgate))
        key_ref[h] = keys
        value_ref[h] = values
        norm_ref[h] = carried * normer + fresh * keys
    head_ref[...] = (jnp.concatenate(outs, axis=0).T * gain_ref[...]).astype(BF16)


def mix_kernel(cols, own_ref, got_ref, w_own_ref, w_got_ref, keep_ref, *out_refs):
    own, got = own_ref[...], got_ref[...]
    for k, out_ref in enumerate((keep_ref,) + out_refs):
        at = slice(k * cols, (k + 1) * cols)
        value = jnp.dot(own, w_own_ref[:, at], preferred_element_type=F32)
        value = value + jnp.dot(got, w_got_ref[:, at], preferred_element_type=F32)
        out_ref[...] = value.astype(out_ref.dtype)


def after_kernel(done_ref, *refs):
    total = refs[0][...]
    for ref in refs[1:-1]:
        total = total + ref[...].astype(F32)
    refs[-1][...] = total.astype(BF16)


def route_kernel(per_group, normed_ref, group_ref, expert_ref, ids_ref, at_ref, *refs):
    high_ref, low_ref = refs
    rows, slots = high_ref.shape
    groups, experts = group_ref.shape[0], expert_ref.shape[0]
    group_exp = jnp.exp(dot(group_ref[...], normed_ref[...], 1, 1))
    group_prob = group_exp / jnp.sum(group_exp, axis=0, keepdims=True)
    logits = dot(expert_ref[...], normed_ref[...], 1, 1)
    expert_iota = lax.broadcasted_iota(jnp.int32, (experts, rows), 0)
    group_iota = lax.broadcasted_iota(jnp.int32, (groups, rows), 0)
    slot_iota = lax.broadcasted_iota(jnp.int32, (slots, rows), 0)
    chosen, shares = [], []
    for j in range(ids_ref.shape[0]):
        ids = ids_ref[j : j + 1, :]
        hot = expert_iota == ids
        chosen.append(jnp.exp(jnp.sum(jnp.where(hot, logits, 0.0), axis=0, keepdims=True)))
        first = group_iota * per_group
        hot = (first <= ids) & (ids < first + per_group)
        shares.append(jnp.sum(jnp.where(hot, group_prob, 0.0), axis=0, keepdims=True))
    total = functools.reduce(lambda x, y: x + y, chosen)
    combine = jnp.zeros((slots, rows), F32)
    for j, (value, share) in enumerate(zip(chosen, shares)):
        weight = share * value / total
        combine = combine + jnp.where(slot_iota == at_ref[j : j + 1, :], weight, 0.0)
    combine = combine.T
    high = combine.astype(BF16)
    high_ref[...] = high
    low_ref[...] = (combine - high.astype(F32)).astype(BF16)


def dispatch_kernel(chips, cols, capacity, *refs):
    own_refs = refs[:chips]
    other_ref, gain_ref, pick_ref = refs[chips : chips + 3]
    normed_ref, out_refs, full_ref = refs[chips + 3], refs[chips + 4 : -1], refs[-1]
    core = lax.axis_index("tp") % CORES
    for k in range(chips):
        full_ref[:, block_cols(k, core, cols)] = own_refs[k][...].astype(F32)
        full_ref[:, block_cols(k, 1 - core, cols)] = other_ref[
            :, k * cols : (k + 1) * cols
        ].astype(F32)
    full = full_ref[...]
    factor = lax.rsqrt(jnp.sum(full * full, axis=1, keepdims=True) / full.shape[1] + EPSILON)
    normed = (full * factor * gain_ref[...]).astype(BF16)
    normed_ref[...] = normed
    picked = jnp.dot(pick_ref[...], normed, preferred_element_type=F32)
    for k, out_ref in enumerate(out_refs):
        out_ref[...] = picked[k * capacity : (k + 1) * capacity].astype(BF16)


def expert_kernel(x_ref, *refs):
    weights, out_ref = refs[:6], refs[6]
    x = x_ref[...]
    result = None
    for gate_ref, up_ref, down_ref in (weights[:3], weights[3:]):
        gate = jnp.dot(x, gate_ref[...], preferred_element_type=F32)
        up = jnp.dot(x, up_ref[...], preferred_element_type=F32)
        units = (jax.nn.silu(gate) * up).astype(BF16)
        part = jnp.dot(units, down_ref[...], preferred_element_type=F32)
        result = part if result is None else result + part
    out_ref[...] = result.astype(BF16)


def combine_kernel(chips, cols, blocks, *refs):
    y_refs = refs[:blocks]
    high_ref, low_ref, away_ref, keep_ref = refs[blocks:]
    core = lax.axis_index("tp") % CORES
    for k in range(chips):
        at = slice(k * cols, (k + 1) * cols)
        for target, out_ref in ((1 - core, away_ref), (core, keep_ref)):
            ds = block_cols(k, target, cols)
            y = jnp.concatenate([ref[:, ds] for ref in y_refs], axis=0)
            value = jnp.dot(high_ref[...], y, preferred_element_type=F32)
            value = value + jnp.dot(low_ref[...], y, preferred_element_type=F32)
            out_ref[:, at] = value.astype(out_ref.dtype)


def per_device(
    resid,
    norm1_gain,
    w_query,
    w_key,
    w_value,
    w_outgate,
    w_igate,
    w_fgate,
    forget_bias,
    head_gain,
    w_out,
    state_matrix,
    state_norm,
    state_max,
    norm2_gain,
    group_router,
    expert_router,
    expert_ids,
    exp_gate,
    exp_up,
    exp_down,
):
    rows, width = resid.shape
    heads, size = state_matrix.shape[1], state_matrix.shape[2]
    ep_count, tp_count = lax.axis_size("ep"), lax.axis_size("tp")
    chips = tp_count // CORES
    cols = width // tp_count
    depth = w_query.shape[0]
    experts_all, groups = expert_router.shape[1], group_router.shape[1]
    per_group = experts_all // groups
    topk = expert_ids.shape[1]
    local_experts, _, _ = exp_gate.shape
    assert local_experts == CORES
    capacity = max(2, 3 * rows * topk // (2 * experts_all))
    half = chips * cols
    others = range(1, ep_count)

    normed, own_resid, *blocks = call(
        functools.partial(norm_kernel, range(ep_count), depth, cols),
        [((rows, width), BF16), ((rows, cols), F32)] + [((rows, depth), BF16)] * ep_count,
        resid,
        norm1_gain[None, :],
        far=(0, 1),
        scratch=[
            pltpu.VMEM((rows, width), BF16),
            pltpu.VMEM((1, width), F32),
            pltpu.SemaphoreType.DMA((2,)),
        ],
    )
    arrived = [ep_send(blocks[k], k) for k in others]
    matrix = state_matrix.transpose(1, 2, 3, 0)
    normer = state_norm.transpose(1, 2, 0)
    weights = (w_query, w_key, w_value, w_outgate)
    all_heads = w_igate.shape[1]
    *weights, gates, new_max = call(
        functools.partial(gates_kernel, heads, len(weights)),
        [(value.shape, value.dtype) for value in weights]
        + [((2 * heads, rows), F32), ((heads, rows), F32)],
        normed,
        w_igate.T,
        w_fgate.T,
        forget_bias[None, :],
        state_max.T,
        *weights,
        far=range(1, 5 + len(weights)),
        scratch=[
            pltpu.VMEM((all_heads, width), BF16),
            pltpu.VMEM((all_heads, width), BF16),
            pltpu.VMEM((1, all_heads), F32),
            pltpu.VMEM((heads, rows), F32),
            pltpu.VMEM((2 * all_heads, rows), F32),
            pltpu.SemaphoreType.DMA((4 + len(weights),)),
        ],
    )
    span = 4 * heads * size
    (own,) = call(project_kernel, [((rows, span), F32)], blocks[0], *weights)
    parts, sent = [], []
    for k in others:
        (part,) = call(project_kernel, [((rows, span), BF16)], arrived[k - 1], *weights)
        parts.append(part)
        sent.append(ep_send(part, k))

    stage_outs = [(value.shape, value.dtype) for value in (matrix, normer)]
    stage_outs += [((heads * size, half), BF16)] * 2
    matrix, normer, w_own, w_sent = call(
        functools.partial(stage_kernel, len(parts), 2, chips, cols),
        stage_outs,
        *parts,
        w_out,
        matrix,
        normer,
        far=range(len(parts), len(parts) + 3),
        unread=range(len(parts)),
        scratch=[pltpu.SemaphoreType.DMA((2 + 2 * chips,))],
        limit=16,
    )
    w_got = core_send(w_sent)

    pair = (exp_gate, exp_up, exp_down)
    slots = ep_count * capacity
    *mine_and_theirs, picks, places = call(
        functools.partial(swap_kernel, len(pair), experts_all),
        [(value.shape[1:], value.dtype) for value in pair for _ in range(2)]
        + [((slots, rows), BF16), ((topk, rows), jnp.int32)],
        w_sent,
        expert_ids.T,
        *pair,
        far=range(2, 2 + len(pair)),
        unread=(0,),
        scratch=[pltpu.SemaphoreType.DMA((2 * len(pair),))],
        limit=8,
    )
    expert_mine = mine_and_theirs[::2]
    expert_got = [core_send(value) for value in mine_and_theirs[1::2]]

    head_out, key_rows, value_rows, new_normer = call(
        functools.partial(cell_kernel, heads, size, ep_count - 1),
        [((rows, heads * size), BF16)] + [((heads, size, rows), F32)] * 3,
        own,
        *sent,
        gates,
        matrix,
        normer,
        head_gain[None, :],
        mine_and_theirs[0],
        w_got,
        unread=(ep_count + 4, ep_count + 5),
        scratch=[pltpu.VMEM((span, rows), F32)],
        limit=20,
    )

    mix_own, *mix_sent = call(
        functools.partial(mix_kernel, cols),
        [((rows, cols), F32)] + [((rows, cols), BF16)] * (chips - 1),
        head_out,
        core_send(head_out),
        w_own,
        w_got,
    )
    mix_got = [chip_send(mix_sent[k - 1], k) for k in range(1, chips)]

    new_matrix, done = call(
        functools.partial(update_kernel, heads, size),
        [((heads, size, size, rows), F32), ((8, 128), F32)],
        mix_sent[-1],
        matrix,
        key_rows,
        value_rows,
        gates,
        unread=(0,),
        far_out=(0,),
        scratch=[pltpu.VMEM((2, size, size, rows), F32), pltpu.SemaphoreType.DMA((2,))],
        limit=14,
    )

    (after_cols,) = call(
        after_kernel,
        [((rows, cols), BF16)],
        done,
        own_resid,
        mix_own,
        *mix_got,
        unread=(0,),
        limit=4,
    )
    after_parts = [after_cols] + [chip_send(after_cols, k) for k in range(1, chips)]
    after_other = core_send(jnp.concatenate(after_parts, axis=1))

    normed2, *buffers = call(
        functools.partial(dispatch_kernel, chips, cols, capacity),
        [((rows, width), BF16)] + [((capacity, width), BF16)] * ep_count,
        *after_parts,
        after_other,
        norm2_gain[None, :],
        picks,
        scratch=[pltpu.VMEM((rows, width), F32)],
        limit=10,
    )
    taken = [buffers[0]] + [ep_send(buffers[k], k) for k in others]

    combine_high, combine_low = call(
        functools.partial(route_kernel, per_group),
        [((rows, slots), BF16)] * 2,
        normed2,
        group_router.T,
        expert_router.T,
        expert_ids.T,
        places,
    )

    terms = []
    for k in range(ep_count):
        (part,) = call(
            expert_kernel,
            [((capacity, width), BF16)],
            taken[k],
            *expert_mine,
            *expert_got,
            limit=12,
        )
        terms.append(part)
    back = [terms[0]] + [ep_send(terms[k], k) for k in others]
    moe_away, moe_keep = call(
        functools.partial(combine_kernel, chips, cols, ep_count),
        [((rows, half), BF16), ((rows, half), F32)],
        *back,
        combine_high,
        combine_low,
    )
    moe = moe_keep + core_send(moe_away).astype(F32)
    moe_parts = [moe[:, k * cols : (k + 1) * cols] for k in range(chips)]
    moe_got = [chip_send(moe_parts[k].astype(BF16), k) for k in range(1, chips)]
    final = after_cols.astype(F32) + moe_parts[0]
    for value in moe_got:
        final = final + value.astype(F32)
    return (
        final.astype(BF16),
        new_matrix.transpose(3, 0, 1, 2),
        new_normer.transpose(2, 0, 1),
        new_max.T,
    )


def solution(mesh):
    in_specs = (
        P("ep", None),
        P(),
        P("ep", "tp"),
        P("ep", "tp"),
        P("ep", "tp"),
        P("ep", "tp"),
        P(),
        P(),
        P(),
        P("tp"),
        P("tp", None),
        P("ep", "tp", None, None),
        P("ep", "tp", None),
        P("ep", "tp"),
        P(),
        P(),
        P(),
        P("ep", None),
        P("ep", None, "tp"),
        P("ep", None, "tp"),
        P("ep", "tp", None),
    )
    out_specs = (P("ep", "tp"), P("ep", "tp", None, None), P("ep", "tp", None), P("ep", "tp"))
    return jax.shard_map(
        per_device, mesh=mesh, in_specs=in_specs, out_specs=out_specs, check_vma=False
    )
```

profile of v0, /device:TPU:0, one launch (start us, length us, event | category | flops | bytes accessed | tf_op | source)
XLA Modules:
  0.0 90.6 jit_solution(8331176753378522536)
XLA Ops:
  0.6 1.3 %shard_map.228 = (bf16[128,2048]{1,0:T(8,128)(2,1)S(1)}, f32[128,256]{1,0:T(8,128)S(1)}, bf16[128,512]{1,0:T(8,128)(2,1)S(1)}, bf16[128,512]{1,0:T(8,128)(2,1)S(...) custom-call(bf16[128,2048]{1,0:T(8,128)(2,1)} %resid_ref.1, f32[1,2048]{1,0:T(1,128)} %bitcast.25), custom_call_target="tpu_custom_call" | custom-call | tf_op jit(solution)/shard_map/pallas_call | solution.py:43
  2.0 4.0 %collective-permute-start.4 = (bf16[128,512]{1,0:T(8,128)(2,1)S(1)}, bf16[128,512]{1,0:T(8,128)(2,1)S(1)}, u32[]{:S(2)}, u32[]{:S(2)}) collective-permute-start(bf16[128,512]{1,0:T(8,128)(2,1)S(1)} %get-tuple-element.55), channel_id=1, source_target_pairs={{0,24},{8,16},{16,8},{24,0},{1,25},{9,17},{17,9},{25,1},{2,26},{10... | collective-permute-start | bytes 393224 | tf_op jit(solution)/shard_map/ppermute | solution.py:19
  6.6 2.1 %shard_map.229 = (bf16[512,256]{1,0:T(8,128)(2,1)S(1)}, bf16[512,256]{1,0:T(8,128)(2,1)S(1)}, bf16[512,256]{1,0:T(8,128)(2,1)S(1)}, bf16[512,256]{1,0:T(8,128)(2...) custom-call(bf16[128,2048]{1,0:T(8,128)(2,1)S(1)} %get-tuple-element.48.normed_ref, bf16[32,2048]{1,0:T(8,128)(2,1)} %bitcast.23, ...), custom_call_target="tpu_custom_call" | custom-call | tf_op jit(solution)/shard_map/pallas_call | solution.py:43
  8.7 1.1 %collective-permute-done.4.x_ref = bf16[128,512]{1,0:T(8,128)(2,1)S(1)} collective-permute-done((bf16[128,512]{1,0:T(8,128)(2,1)S(1)}, bf16[128,512]{1,0:T(8,128)(2,1)S(1)}, u32[]{:S(2)}, u32[]{:S(2)}) %collective-permute-start.4) | collective-permute-done | bytes 131104 | tf_op jit(solution)/shard_map/ppermute | solution.py:19
  10.2 2.1 %collective-permute-done.2.x_ref = bf16[128,512]{1,0:T(8,128)(2,1)S(1)} collective-permute-done((bf16[128,512]{1,0:T(8,128)(2,1)S(1)}, bf16[128,512]{1,0:T(8,128)(2,1)S(1)}, u32[]{:S(2)}, u32[]{:S(2)}) %collective-permute-start.2) | collective-permute-done | bytes 131104 | tf_op jit(solution)/shard_map/ppermute | solution.py:19
  12.9 3.7 %shard_map.234 = (f32[4,64,64,128]{3,2,1,0:T(8,128)S(1)}, f32[4,64,128]{2,1,0:T(8,128)S(1)}, bf16[256,1024]{1,0:T(8,128)(2,1)S(1)}, bf16[256,1024]{1,0:T(8,128)(2,1)S(1)}) custom-call(bf16[128,1024]{1,0:T(8,128)(2,1)S(1)} %shard_map.231.refs_0_, bf16[128,1024]{1,0:T(8,128)(2,1)S(1)} %shard_map.232.refs_1_, bf16[128,1024]{1,0:T(8,128)(2,1)S(1)} %shard_map.233.refs_2_, ...), custom_call_target="tpu_custom_call" | custom-call | tf_op jit(solution)/shard_map/pallas_call | solution.py:43
  16.7 1.7 %collective-permute-start.1 = (bf16[128,1024]{1,0:T(8,128)(2,1)S(1)}, bf16[128,1024]{1,0:T(8,128)(2,1)S(1)}, u32[]{:S(2)}, u32[]{:S(2)}) collective-permute-start(bf16[128,1024]{1,0:T(8,128)(2,1)S(1)} %shard_map.231.refs_0_), channel_id=1, source_target_pairs={{0,8},{8,0},{16,24},{24,16},{1,9},{9,1},{17,25},{25,17},{2,10},{10... | collective-permute-start | bytes 786440 | tf_op jit(solution)/shard_map/ppermute | solution.py:19
  18.5 0.7 collective-permute-start.3
  19.2 1.1 %collective-permute-start.5 = (bf16[128,1024]{1,0:T(8,128)(2,1)S(1)}, bf16[128,1024]{1,0:T(8,128)(2,1)S(1)}, u32[]{:S(2)}, u32[]{:S(2)}) collective-permute-start(bf16[128,1024]{1,0:T(8,128)(2,1)S(1)} %shard_map.233.refs_2_), channel_id=1, source_target_pairs={{0,24},{8,16},{16,8},{24,0},{1,25},{9,17},{17,9},{25,1},{2,26},{10... | collective-permute-start | bytes 786440 | tf_op jit(solution)/shard_map/ppermute | solution.py:19
  20.6 1.9 %shard_map.235 = (bf16[2048,128]{1,0:T(8,128)(2,1)S(1)}, bf16[2048,128]{1,0:T(8,128)(2,1)S(1)}, bf16[2048,128]{1,0:T(8,128)(2,1)S(1)}, bf16[2048,128]{1,0:T(8,12...) custom-call(bf16[256,1024]{1,0:T(8,128)(2,1)S(1)} %get-tuple-element, ...), custom_call_target="tpu_custom_call" | custom-call | tf_op jit(solution)/shard_map/pallas_call | solution.py:43
  22.5 3.5 %collective-permute-done.1.refs_1_ = bf16[128,1024]{1,0:T(8,128)(2,1)S(1)} collective-permute-done((bf16[128,1024]{1,0:T(8,128)(2,1)S(1)}, bf16[128,1024]{1,0:T(8,128)(2,1)S(1)}, u32[]{:S(2)}, u32[]{:S(2)}) %collective-permute-start.1) | collective-permute-done | bytes 262176 | tf_op jit(solution)/shard_map/ppermute | solution.py:19
  26.0 6.5 %collective-permute-done.3.refs_2_ = bf16[128,1024]{1,0:T(8,128)(2,1)S(1)} collective-permute-done((bf16[128,1024]{1,0:T(8,128)(2,1)S(1)}, bf16[128,1024]{1,0:T(8,128)(2,1)S(1)}, u32[]{:S(2)}, u32[]{:S(2)}) %collective-permute-start.3) | collective-permute-done | bytes 262176 | tf_op jit(solution)/shard_map/ppermute | solution.py:19
  32.5 1.8 %shard_map.236 = (bf16[128,256]{1,0:T(8,128)(2,1)S(1)}, f32[4,64,128]{2,1,0:T(8,128)S(1)}, f32[4,64,128]{2,1,0:T(8,128)S(1)}, f32[4,64,128]{2,1,0:T(8,128)}) custom-call(f32[128,1024]{1,0:T(8,128)S(1)} %shard_map.230.refs_0_, bf16[128,1024]{1,0:T(8,128)(2,1)S(1)} %collective-permute-done.1.refs_1_, bf16[128,1024]{1,0:T(8,128)(2,1)S(1)} %collective-permute-done.3.refs_2_, ...), custom_call_target="tpu_custom_call" | custom-call | tf_op jit(solution)/shard_map/pallas_call | solution.py:43
  34.2 0.5 collective-permute-start.15
  34.8 0.7 collective-permute-done.7.got_ref
  35.8 1.6 %collective-permute-start.8 = (bf16[128,256]{1,0:T(8,128)(2,1)S(1)}, bf16[128,256]{1,0:T(8,128)(2,1)S(1)}, u32[]{:S(2)}, u32[]{:S(2)}) collective-permute-start(bf16[128,256]{1,0:T(8,128)(2,1)S(1)} %get-tuple-element.69), channel_id=1, source_target_pairs={{0,2},{1,3},{2,0},{3,1},{4,6},{5,7},{6,4},{7,5},{8,10},{9,11},{10,... | collective-permute-start | bytes 196616 | tf_op jit(solution)/shard_map/ppermute | solution.py:24
  37.5 2.6 %collective-permute-start.9 = (bf16[128,256]{1,0:T(8,128)(2,1)S(1)}, bf16[128,256]{1,0:T(8,128)(2,1)S(1)}, u32[]{:S(2)}, u32[]{:S(2)}) collective-permute-start(bf16[128,256]{1,0:T(8,128)(2,1)S(1)} %get-tuple-element.70), channel_id=1, source_target_pairs={{0,4},{1,5},{2,6},{3,7},{4,0},{5,1},{6,2},{7,3},{8,12},{9,13},{10,... | collective-permute-start | bytes 196616 | tf_op jit(solution)/shard_map/ppermute | solution.py:24
  40.3 3.8 %shard_map.238 = (f32[4,64,64,128]{3,2,1,0:T(8,128)}, f32[8,128]{1,0:T(8,128)S(1)}) custom-call(bf16[128,256]{1,0:T(8,128)(2,1)S(1)} %get-tuple-element.63.after_ref, f32[4,64,64,128]{3,2,1,0:T(8,128)S(1)} %get-tuple-element.57.refs_5_.matrix_ref, f32[4,64,128]{2,1,0:T(8,128)S(1)} %get-tuple-element.64.key_ref, ...), custom_call_target="tpu_custom_call" | custom-call | tf_op jit(solution)/shard_map/pallas_call | solution.py:43
  44.1 0.9 collective-permute-done.9.refs_3_
  45.0 1.2 %collective-permute-done.10.refs_4_ = bf16[128,256]{1,0:T(8,128)(2,1)S(1)} collective-permute-done((bf16[128,256]{1,0:T(8,128)(2,1)S(1)}, bf16[128,256]{1,0:T(8,128)(2,1)S(1)}, u32[]{:S(2)}, u32[]{:S(2)}) %collective-permute-start.10) | collective-permute-done | bytes 65568 | tf_op jit(solution)/shard_map/ppermute | solution.py:24
  46.3 2.1 %collective-permute-start.13 = (bf16[128,256]{1,0:T(8,128)(2,1)S(1)}, bf16[128,256]{1,0:T(8,128)(2,1)S(1)}, u32[]{:S(2)}, u32[]{:S(2)}) collective-permute-start(bf16[128,256]{1,0:T(8,128)(2,1)S(1)} %shard_map.239.refs_0_), channel_id=1, source_target_pairs={{0,6},{1,7},{2,4},{3,5},{4,2},{5,3},{6,0},{7,1},{8,14},{9,15},{10,... | collective-permute-start | bytes 196616 | tf_op jit(solution)/shard_map/ppermute | solution.py:24
  48.6 2.1 %collective-permute-start.11 = (bf16[128,256]{1,0:T(8,128)(2,1)S(1)}, bf16[128,256]{1,0:T(8,128)(2,1)S(1)}, u32[]{:S(2)}, u32[]{:S(2)}) collective-permute-start(bf16[128,256]{1,0:T(8,128)(2,1)S(1)} %shard_map.239.refs_0_), channel_id=1, source_target_pairs={{0,2},{1,3},{2,0},{3,1},{4,6},{5,7},{6,4},{7,5},{8,10},{9,11},{10,... | collective-permute-start | bytes 196616 | tf_op jit(solution)/shard_map/ppermute | solution.py:24
  50.7 2.4 %collective-permute-done.13.refs_3_ = bf16[128,256]{1,0:T(8,128)(2,1)S(1)} collective-permute-done((bf16[128,256]{1,0:T(8,128)(2,1)S(1)}, bf16[128,256]{1,0:T(8,128)(2,1)S(1)}, u32[]{:S(2)}, u32[]{:S(2)}) %collective-permute-start.13) | collective-permute-done | bytes 65568 | tf_op jit(solution)/shard_map/ppermute | solution.py:24
  53.1 1.3 %collective-permute-done.12.refs_2_ = bf16[128,256]{1,0:T(8,128)(2,1)S(1)} collective-permute-done((bf16[128,256]{1,0:T(8,128)(2,1)S(1)}, bf16[128,256]{1,0:T(8,128)(2,1)S(1)}, u32[]{:S(2)}, u32[]{:S(2)}) %collective-permute-start.12) | collective-permute-done | bytes 65568 | tf_op jit(solution)/shard_map/ppermute | solution.py:24
  54.5 1.5 %collective-permute-done.14.refs_4_ = bf16[128,1024]{1,0:T(8,128)(2,1)S(1)} collective-permute-done((bf16[128,1024]{1,0:T(8,128)(2,1)S(1)}, bf16[128,1024]{1,0:T(8,128)(2,1)S(1)}, u32[]{:S(2)}, u32[]{:S(2)}) %collective-permute-start.14) | collective-permute-done | bytes 262176 | tf_op jit(solution)/shard_map/ppermute | solution.py:29
  56.0 0.6 shard_map.240
  56.6 0.6 collective-permute-start.18
  57.2 1.5 %collective-permute-start.20 = (bf16[48,2048]{1,0:T(8,128)(2,1)S(1)}, bf16[48,2048]{1,0:T(8,128)(2,1)S(1)}, u32[]{:S(2)}, u32[]{:S(2)}) collective-permute-start(bf16[48,2048]{1,0:T(8,128)(2,1)S(1)} %get-tuple-element.79), channel_id=1, source_target_pairs={{0,16},{8,24},{16,0},{24,8},{1,17},{9,25},{17,1},{25,9},{2,18},{10... | collective-permute-start | bytes 589832 | tf_op jit(solution)/shard_map/ppermute | solution.py:19
  58.7 1.4 %collective-permute-start.22 = (bf16[48,2048]{1,0:T(8,128)(2,1)S(1)}, bf16[48,2048]{1,0:T(8,128)(2,1)S(1)}, u32[]{:S(2)}, u32[]{:S(2)}) collective-permute-start(bf16[48,2048]{1,0:T(8,128)(2,1)S(1)} %get-tuple-element.80), channel_id=1, source_target_pairs={{0,24},{8,16},{16,8},{24,0},{1,25},{9,17},{17,9},{25,1},{2,26},{10... | collective-permute-start | bytes 589832 | tf_op jit(solution)/shard_map/ppermute | solution.py:19
  60.1 4.3 %collective-permute-done.18.x_ref = bf16[48,2048]{1,0:T(8,128)(2,1)S(1)} collective-permute-done((bf16[48,2048]{1,0:T(8,128)(2,1)S(1)}, bf16[48,2048]{1,0:T(8,128)(2,1)S(1)}, u32[]{:S(2)}, u32[]{:S(2)}) %collective-permute-start.18) | collective-permute-done | bytes 196640 | tf_op jit(solution)/shard_map/ppermute | solution.py:19
  64.4 0.7 shard_map.242
  65.1 0.6 collective-permute-start.19
  65.7 0.7 collective-permute-done.20.x_ref
  66.4 0.7 shard_map.243
  67.1 3.0 %collective-permute-start.21 = (bf16[48,2048]{1,0:T(8,128)(2,1)S(1)}, bf16[48,2048]{1,0:T(8,128)(2,1)S(1)}, u32[]{:S(2)}, u32[]{:S(2)}) collective-permute-start(bf16[48,2048]{1,0:T(8,128)(2,1)S(1)} %shard_map.243), channel_id=1, source_target_pairs={{0,16},{8,24},{16,0},{24,8},{1,17},{9,25},{17,1},{25,9},{2,18},{10... | collective-permute-start | bytes 589832 | tf_op jit(solution)/shard_map/ppermute | solution.py:19
  70.0 0.7 shard_map.244
  70.7 1.4 %collective-permute-start.23 = (bf16[48,2048]{1,0:T(8,128)(2,1)S(1)}, bf16[48,2048]{1,0:T(8,128)(2,1)S(1)}, u32[]{:S(2)}, u32[]{:S(2)}) collective-permute-start(bf16[48,2048]{1,0:T(8,128)(2,1)S(1)} %shard_map.244), channel_id=1, source_target_pairs={{0,24},{8,16},{16,8},{24,0},{1,25},{9,17},{17,9},{25,1},{2,26},{10... | collective-permute-start | bytes 589832 | tf_op jit(solution)/shard_map/ppermute | solution.py:19
  72.1 0.5 shard_map.245
  72.6 0.7 shard_map.241.refs_0_
  73.3 4.6 %collective-permute-done.21.refs_2_ = bf16[48,2048]{1,0:T(8,128)(2,1)S(1)} collective-permute-done((bf16[48,2048]{1,0:T(8,128)(2,1)S(1)}, bf16[48,2048]{1,0:T(8,128)(2,1)S(1)}, u32[]{:S(2)}, u32[]{:S(2)}) %collective-permute-start.21) | collective-permute-done | bytes 196640 | tf_op jit(solution)/shard_map/ppermute | solution.py:19
  78.4 1.5 %collective-permute-done.24 = bf16[128,1024]{1,0:T(8,128)(2,1)S(1)} collective-permute-done((bf16[128,1024]{1,0:T(8,128)(2,1)S(1)}, bf16[128,1024]{1,0:T(8,128)(2,1)S(1)}, u32[]{:S(2)}, u32[]{:S(2)}) %collective-permute-start.24) | collective-permute-done | bytes 262176 | tf_op jit(solution)/shard_map/ppermute | solution.py:29
  80.1 0.7 collective-permute-start.25
  80.7 2.0 %collective-permute-start.27 = (bf16[128,256]{1,0:T(8,128)(2,1)S(1)}, bf16[128,256]{1,0:T(8,128)(2,1)S(1)}, u32[]{:S(2)}, u32[]{:S(2)}) collective-permute-start(bf16[128,256]{1,0:T(8,128)(2,1)S(1)} %get-tuple-element.93), channel_id=1, source_target_pairs={{0,6},{1,7},{2,4},{3,5},{4,2},{5,3},{6,0},{7,1},{8,14},{9,15},{10,... | collective-permute-start | bytes 196616 | tf_op jit(solution)/shard_map/ppermute | solution.py:24
  82.8 0.8 collective-permute-start.26
  83.6 0.8 collective-permute-done.25
  84.4 2.9 %collective-permute-done.27 = bf16[128,256]{1,0:T(8,128)(2,1)S(1)} collective-permute-done((bf16[128,256]{1,0:T(8,128)(2,1)S(1)}, bf16[128,256]{1,0:T(8,128)(2,1)S(1)}, u32[]{:S(2)}, u32[]{:S(2)}) %collective-permute-start.27) | collective-permute-done | bytes 65568 | tf_op jit(solution)/shard_map/ppermute | solution.py:24
  87.3 2.6 %collective-permute-done.26 = bf16[128,256]{1,0:T(8,128)(2,1)S(1)} collective-permute-done((bf16[128,256]{1,0:T(8,128)(2,1)S(1)}, bf16[128,256]{1,0:T(8,128)(2,1)S(1)}, u32[]{:S(2)}, u32[]{:S(2)}) %collective-permute-start.26) | collective-permute-done | bytes 65568 | tf_op jit(solution)/shard_map/ppermute | solution.py:24
  89.9 0.7 fusion.3
  (41 shorter events, 3.6 us)
Async XLA Ops:
  2.0 7.9 %collective-permute-start.4 = (bf16[128,512]{1,0:T(8,128)(2,1)S(1)}, bf16[128,512]{1,0:T(8,128)(2,1)S(1)}, u32[]{:S(2)}, u32[]{:S(2)}) collective-permute-start(bf16[128,512]{1,0:T(8,128)(2,1)S(1)} %get-tuple-element.55), channel_id=1, source_target_pairs={{0,24},{8,16},{16,8},{24,0},{1,25},{9,17},{17,9},{25,1},{2,26},{10... | collective-permute-start | bytes 393224 | tf_op jit(solution)/shard_map/ppermute | solution.py:19
  6.0 6.3 %collective-permute-start.2 = (bf16[128,512]{1,0:T(8,128)(2,1)S(1)}, bf16[128,512]{1,0:T(8,128)(2,1)S(1)}, u32[]{:S(2)}, u32[]{:S(2)}) collective-permute-start(bf16[128,512]{1,0:T(8,128)(2,1)S(1)} %get-tuple-element.54), channel_id=1, source_target_pairs={{0,16},{8,24},{16,0},{24,8},{1,17},{9,25},{17,1},{25,9},{2,18},{10... | collective-permute-start | bytes 393224 | tf_op jit(solution)/shard_map/ppermute | solution.py:19
  6.5 6.1 %collective-permute-start = (bf16[128,512]{1,0:T(8,128)(2,1)S(1)}, bf16[128,512]{1,0:T(8,128)(2,1)S(1)}, u32[]{:S(2)}, u32[]{:S(2)}) collective-permute-start(bf16[128,512]{1,0:T(8,128)(2,1)S(1)} %get-tuple-element.53), channel_id=1, source_target_pairs={{0,8},{8,0},{16,24},{24,16},{1,9},{9,1},{17,25},{25,17},{2,10},{10... | collective-permute-start | bytes 393224 | tf_op jit(solution)/shard_map/ppermute | solution.py:19
  8.7 11.9 %copy-start.3 = (s32[128,2]{0,1:T(2,128)S(1)}, s32[128,2]{0,1:T(2,128)}, u32[]{:S(2)}) copy-start(s32[128,2]{0,1:T(2,128)} %param.38) | copy-start | bytes 3076
  12.6 19.9 %copy-start.4 = (f32[256]{0:T(256)S(1)}, f32[256]{0:T(256)}, u32[]{:S(2)}) copy-start(f32[256]{0:T(256)} %param.30) | copy-start | bytes 3076
  16.6 15.8 %collective-permute-start.6 = (bf16[256,1024]{1,0:T(8,128)(2,1)S(1)}, bf16[256,1024]{1,0:T(8,128)(2,1)S(1)}, u32[]{:S(2)}, u32[]{:S(2)}) collective-permute-start(bf16[256,1024]{1,0:T(8,128)(2,1)S(1)} %get-tuple-element.59.after_ref), channel_id=1, source_target_pairs={{0,1},{1,0},{2,3},{3,2},{4,5},{5,4},{6,7},{7,6},{8,9},{9,8},{10,11... | collective-permute-start | bytes 1572872 | tf_op jit(solution)/shard_map/ppermute | solution.py:29
  16.7 9.2 %collective-permute-start.1 = (bf16[128,1024]{1,0:T(8,128)(2,1)S(1)}, bf16[128,1024]{1,0:T(8,128)(2,1)S(1)}, u32[]{:S(2)}, u32[]{:S(2)}) collective-permute-start(bf16[128,1024]{1,0:T(8,128)(2,1)S(1)} %shard_map.231.refs_0_), channel_id=1, source_target_pairs={{0,8},{8,0},{16,24},{24,16},{1,9},{9,1},{17,25},{25,17},{2,10},{10... | collective-permute-start | bytes 786440 | tf_op jit(solution)/shard_map/ppermute | solution.py:19
  18.5 14.0 %collective-permute-start.3 = (bf16[128,1024]{1,0:T(8,128)(2,1)S(1)}, bf16[128,1024]{1,0:T(8,128)(2,1)S(1)}, u32[]{:S(2)}, u32[]{:S(2)}) collective-permute-start(bf16[128,1024]{1,0:T(8,128)(2,1)S(1)} %shard_map.232.refs_1_), channel_id=1, source_target_pairs={{0,16},{8,24},{16,0},{24,8},{1,17},{9,25},{17,1},{25,9},{2,18},{10... | collective-permute-start | bytes 786440 | tf_op jit(solution)/shard_map/ppermute | solution.py:19
  19.2 13.3 %collective-permute-start.5 = (bf16[128,1024]{1,0:T(8,128)(2,1)S(1)}, bf16[128,1024]{1,0:T(8,128)(2,1)S(1)}, u32[]{:S(2)}, u32[]{:S(2)}) collective-permute-start(bf16[128,1024]{1,0:T(8,128)(2,1)S(1)} %shard_map.233.refs_2_), channel_id=1, source_target_pairs={{0,24},{8,16},{16,8},{24,0},{1,25},{9,17},{17,9},{25,1},{2,26},{10... | collective-permute-start | bytes 786440 | tf_op jit(solution)/shard_map/ppermute | solution.py:19
  32.4 23.5 %copy-start.2 = (f32[2048]{0:T(1024)S(1)}, f32[2048]{0:T(1024)}, u32[]{:S(2)}) copy-start(f32[2048]{0:T(1024)} %param.35) | copy-start | bytes 24580
  34.2 1.3 %collective-permute-start.7 = (bf16[128,256]{1,0:T(8,128)(2,1)S(1)}, bf16[128,256]{1,0:T(8,128)(2,1)S(1)}, u32[]{:S(2)}, u32[]{:S(2)}) collective-permute-start(bf16[128,256]{1,0:T(8,128)(2,1)S(1)} %get-tuple-element.61.own_ref), channel_id=1, source_target_pairs={{0,1},{1,0},{2,3},{3,2},{4,5},{5,4},{6,7},{7,6},{8,9},{9,8},{10,11... | collective-permute-start | bytes 196616 | tf_op jit(solution)/shard_map/ppermute | solution.py:29
  34.2 24.5 %collective-permute-start.15 = (bf16[2048,128]{1,0:T(8,128)(2,1)S(1)}, bf16[2048,128]{1,0:T(8,128)(2,1)S(1)}, u32[]{:S(2)}, u32[]{:S(2)}) collective-permute-start(bf16[2048,128]{1,0:T(8,128)(2,1)S(1)} %get-tuple-element.75), channel_id=1, source_target_pairs={{0,1},{1,0},{2,3},{3,2},{4,5},{5,4},{6,7},{7,6},{8,9},{9,8},{10,11... | collective-permute-start | bytes 1572872 | tf_op jit(solution)/shard_map/ppermute | solution.py:29
  35.8 8.3 %collective-permute-start.8 = (bf16[128,256]{1,0:T(8,128)(2,1)S(1)}, bf16[128,256]{1,0:T(8,128)(2,1)S(1)}, u32[]{:S(2)}, u32[]{:S(2)}) collective-permute-start(bf16[128,256]{1,0:T(8,128)(2,1)S(1)} %get-tuple-element.69), channel_id=1, source_target_pairs={{0,2},{1,3},{2,0},{3,1},{4,6},{5,7},{6,4},{7,5},{8,10},{9,11},{10,... | collective-permute-start | bytes 196616 | tf_op jit(solution)/shard_map/ppermute | solution.py:24
  37.5 7.5 %collective-permute-start.9 = (bf16[128,256]{1,0:T(8,128)(2,1)S(1)}, bf16[128,256]{1,0:T(8,128)(2,1)S(1)}, u32[]{:S(2)}, u32[]{:S(2)}) collective-permute-start(bf16[128,256]{1,0:T(8,128)(2,1)S(1)} %get-tuple-element.70), channel_id=1, source_target_pairs={{0,4},{1,5},{2,6},{3,7},{4,0},{5,1},{6,2},{7,3},{8,12},{9,13},{10,... | collective-permute-start | bytes 196616 | tf_op jit(solution)/shard_map/ppermute | solution.py:24
  40.1 6.2 %collective-permute-start.10 = (bf16[128,256]{1,0:T(8,128)(2,1)S(1)}, bf16[128,256]{1,0:T(8,128)(2,1)S(1)}, u32[]{:S(2)}, u32[]{:S(2)}) collective-permute-start(bf16[128,256]{1,0:T(8,128)(2,1)S(1)} %get-tuple-element.63.after_ref), channel_id=1, source_target_pairs={{0,6},{1,7},{2,4},{3,5},{4,2},{5,3},{6,0},{7,1},{8,14},{9,15},{10,... | collective-permute-start | bytes 196616 | tf_op jit(solution)/shard_map/ppermute | solution.py:24
  40.3 31.8 %copy-start = (bf16[2048,8]{0,1:T(8,128)(2,1)S(1)}, bf16[2048,8]{0,1:T(8,128)(2,1)}, u32[]{:S(2)}) copy-start(bf16[2048,8]{0,1:T(8,128)(2,1)} %param.37) | copy-start | bytes 98308
  40.3 31.8 %copy-start.1 = (bf16[2048,4]{0,1:T(4,128)(2,1)S(1)}, bf16[2048,4]{0,1:T(4,128)(2,1)}, u32[]{:S(2)}) copy-start(bf16[2048,4]{0,1:T(4,128)(2,1)} %param.36) | copy-start | bytes 49156
  46.3 6.8 %collective-permute-start.13 = (bf16[128,256]{1,0:T(8,128)(2,1)S(1)}, bf16[128,256]{1,0:T(8,128)(2,1)S(1)}, u32[]{:S(2)}, u32[]{:S(2)}) collective-permute-start(bf16[128,256]{1,0:T(8,128)(2,1)S(1)} %shard_map.239.refs_0_), channel_id=1, source_target_pairs={{0,6},{1,7},{2,4},{3,5},{4,2},{5,3},{6,0},{7,1},{8,14},{9,15},{10,... | collective-permute-start | bytes 196616 | tf_op jit(solution)/shard_map/ppermute | solution.py:24
  48.3 6.0 %collective-permute-start.12 = (bf16[128,256]{1,0:T(8,128)(2,1)S(1)}, bf16[128,256]{1,0:T(8,128)(2,1)S(1)}, u32[]{:S(2)}, u32[]{:S(2)}) collective-permute-start(bf16[128,256]{1,0:T(8,128)(2,1)S(1)} %shard_map.239.refs_0_), channel_id=1, source_target_pairs={{0,4},{1,5},{2,6},{3,7},{4,0},{5,1},{6,2},{7,3},{8,12},{9,13},{10,... | collective-permute-start | bytes 196616 | tf_op jit(solution)/shard_map/ppermute | solution.py:24
  48.6 5.7 %collective-permute-start.11 = (bf16[128,256]{1,0:T(8,128)(2,1)S(1)}, bf16[128,256]{1,0:T(8,128)(2,1)S(1)}, u32[]{:S(2)}, u32[]{:S(2)}) collective-permute-start(bf16[128,256]{1,0:T(8,128)(2,1)S(1)} %shard_map.239.refs_0_), channel_id=1, source_target_pairs={{0,2},{1,3},{2,0},{3,1},{4,6},{5,7},{6,4},{7,5},{8,10},{9,11},{10,... | collective-permute-start | bytes 196616 | tf_op jit(solution)/shard_map/ppermute | solution.py:24
  50.7 9.4 %collective-permute-start.16 = (bf16[2048,128]{1,0:T(8,128)(2,1)S(1)}, bf16[2048,128]{1,0:T(8,128)(2,1)S(1)}, u32[]{:S(2)}, u32[]{:S(2)}) collective-permute-start(bf16[2048,128]{1,0:T(8,128)(2,1)S(1)} %get-tuple-element.76), channel_id=1, source_target_pairs={{0,1},{1,0},{2,3},{3,2},{4,5},{5,4},{6,7},{7,6},{8,9},{9,8},{10,11... | collective-permute-start | bytes 1572872 | tf_op jit(solution)/shard_map/ppermute | solution.py:29
  53.1 7.1 %collective-permute-start.17 = (bf16[128,2048]{1,0:T(8,128)(2,1)S(1)}, bf16[128,2048]{1,0:T(8,128)(2,1)S(1)}, u32[]{:S(2)}, u32[]{:S(2)}) collective-permute-start(bf16[128,2048]{1,0:T(8,128)(2,1)S(1)} %get-tuple-element.77), channel_id=1, source_target_pairs={{0,1},{1,0},{2,3},{3,2},{4,5},{5,4},{6,7},{7,6},{8,9},{9,8},{10,11... | collective-permute-start | bytes 1572872 | tf_op jit(solution)/shard_map/ppermute | solution.py:29
  54.4 1.6 %collective-permute-start.14 = (bf16[128,1024]{1,0:T(8,128)(2,1)S(1)}, bf16[128,1024]{1,0:T(8,128)(2,1)S(1)}, u32[]{:S(2)}, u32[]{:S(2)}) collective-permute-start(bf16[128,1024]{1,0:T(8,128)(2,1)S(1)} %pad_maximum_fusion), channel_id=1, source_target_pairs={{0,1},{1,0},{2,3},{3,2},{4,5},{5,4},{6,7},{7,6},{8,9},{9,8},{10,11... | collective-permute-start | bytes 786440 | tf_op jit(solution)/shard_map/ppermute | solution.py:29
  56.6 7.8 %collective-permute-start.18 = (bf16[48,2048]{1,0:T(8,128)(2,1)S(1)}, bf16[48,2048]{1,0:T(8,128)(2,1)S(1)}, u32[]{:S(2)}, u32[]{:S(2)}) collective-permute-start(bf16[48,2048]{1,0:T(8,128)(2,1)S(1)} %get-tuple-element.78), channel_id=1, source_target_pairs={{0,8},{8,0},{16,24},{24,16},{1,9},{9,1},{17,25},{25,17},{2,10},{10... | collective-permute-start | bytes 589832 | tf_op jit(solution)/shard_map/ppermute | solution.py:19
  57.2 9.2 %collective-permute-start.20 = (bf16[48,2048]{1,0:T(8,128)(2,1)S(1)}, bf16[48,2048]{1,0:T(8,128)(2,1)S(1)}, u32[]{:S(2)}, u32[]{:S(2)}) collective-permute-start(bf16[48,2048]{1,0:T(8,128)(2,1)S(1)} %get-tuple-element.79), channel_id=1, source_target_pairs={{0,16},{8,24},{16,0},{24,8},{1,17},{9,25},{17,1},{25,9},{2,18},{10... | collective-permute-start | bytes 589832 | tf_op jit(solution)/shard_map/ppermute | solution.py:19
  58.7 11.3 %collective-permute-start.22 = (bf16[48,2048]{1,0:T(8,128)(2,1)S(1)}, bf16[48,2048]{1,0:T(8,128)(2,1)S(1)}, u32[]{:S(2)}, u32[]{:S(2)}) collective-permute-start(bf16[48,2048]{1,0:T(8,128)(2,1)S(1)} %get-tuple-element.80), channel_id=1, source_target_pairs={{0,24},{8,16},{16,8},{24,0},{1,25},{9,17},{17,9},{25,1},{2,26},{10... | collective-permute-start | bytes 589832 | tf_op jit(solution)/shard_map/ppermute | solution.py:19
  65.1 8.2 %collective-permute-start.19 = (bf16[48,2048]{1,0:T(8,128)(2,1)S(1)}, bf16[48,2048]{1,0:T(8,128)(2,1)S(1)}, u32[]{:S(2)}, u32[]{:S(2)}) collective-permute-start(bf16[48,2048]{1,0:T(8,128)(2,1)S(1)} %shard_map.242), channel_id=1, source_target_pairs={{0,8},{8,0},{16,24},{24,16},{1,9},{9,1},{17,25},{25,17},{2,10},{10... | collective-permute-start | bytes 589832 | tf_op jit(solution)/shard_map/ppermute | solution.py:19
  67.1 10.8 %collective-permute-start.21 = (bf16[48,2048]{1,0:T(8,128)(2,1)S(1)}, bf16[48,2048]{1,0:T(8,128)(2,1)S(1)}, u32[]{:S(2)}, u32[]{:S(2)}) collective-permute-start(bf16[48,2048]{1,0:T(8,128)(2,1)S(1)} %shard_map.243), channel_id=1, source_target_pairs={{0,16},{8,24},{16,0},{24,8},{1,17},{9,25},{17,1},{25,9},{2,18},{10... | collective-permute-start | bytes 589832 | tf_op jit(solution)/shard_map/ppermute | solution.py:19
  70.7 7.2 %collective-permute-start.23 = (bf16[48,2048]{1,0:T(8,128)(2,1)S(1)}, bf16[48,2048]{1,0:T(8,128)(2,1)S(1)}, u32[]{:S(2)}, u32[]{:S(2)}) collective-permute-start(bf16[48,2048]{1,0:T(8,128)(2,1)S(1)} %shard_map.244), channel_id=1, source_target_pairs={{0,24},{8,16},{16,8},{24,0},{1,25},{9,17},{17,9},{25,1},{2,26},{10... | collective-permute-start | bytes 589832 | tf_op jit(solution)/shard_map/ppermute | solution.py:19
  78.4 1.6 %collective-permute-start.24 = (bf16[128,1024]{1,0:T(8,128)(2,1)S(1)}, bf16[128,1024]{1,0:T(8,128)(2,1)S(1)}, u32[]{:S(2)}, u32[]{:S(2)}) collective-permute-start(bf16[128,1024]{1,0:T(8,128)(2,1)S(1)} %get-tuple-element.86), channel_id=1, source_target_pairs={{0,1},{1,0},{2,3},{3,2},{4,5},{5,4},{6,7},{7,6},{8,9},{9,8},{10,11... | collective-permute-start | bytes 786440 | tf_op jit(solution)/shard_map/ppermute | solution.py:29
  80.1 4.3 %collective-permute-start.25 = (bf16[128,256]{1,0:T(8,128)(2,1)S(1)}, bf16[128,256]{1,0:T(8,128)(2,1)S(1)}, u32[]{:S(2)}, u32[]{:S(2)}) collective-permute-start(bf16[128,256]{1,0:T(8,128)(2,1)S(1)} %get-tuple-element.92), channel_id=1, source_target_pairs={{0,2},{1,3},{2,0},{3,1},{4,6},{5,7},{6,4},{7,5},{8,10},{9,11},{10,... | collective-permute-start | bytes 196616 | tf_op jit(solution)/shard_map/ppermute | solution.py:24
  80.7 6.5 %collective-permute-start.27 = (bf16[128,256]{1,0:T(8,128)(2,1)S(1)}, bf16[128,256]{1,0:T(8,128)(2,1)S(1)}, u32[]{:S(2)}, u32[]{:S(2)}) collective-permute-start(bf16[128,256]{1,0:T(8,128)(2,1)S(1)} %get-tuple-element.93), channel_id=1, source_target_pairs={{0,6},{1,7},{2,4},{3,5},{4,2},{5,3},{6,0},{7,1},{8,14},{9,15},{10,... | collective-permute-start | bytes 196616 | tf_op jit(solution)/shard_map/ppermute | solution.py:24
  82.8 7.2 %collective-permute-start.26 = (bf16[128,256]{1,0:T(8,128)(2,1)S(1)}, bf16[128,256]{1,0:T(8,128)(2,1)S(1)}, u32[]{:S(2)}, u32[]{:S(2)}) collective-permute-start(bf16[128,256]{1,0:T(8,128)(2,1)S(1)} %get-tuple-element.94), channel_id=1, source_target_pairs={{0,4},{1,5},{2,6},{3,7},{4,0},{5,1},{6,2},{7,3},{8,12},{9,13},{10,... | collective-permute-start | bytes 196616 | tf_op jit(solution)/shard_map/ppermute | solution.py:24
where the time goes:
time: 90.8 us; the launch traced here: 90.6 us
  waiting for transfers between devices  38.6 us (43%)
  starting transfers between devices  29.9 us (33%)
  Pallas kernels  20.5 us (23%)
    ppermute x12, waiting for transfers between devices, ep_send(): return lax.ppermute(value, 'ep', [(i, i ^ step) for i in range(count)])  22.7 us
    pallas_call x19, Pallas kernels, call(): pl.pallas_call(kernel, out_shape=[jax.ShapeDtypeStruct(shape, dtype) for...  20.5 us
    ppermute x12, starting transfers between devices, ep_send(): return lax.ppermute(value, 'ep', [(i, i ^ step) for i in range(count)])  16.7 us
    ppermute x9, starting transfers between devices, chip_send(): lax.ppermute(value, 'tp', [(i, i ^ CORES * step) for i in range(count)])  12.5 us
    ppermute x9, waiting for transfers between devices, chip_send(): lax.ppermute(value, 'tp', [(i, i ^ CORES * step) for i in range(count)])  12 us
    ppermute x7, waiting for transfers between devices, core_send(): return lax.ppermute(value, 'tp', [(i, i ^ 1) for i in range(count)])  3.8 us
  transfers between devices with their start and end apart: 28, of which 17 were waited for; matrix products, arithmetic and copies ran while one was open for 0% of the time, Pallas kernels for 14%

commit v1 on v0

--- a/solution.py
+++ b/solution.py
@@ -60,49 +60,51 @@
     return pl.ds(pl.multiple_of((chip * CORES + core) * cols, cols), cols)
 
 
-def norm_kernel(steps, depth, cols, resid_ref, gain_ref, normed_ref, own_ref, *refs):
-    block_refs, (rows_ref, row_ref, sems) = refs[:-3], refs[-3:]
+def split_kernel(depth, resid_ref, *refs):
+    out_refs, sems = refs[:-1], refs[-1]
+    copies = []
+    for step, out_ref in enumerate(out_refs):
+        start = pl.multiple_of((lax.axis_index("ep") ^ step) * depth, depth)
+        copies.append(
+            pltpu.make_async_copy(resid_ref.at[:, pl.ds(start, depth)], out_ref, sems.at[step])
+        )
+    for copy in copies:
+        copy.start()
+    for copy in copies:
+        copy.wait()
+
+
+def load_kernel(count, depth, gain_ref, *refs):
+    sources, outs, sems = refs[:count], refs[count : 2 * count], refs[-1]
+    start = pl.multiple_of(lax.axis_index("ep") * depth, depth)
+    pairs = [(gain_ref.at[:, pl.ds(start, depth)], refs[2 * count])] + list(zip(sources, outs))
     copies = [
-        pltpu.make_async_copy(resid_ref, rows_ref, sems.at[0]),
-        pltpu.make_async_copy(gain_ref, row_ref, sems.at[1]),
+        pltpu.make_async_copy(source, target, sems.at[i])
+        for i, (source, target) in enumerate(pairs)
     ]
     for copy in copies:
         copy.start()
     for copy in copies:
         copy.wait()
-    width = rows_ref.shape[1]
+
+
+def gates_step(heads, cols, targets, outs, both_ref):
+    igate_ref, fgate_ref, bias_ref, max_ref, rows_ref, row_ref = targets
+    gates_ref, new_max_ref, factor_ref, own_ref = outs
     wide = rows_ref[...].astype(F32)
-    factor = lax.rsqrt(jnp.sum(wide * wide, axis=1, keepdims=True) / width + EPSILON)
-    normed_ref[...] = (wide * factor * row_ref[...]).astype(BF16)
-    for step, block_ref in zip(steps, block_refs):
-        start = pl.multiple_of((lax.axis_index("ep") ^ step) * depth, depth)
-        block_ref[...] = normed_ref[:, pl.ds(start, depth)]
+    factor = lax.rsqrt(jnp.mean(wide * wide, axis=1, keepdims=True) + EPSILON)
+    normed = (wide * factor * row_ref[...]).astype(BF16)
+    factor_ref[...] = jnp.broadcast_to(factor, factor_ref.shape)
     start = pl.multiple_of(lax.axis_index("tp") * cols, cols)
     own_ref[...] = rows_ref[:, pl.ds(start, cols)].astype(F32)
-
-
-def gates_kernel(heads, count, normed_ref, *refs):
-    gate_args, refs = refs[:4], refs[4:]
-    sources, outs, refs = refs[:count], refs[count : 2 * count], refs[2 * count :]
-    gates_ref, new_max_ref = refs[:2]
-    igate_ref, fgate_ref, bias_ref, max_ref, both_ref, sems = refs[2:]
-    targets = (igate_ref, fgate_ref, bias_ref, max_ref) + tuple(outs)
-    copies = [
-        pltpu.make_async_copy(source, target, sems.at[i])
-        for i, (source, target) in enumerate(zip(tuple(gate_args) + tuple(sources), targets))
-    ]
-    for copy in copies:
-        copy.start()
-    for copy in copies[:4]:
-        copy.wait()
     all_heads = igate_ref.shape[0]
     square = (all_heads, all_heads)
     diagonal = lax.broadcasted_iota(jnp.int32, square, 0) == lax.broadcasted_iota(
         jnp.int32, square, 1
     )
     bias = jnp.sum(jnp.where(diagonal, bias_ref[...], 0.0), axis=1, keepdims=True)
-    both_ref[:all_heads] = dot(igate_ref[...], normed_ref[...], 1, 1)
-    both_ref[all_heads:] = dot(fgate_ref[...], normed_ref[...], 1, 1) + bias
+    both_ref[:all_heads] = dot(igate_ref[...], normed, 1, 1)
+    both_ref[all_heads:] = dot(fgate_ref[...], normed, 1, 1) + bias
     start = lax.axis_index("tp") * heads
     in_gate = both_ref[pl.ds(start, heads)]
     forget = both_ref[pl.ds(all_heads + start, heads)]
@@ -112,44 +114,12 @@
     new_max_ref[...] = new_max
     gates_ref[:heads] = jnp.exp(running - new_max)
     gates_ref[heads:] = jnp.exp(in_gate - new_max)
-    for copy in copies[4:]:
-        copy.wait()
-
-
-def stage_kernel(skip, count, chips, cols, *refs):
-    w_ref, refs = refs[skip], refs[skip + 1 :]
-    sources, outs = refs[:count], refs[count : 2 * count]
-    keep_ref, away_ref, sems = refs[2 * count :]
+
+
+def slots_step(experts, local, ids_ref, picks_ref, at_ref):
     core = lax.axis_index("tp") % CORES
-    pairs = list(zip(sources, outs))
-    for out_ref, target in ((away_ref, 1 - core), (keep_ref, core)):
-        for k in range(chips):
-            at = pl.ds(k * cols, cols)
-            pairs.append((w_ref.at[:, block_cols(k, target, cols)], out_ref.at[:, at]))
-    copies = [
-        pltpu.make_async_copy(source, target, sems.at[i])
-        for i, (source, target) in enumerate(pairs)
-    ]
-    for copy in copies:
-        copy.start()
-    for copy in copies:
-        copy.wait()
-
-
-def swap_kernel(count, experts, after_ref, ids_ref, *refs):
-    sources, outs = refs[:count], refs[count:-3]
-    picks_ref, at_ref, sems = refs[-3:]
-    core = lax.axis_index("tp") % CORES
-    copies = []
-    for i, source in enumerate(sources):
-        for j, index in enumerate((core, 1 - core)):
-            at = 2 * i + j
-            copies.append(pltpu.make_async_copy(source.at[index], outs[at], sems.at[at]))
-    for copy in copies:
-        copy.start()
     topk, rows = ids_ref.shape
     slots = picks_ref.shape[0]
-    local = sources[0].shape[0]
     capacity = slots // (experts // local)
     expert_iota = lax.broadcasted_iota(jnp.int32, (experts, rows), 0)
     hots = [(expert_iota == ids_ref[j : j + 1, :]).astype(F32) for j in range(topk)]
@@ -168,7 +138,35 @@
         at_ref[j : j + 1, :] = at
         picked = picked + (slot_iota == at).astype(F32)
     picks_ref[...] = picked.astype(BF16)
+
+
+def stage_kernel(skip, heads, chips, cols, experts, *refs):
+    ids_ref, refs = refs[skip], refs[skip + 1 :]
+    gate_sources, (w_ref, matrix_ref, normer_ref), pair = refs[:6], refs[6:9], refs[9:12]
+    outs, scratch = refs[12:28], refs[28:]
+    targets, both_ref, sems = scratch[:6], scratch[6], scratch[7]
+    core = lax.axis_index("tp") % CORES
+    away_ref, keep_ref, matrix_out, normer_out = outs[:4]
+    pairs = list(zip(gate_sources, targets))
+    for out_ref, target in ((away_ref, 1 - core), (keep_ref, core)):
+        for k in range(chips):
+            at = pl.ds(k * cols, cols)
+            pairs.append((w_ref.at[:, block_cols(k, target, cols)], out_ref.at[:, at]))
+    for i, source in enumerate(pair):
+        pairs.append((source.at[1 - core], outs[4 + i]))
+        pairs.append((source.at[core], outs[7 + i]))
+    pairs += [(normer_ref, normer_out), (matrix_ref, matrix_out)]
+    copies = [
+        pltpu.make_async_copy(source, target, sems.at[i])
+        for i, (source, target) in enumerate(pairs)
+    ]
     for copy in copies:
+        copy.start()
+    slots_step(experts, pair[0].shape[0], ids_ref, outs[14], outs[15])
+    for copy in copies[:6]:
+        copy.wait()
+    gates_step(heads, cols, targets, outs[10:14], both_ref)
+    for copy in copies[6:]:
         copy.wait()
 
 
@@ -191,23 +189,25 @@
     done_ref[...] = jnp.zeros_like(done_ref)
 
 
-def project_kernel(x_ref, *refs):
+def project_kernel(x_ref, gain_ref, *refs):
     weights, out_ref = refs[:-1], refs[-1]
     cols = weights[0].shape[1]
+    x = (x_ref[...].astype(F32) * gain_ref[...]).astype(BF16)
     for i, w_ref in enumerate(weights):
         out_ref[:, i * cols : (i + 1) * cols] = jnp.dot(
-            x_ref[...], w_ref[...], preferred_element_type=F32
+            x, w_ref[...], preferred_element_type=F32
         ).astype(out_ref.dtype)
 
 
 def cell_kernel(heads, size, received, *refs):
     own_ref = refs[0]
     got_refs = refs[1 : 1 + received]
-    gates_ref, matrix_ref, normer_ref, gain_ref = refs[1 + received : 5 + received]
+    gates_ref, matrix_ref, normer_ref, gain_ref, factor_ref = refs[1 + received : 6 + received]
     head_ref, key_ref, value_ref, norm_ref, turned_ref = refs[-5:]
     total = own_ref[...]
     for ref in got_refs:
         total = total + ref[...].astype(F32)
+    total = total * factor_ref[:, :1]
     turned_ref[...] = total.astype(BF16).astype(F32).T
     span = heads * size
     outs = []
@@ -243,11 +243,15 @@
         out_ref[...] = value.astype(out_ref.dtype)
 
 
-def after_kernel(done_ref, *refs):
-    total = refs[0][...]
+def final_kernel(*refs):
+    total = refs[0][...].astype(F32)
     for ref in refs[1:-1]:
         total = total + ref[...].astype(F32)
     refs[-1][...] = total.astype(BF16)
+
+
+def after_kernel(done_ref, *refs):
+    final_kernel(*refs)
 
 
 def route_kernel(per_group, normed_ref, group_ref, expert_ref, ids_ref, at_ref, *refs):
@@ -281,14 +285,13 @@
 
 def dispatch_kernel(chips, cols, capacity, *refs):
     own_refs = refs[:chips]
-    other_ref, gain_ref, pick_ref = refs[chips : chips + 3]
-    normed_ref, out_refs, full_ref = refs[chips + 3], refs[chips + 4 : -1], refs[-1]
+    other_refs, refs = refs[chips : 2 * chips], refs[2 * chips :]
+    gain_ref, pick_ref, normed_ref = refs[:3]
+    out_refs, full_ref = refs[3:-1], refs[-1]
     core = lax.axis_index("tp") % CORES
     for k in range(chips):
         full_ref[:, block_cols(k, core, cols)] = own_refs[k][...].astype(F32)
-        full_ref[:, block_cols(k, 1 - core, cols)] = other_ref[
-            :, k * cols : (k + 1) * cols
-        ].astype(F32)
+        full_ref[:, block_cols(k, 1 - core, cols)] = other_refs[k][...].astype(F32)
     full = full_ref[...]
     factor = lax.rsqrt(jnp.sum(full * full, axis=1, keepdims=True) / full.shape[1] + EPSILON)
     normed = (full * factor * gain_ref[...]).astype(BF16)
@@ -363,43 +366,26 @@
     half = chips * cols
     others = range(1, ep_count)
 
-    normed, own_resid, *blocks = call(
-        functools.partial(norm_kernel, range(ep_count), depth, cols),
-        [((rows, width), BF16), ((rows, cols), F32)] + [((rows, depth), BF16)] * ep_count,
+    blocks = call(
+        functools.partial(split_kernel, depth),
+        [((rows, depth), BF16)] * ep_count,
         resid,
-        norm1_gain[None, :],
-        far=(0, 1),
-        scratch=[
-            pltpu.VMEM((rows, width), BF16),
-            pltpu.VMEM((1, width), F32),
-            pltpu.SemaphoreType.DMA((2,)),
-        ],
+        far=(0,),
+        scratch=[pltpu.SemaphoreType.DMA((ep_count,))],
     )
     arrived = [ep_send(blocks[k], k) for k in others]
     matrix = state_matrix.transpose(1, 2, 3, 0)
     normer = state_norm.transpose(1, 2, 0)
     weights = (w_query, w_key, w_value, w_outgate)
-    all_heads = w_igate.shape[1]
-    *weights, gates, new_max = call(
-        functools.partial(gates_kernel, heads, len(weights)),
-        [(value.shape, value.dtype) for value in weights]
-        + [((2 * heads, rows), F32), ((heads, rows), F32)],
-        normed,
-        w_igate.T,
-        w_fgate.T,
-        forget_bias[None, :],
-        state_max.T,
+    *weights, gain = call(
+        functools.partial(load_kernel, len(weights), depth),
+        [(value.shape, value.dtype) for value in weights] + [((1, depth), F32)],
+        norm1_gain[None, :],
         *weights,
-        far=range(1, 5 + len(weights)),
-        scratch=[
-            pltpu.VMEM((all_heads, width), BF16),
-            pltpu.VMEM((all_heads, width), BF16),
-            pltpu.VMEM((1, all_heads), F32),
-            pltpu.VMEM((heads, rows), F32),
-            pltpu.VMEM((2 * all_heads, rows), F32),
-            pltpu.SemaphoreType.DMA((4 + len(weights),)),
-        ],
-    )
+        far=range(1 + len(weights)),
+        scratch=[pltpu.SemaphoreType.DMA((1 + len(weights),))],
+    )
+    weights = [gain] + weights
     span = 4 * heads * size
     (own,) = call(project_kernel, [((rows, span), F32)], blocks[0], *weights)
     parts, sent = [], []
@@ -408,38 +394,48 @@
         parts.append(part)
         sent.append(ep_send(part, k))
 
-    stage_outs = [(value.shape, value.dtype) for value in (matrix, normer)]
-    stage_outs += [((heads * size, half), BF16)] * 2
-    matrix, normer, w_own, w_sent = call(
-        functools.partial(stage_kernel, len(parts), 2, chips, cols),
-        stage_outs,
+    all_heads = w_igate.shape[1]
+    slots = ep_count * capacity
+    pair = (exp_gate, exp_up, exp_down)
+    expert_outs = [(value.shape[1:], value.dtype) for value in pair]
+    w_sent, w_own, matrix, normer, *staged = call(
+        functools.partial(stage_kernel, len(parts), heads, chips, cols, experts_all),
+        [((heads * size, half), BF16)] * 2
+        + [(matrix.shape, F32), (normer.shape, F32)]
+        + expert_outs * 2
+        + [((2 * heads, rows), F32), ((heads, rows), F32)]
+        + [((rows, 128), F32), ((rows, cols), F32)]
+        + [((slots, rows), BF16), ((topk, rows), jnp.int32)],
         *parts,
+        expert_ids.T,
+        w_igate.T,
+        w_fgate.T,
+        forget_bias[None, :],
+        state_max.T,
+        resid,
+        norm1_gain[None, :],
         w_out,
         matrix,
         normer,
-        far=range(len(parts), len(parts) + 3),
+        *pair,
+        far=range(len(parts) + 1, len(parts) + 13),
         unread=range(len(parts)),
-        scratch=[pltpu.SemaphoreType.DMA((2 + 2 * chips,))],
-        limit=16,
-    )
+        scratch=[
+            pltpu.VMEM((all_heads, width), BF16),
+            pltpu.VMEM((all_heads, width), BF16),
+            pltpu.VMEM((1, all_heads), F32),
+            pltpu.VMEM((heads, rows), F32),
+            pltpu.VMEM((rows, width), BF16),
+            pltpu.VMEM((1, width), F32),
+            pltpu.VMEM((2 * all_heads, rows), F32),
+            pltpu.SemaphoreType.DMA((14 + 2 * chips,)),
+        ],
+        limit=24,
+    )
+    expert_sent, expert_mine = staged[:3], staged[3:6]
+    gates, new_max, factor, own_resid, picks, places = staged[6:]
     w_got = core_send(w_sent)
-
-    pair = (exp_gate, exp_up, exp_down)
-    slots = ep_count * capacity
-    *mine_and_theirs, picks, places = call(
-        functools.partial(swap_kernel, len(pair), experts_all),
-        [(value.shape[1:], value.dtype) for value in pair for _ in range(2)]
-        + [((slots, rows), BF16), ((topk, rows), jnp.int32)],
-        w_sent,
-        expert_ids.T,
-        *pair,
-        far=range(2, 2 + len(pair)),
-        unread=(0,),
-        scratch=[pltpu.SemaphoreType.DMA((2 * len(pair),))],
-        limit=8,
-    )
-    expert_mine = mine_and_theirs[::2]
-    expert_got = [core_send(value) for value in mine_and_theirs[1::2]]
+    expert_got = [core_send(value) for value in expert_sent]
 
     head_out, key_rows, value_rows, new_normer = call(
         functools.partial(cell_kernel, heads, size, ep_count - 1),
@@ -450,9 +446,9 @@
         matrix,
         normer,
         head_gain[None, :],
-        mine_and_theirs[0],
+        factor,
         w_got,
-        unread=(ep_count + 4, ep_count + 5),
+        unread=(ep_count + 5,),
         scratch=[pltpu.VMEM((span, rows), F32)],
         limit=20,
     )
@@ -492,13 +488,13 @@
         limit=4,
     )
     after_parts = [after_cols] + [chip_send(after_cols, k) for k in range(1, chips)]
-    after_other = core_send(jnp.concatenate(after_parts, axis=1))
+    after_others = [core_send(part) for part in after_parts]
 
     normed2, *buffers = call(
         functools.partial(dispatch_kernel, chips, cols, capacity),
         [((rows, width), BF16)] + [((capacity, width), BF16)] * ep_count,
         *after_parts,
-        after_other,
+        *after_others,
         norm2_gain[None, :],
         picks,
         scratch=[pltpu.VMEM((rows, width), F32)],
@@ -538,11 +534,11 @@
     moe = moe_keep + core_send(moe_away).astype(F32)
     moe_parts = [moe[:, k * cols : (k + 1) * cols] for k in range(chips)]
     moe_got = [chip_send(moe_parts[k].astype(BF16), k) for k in range(1, chips)]
-    final = after_cols.astype(F32) + moe_parts[0]
-    for value in moe_got:
-        final = final + value.astype(F32)
+    (mixed,) = call(
+        final_kernel, [((rows, cols), BF16)], after_cols, moe_parts[0], *moe_got, limit=4
+    )
     return (
-        final.astype(BF16),
+        mixed,
         new_matrix.transpose(3, 0, 1, 2),
         new_normer.transpose(2, 0, 1),
         new_max.T,

time: 90.8 us -> 95.9 us (1.056)
  waiting for transfers between devices: 38.6 us -> 43.8 us
    ppermute x12, waiting for transfers between devices: 22.7 us -> 25.9 us  [ep_send(): return lax.ppermute(value, 'ep', [(i, i ^ step) for i in range(count)])]
    ppermute x9, waiting for transfers between devices: 12 us -> 14.2 us  [chip_send(): lax.ppermute(value, 'tp', [(i, i ^ CORES * step) for i in range(count)])]
    ppermute x7 -> x10, waiting for transfers between devices: 3.8 us -> 3.69 us  [core_send(): return lax.ppermute(value, 'tp', [(i, i ^ 1) for i in range(count)])]
  transfers between devices with their start and end apart: 28 -> 31, of which waited for: 17 -> 18; matrix products, arithmetic and copies ran while one was open for 0% -> 0% of each run, Pallas kernels for 14% -> 13%
where the time goes in v1:
time: 95.9 us; the launch traced here: 95.7 us
  waiting for transfers between devices  43.8 us (46%)
  starting transfers between devices  29.9 us (31%)
  Pallas kernels  20.4 us (21%)
    ppermute x12, waiting for transfers between devices, ep_send(): return lax.ppermute(value, 'ep', [(i, i ^ step) for i in range(count)])  25.9 us
    pallas_call x19, Pallas kernels, call(): pl.pallas_call(kernel, out_shape=[jax.ShapeDtypeStruct(shape, dtype) for...  20.4 us
    ppermute x12, starting transfers between devices, ep_send(): return lax.ppermute(value, 'ep', [(i, i ^ step) for i in range(count)])  16.7 us
    ppermute x9, waiting for transfers between devices, chip_send(): lax.ppermute(value, 'tp', [(i, i ^ CORES * step) for i in range(count)])  14.2 us
    ppermute x9, starting transfers between devices, chip_send(): lax.ppermute(value, 'tp', [(i, i ^ CORES * step) for i in range(count)])  12 us
    ppermute x10, waiting for transfers between devices, core_send(): return lax.ppermute(value, 'tp', [(i, i ^ 1) for i in range(count)])  3.69 us
  transfers between devices with their start and end apart: 31, of which 18 were waited for; matrix products, arithmetic and copies ran while one was open for 0% of the time, Pallas kernels for 13%

profile of v1, /device:TPU:0, one launch (start us, length us, event | category | flops | bytes accessed | tf_op | source)
XLA Modules:
  0.0 95.7 jit_solution(2940779237020360654)
XLA Ops:
  0.6 1.1 %shard_map.228 = (bf16[128,512]{1,0:T(8,128)(2,1)S(1)}, bf16[128,512]{1,0:T(8,128)(2,1)S(1)}, bf16[128,512]{1,0:T(8,128)(2,1)S(1)}, bf16[128,512]{1,0:T(8,128)(2,1)S(1)}) custom-call(bf16[128,2048]{1,0:T(8,128)(2,1)} %refs_8_.1), custom_call_target="tpu_custom_call" | custom-call | tf_op jit(solution)/shard_map/pallas_call | solution.py:43
  1.8 4.0 %collective-permute-start.4 = (bf16[128,512]{1,0:T(8,128)(2,1)S(1)}, bf16[128,512]{1,0:T(8,128)(2,1)S(1)}, u32[]{:S(2)}, u32[]{:S(2)}) collective-permute-start(bf16[128,512]{1,0:T(8,128)(2,1)S(1)} %get-tuple-element.56), channel_id=1, source_target_pairs={{0,24},{8,16},{16,8},{24,0},{1,25},{9,17},{17,9},{25,1},{2,26},{10... | collective-permute-start | bytes 393224 | tf_op jit(solution)/shard_map/ppermute | solution.py:19
  5.8 0.5 collective-permute-start.2
  6.4 1.2 %shard_map.229 = (bf16[512,256]{1,0:T(8,128)(2,1)S(1)}, bf16[512,256]{1,0:T(8,128)(2,1)S(1)}, bf16[512,256]{1,0:T(8,128)(2,1)S(1)}, bf16[512,256]{1,0:T(8,128)(2,1)S(1)}, f32[1,512]{1,0:T(1,128)S(1)}) custom-call(f32[1,2048]{1,0:T(1,128)} %bitcast.25, bf16[512,256]{1,0:T(8,128)(2,1)} %refs_0_.1, bf16[512,256]{1,0:T(8,128)(2,1)} %refs_1_.1, ...), custom_call_target="tpu_custom_call" | custom-call | tf_op jit(solution)/shard_map/pallas_call | solution.py:43
  7.7 2.0 %collective-permute-done.4.x_ref = bf16[128,512]{1,0:T(8,128)(2,1)S(1)} collective-permute-done((bf16[128,512]{1,0:T(8,128)(2,1)S(1)}, bf16[128,512]{1,0:T(8,128)(2,1)S(1)}, u32[]{:S(2)}, u32[]{:S(2)}) %collective-permute-start.4) | collective-permute-done | bytes 131104 | tf_op jit(solution)/shard_map/ppermute | solution.py:19
  10.0 2.1 %collective-permute-done.2.x_ref = bf16[128,512]{1,0:T(8,128)(2,1)S(1)} collective-permute-done((bf16[128,512]{1,0:T(8,128)(2,1)S(1)}, bf16[128,512]{1,0:T(8,128)(2,1)S(1)}, u32[]{:S(2)}, u32[]{:S(2)}) %collective-permute-start.2) | collective-permute-done | bytes 131104 | tf_op jit(solution)/shard_map/ppermute | solution.py:19
  12.8 0.7 copy-done.3
  13.4 5.8 %shard_map.234 = (bf16[256,1024]{1,0:T(8,128)(2,1)S(1)}, bf16[256,1024]{1,0:T(8,128)(2,1)S(1)}, f32[4,64,64,128]{3,2,1,0:T(8,128)S(1)}, f32[4,64,128]{2,1,0:T(8,...) custom-call(bf16[128,1024]{1,0:T(8,128)(2,1)S(1)} %shard_map.231.ref, ...), custom_call_target="tpu_custom_call" | custom-call | tf_op jit(solution)/shard_map/pallas_call | solution.py:43
  19.4 1.7 %collective-permute-start.1 = (bf16[128,1024]{1,0:T(8,128)(2,1)S(1)}, bf16[128,1024]{1,0:T(8,128)(2,1)S(1)}, u32[]{:S(2)}, u32[]{:S(2)}) collective-permute-start(bf16[128,1024]{1,0:T(8,128)(2,1)S(1)} %shard_map.231.refs_0_), channel_id=1, source_target_pairs={{0,8},{8,0},{16,24},{24,16},{1,9},{9,1},{17,25},{25,17},{2,10},{10... | collective-permute-start | bytes 786440 | tf_op jit(solution)/shard_map/ppermute | solution.py:19
  21.1 0.7 collective-permute-start.3
  21.8 1.1 %collective-permute-start.5 = (bf16[128,1024]{1,0:T(8,128)(2,1)S(1)}, bf16[128,1024]{1,0:T(8,128)(2,1)S(1)}, u32[]{:S(2)}, u32[]{:S(2)}) collective-permute-start(bf16[128,1024]{1,0:T(8,128)(2,1)S(1)} %shard_map.233.refs_2_), channel_id=1, source_target_pairs={{0,24},{8,16},{16,8},{24,0},{1,25},{9,17},{17,9},{25,1},{2,26},{10... | collective-permute-start | bytes 786440 | tf_op jit(solution)/shard_map/ppermute | solution.py:19
  23.2 5.4 %collective-permute-done.1.refs_1_ = bf16[128,1024]{1,0:T(8,128)(2,1)S(1)} collective-permute-done((bf16[128,1024]{1,0:T(8,128)(2,1)S(1)}, bf16[128,1024]{1,0:T(8,128)(2,1)S(1)}, u32[]{:S(2)}, u32[]{:S(2)}) %collective-permute-start.1) | collective-permute-done | bytes 262176 | tf_op jit(solution)/shard_map/ppermute | solution.py:19
  28.6 6.5 %collective-permute-done.3.refs_2_ = bf16[128,1024]{1,0:T(8,128)(2,1)S(1)} collective-permute-done((bf16[128,1024]{1,0:T(8,128)(2,1)S(1)}, bf16[128,1024]{1,0:T(8,128)(2,1)S(1)}, u32[]{:S(2)}, u32[]{:S(2)}) %collective-permute-start.3) | collective-permute-done | bytes 262176 | tf_op jit(solution)/shard_map/ppermute | solution.py:19
  35.1 1.8 %shard_map.235 = (bf16[128,256]{1,0:T(8,128)(2,1)S(1)}, f32[4,64,128]{2,1,0:T(8,128)S(1)}, f32[4,64,128]{2,1,0:T(8,128)S(1)}, f32[4,64,128]{2,1,0:T(8,128)}) custom-call(f32[128,1024]{1,0:T(8,128)S(1)} %shard_map.230.refs_0_, bf16[128,1024]{1,0:T(8,128)(2,1)S(1)} %collective-permute-done.1.refs_1_, bf16[128,1024]{1,0:T(8,128)(2,1)S(1)} %collective-permute-done.3.refs_2_, ...), custom_call_target="tpu_custom_call" | custom-call | tf_op jit(solution)/shard_map/pallas_call | solution.py:43
  36.9 1.3 %collective-permute-done.7.got_ref = bf16[128,256]{1,0:T(8,128)(2,1)S(1)} collective-permute-done((bf16[128,256]{1,0:T(8,128)(2,1)S(1)}, bf16[128,256]{1,0:T(8,128)(2,1)S(1)}, u32[]{:S(2)}, u32[]{:S(2)}) %collective-permute-start.7) | collective-permute-done | bytes 65568 | tf_op jit(solution)/shard_map/ppermute | solution.py:29
  38.5 1.6 %collective-permute-start.8 = (bf16[128,256]{1,0:T(8,128)(2,1)S(1)}, bf16[128,256]{1,0:T(8,128)(2,1)S(1)}, u32[]{:S(2)}, u32[]{:S(2)}) collective-permute-start(bf16[128,256]{1,0:T(8,128)(2,1)S(1)} %get-tuple-element.70), channel_id=1, source_target_pairs={{0,2},{1,3},{2,0},{3,1},{4,6},{5,7},{6,4},{7,5},{8,10},{9,11},{10,... | collective-permute-start | bytes 196616 | tf_op jit(solution)/shard_map/ppermute | solution.py:24
  40.1 2.6 %collective-permute-start.9 = (bf16[128,256]{1,0:T(8,128)(2,1)S(1)}, bf16[128,256]{1,0:T(8,128)(2,1)S(1)}, u32[]{:S(2)}, u32[]{:S(2)}) collective-permute-start(bf16[128,256]{1,0:T(8,128)(2,1)S(1)} %get-tuple-element.71), channel_id=1, source_target_pairs={{0,4},{1,5},{2,6},{3,7},{4,0},{5,1},{6,2},{7,3},{8,12},{9,13},{10,... | collective-permute-start | bytes 196616 | tf_op jit(solution)/shard_map/ppermute | solution.py:24
  43.0 0.5 collective-permute-start.20
  43.5 3.8 %shard_map.237 = (f32[4,64,64,128]{3,2,1,0:T(8,128)}, f32[8,128]{1,0:T(8,128)S(1)}) custom-call(bf16[128,256]{1,0:T(8,128)(2,1)S(1)} %get-tuple-element.64.after_ref, f32[4,64,64,128]{3,2,1,0:T(8,128)S(1)} %get-tuple-element.58.refs_5_.matrix_ref, f32[4,64,128]{2,1,0:T(8,128)S(1)} %get-tuple-element.65.key_ref, ...), custom_call_target="tpu_custom_call" | custom-call | tf_op jit(solution)/shard_map/pallas_call | solution.py:43
  47.7 1.2 %collective-permute-done.10.refs_4_ = bf16[128,256]{1,0:T(8,128)(2,1)S(1)} collective-permute-done((bf16[128,256]{1,0:T(8,128)(2,1)S(1)}, bf16[128,256]{1,0:T(8,128)(2,1)S(1)}, u32[]{:S(2)}, u32[]{:S(2)}) %collective-permute-start.10) | collective-permute-done | bytes 65568 | tf_op jit(solution)/shard_map/ppermute | solution.py:24
  49.0 2.6 %collective-permute-start.13 = (bf16[128,256]{1,0:T(8,128)(2,1)S(1)}, bf16[128,256]{1,0:T(8,128)(2,1)S(1)}, u32[]{:S(2)}, u32[]{:S(2)}) collective-permute-start(bf16[128,256]{1,0:T(8,128)(2,1)S(1)} %shard_map.238.refs_0_), channel_id=1, source_target_pairs={{0,6},{1,7},{2,4},{3,5},{4,2},{5,3},{6,0},{7,1},{8,14},{9,15},{10,... | collective-permute-start | bytes 196616 | tf_op jit(solution)/shard_map/ppermute | solution.py:24
  51.6 0.4 collective-permute-start.12
  52.1 3.9 %collective-permute-done.13.refs_3_ = bf16[128,256]{1,0:T(8,128)(2,1)S(1)} collective-permute-done((bf16[128,256]{1,0:T(8,128)(2,1)S(1)}, bf16[128,256]{1,0:T(8,128)(2,1)S(1)}, u32[]{:S(2)}, u32[]{:S(2)}) %collective-permute-start.13) | collective-permute-done | bytes 65568 | tf_op jit(solution)/shard_map/ppermute | solution.py:24
  56.0 2.2 %collective-permute-done.12.refs_2_ = bf16[128,256]{1,0:T(8,128)(2,1)S(1)} collective-permute-done((bf16[128,256]{1,0:T(8,128)(2,1)S(1)}, bf16[128,256]{1,0:T(8,128)(2,1)S(1)}, u32[]{:S(2)}, u32[]{:S(2)}) %collective-permute-start.12) | collective-permute-done | bytes 65568 | tf_op jit(solution)/shard_map/ppermute | solution.py:24
  58.2 2.0 %collective-permute-done.11.refs_1_ = bf16[128,256]{1,0:T(8,128)(2,1)S(1)} collective-permute-done((bf16[128,256]{1,0:T(8,128)(2,1)S(1)}, bf16[128,256]{1,0:T(8,128)(2,1)S(1)}, u32[]{:S(2)}, u32[]{:S(2)}) %collective-permute-start.11) | collective-permute-done | bytes 65568 | tf_op jit(solution)/shard_map/ppermute | solution.py:24
  60.2 0.5 collective-permute-start.15
  60.7 0.7 collective-permute-done.16.refs_6_
  61.6 0.6 shard_map.239
  62.2 0.6 collective-permute-start.21
  62.8 1.5 %collective-permute-start.23 = (bf16[48,2048]{1,0:T(8,128)(2,1)S(1)}, bf16[48,2048]{1,0:T(8,128)(2,1)S(1)}, u32[]{:S(2)}, u32[]{:S(2)}) collective-permute-start(bf16[48,2048]{1,0:T(8,128)(2,1)S(1)} %get-tuple-element.81), channel_id=1, source_target_pairs={{0,16},{8,24},{16,0},{24,8},{1,17},{9,25},{17,1},{25,9},{2,18},{10... | collective-permute-start | bytes 589832 | tf_op jit(solution)/shard_map/ppermute | solution.py:19
  64.4 1.4 %collective-permute-start.25 = (bf16[48,2048]{1,0:T(8,128)(2,1)S(1)}, bf16[48,2048]{1,0:T(8,128)(2,1)S(1)}, u32[]{:S(2)}, u32[]{:S(2)}) collective-permute-start(bf16[48,2048]{1,0:T(8,128)(2,1)S(1)} %get-tuple-element.82), channel_id=1, source_target_pairs={{0,24},{8,16},{16,8},{24,0},{1,25},{9,17},{17,9},{25,1},{2,26},{10... | collective-permute-start | bytes 589832 | tf_op jit(solution)/shard_map/ppermute | solution.py:19
  65.8 4.3 %collective-permute-done.21.x_ref = bf16[48,2048]{1,0:T(8,128)(2,1)S(1)} collective-permute-done((bf16[48,2048]{1,0:T(8,128)(2,1)S(1)}, bf16[48,2048]{1,0:T(8,128)(2,1)S(1)}, u32[]{:S(2)}, u32[]{:S(2)}) %collective-permute-start.21) | collective-permute-done | bytes 196640 | tf_op jit(solution)/shard_map/ppermute | solution.py:19
  70.1 0.7 shard_map.241
  70.8 0.6 collective-permute-start.22
  71.3 1.1 %collective-permute-done.23.x_ref = bf16[48,2048]{1,0:T(8,128)(2,1)S(1)} collective-permute-done((bf16[48,2048]{1,0:T(8,128)(2,1)S(1)}, bf16[48,2048]{1,0:T(8,128)(2,1)S(1)}, u32[]{:S(2)}, u32[]{:S(2)}) %collective-permute-start.23) | collective-permute-done | bytes 196640 | tf_op jit(solution)/shard_map/ppermute | solution.py:19
  72.5 0.7 shard_map.242
  73.1 3.0 %collective-permute-start.24 = (bf16[48,2048]{1,0:T(8,128)(2,1)S(1)}, bf16[48,2048]{1,0:T(8,128)(2,1)S(1)}, u32[]{:S(2)}, u32[]{:S(2)}) collective-permute-start(bf16[48,2048]{1,0:T(8,128)(2,1)S(1)} %shard_map.242), channel_id=1, source_target_pairs={{0,16},{8,24},{16,0},{24,8},{1,17},{9,25},{17,1},{25,9},{2,18},{10... | collective-permute-start | bytes 589832 | tf_op jit(solution)/shard_map/ppermute | solution.py:19
  76.1 0.7 shard_map.243
  76.8 1.4 %collective-permute-start.26 = (bf16[48,2048]{1,0:T(8,128)(2,1)S(1)}, bf16[48,2048]{1,0:T(8,128)(2,1)S(1)}, u32[]{:S(2)}, u32[]{:S(2)}) collective-permute-start(bf16[48,2048]{1,0:T(8,128)(2,1)S(1)} %shard_map.243), channel_id=1, source_target_pairs={{0,24},{8,16},{16,8},{24,0},{1,25},{9,17},{17,9},{25,1},{2,26},{10... | collective-permute-start | bytes 589832 | tf_op jit(solution)/shard_map/ppermute | solution.py:19
  78.2 0.5 shard_map.244
  78.7 0.7 shard_map.240.refs_0_
  79.4 4.5 %collective-permute-done.24.refs_2_ = bf16[48,2048]{1,0:T(8,128)(2,1)S(1)} collective-permute-done((bf16[48,2048]{1,0:T(8,128)(2,1)S(1)}, bf16[48,2048]{1,0:T(8,128)(2,1)S(1)}, u32[]{:S(2)}, u32[]{:S(2)}) %collective-permute-start.24) | collective-permute-done | bytes 196640 | tf_op jit(solution)/shard_map/ppermute | solution.py:19
  84.5 1.5 %collective-permute-done.27 = bf16[128,1024]{1,0:T(8,128)(2,1)S(1)} collective-permute-done((bf16[128,1024]{1,0:T(8,128)(2,1)S(1)}, bf16[128,1024]{1,0:T(8,128)(2,1)S(1)}, u32[]{:S(2)}, u32[]{:S(2)}) %collective-permute-start.27) | collective-permute-done | bytes 262176 | tf_op jit(solution)/shard_map/ppermute | solution.py:29
  86.1 2.4 %collective-permute-start.30 = (bf16[128,256]{1,0:T(8,128)(2,1)S(1)}, bf16[128,256]{1,0:T(8,128)(2,1)S(1)}, u32[]{:S(2)}, u32[]{:S(2)}) collective-permute-start(bf16[128,256]{1,0:T(8,128)(2,1)S(1)} %get-tuple-element.94), channel_id=1, source_target_pairs={{0,6},{1,7},{2,4},{3,5},{4,2},{5,3},{6,0},{7,1},{8,14},{9,15},{10,... | collective-permute-start | bytes 196616 | tf_op jit(solution)/shard_map/ppermute | solution.py:24
  88.5 2.0 %collective-permute-start.28 = (bf16[128,256]{1,0:T(8,128)(2,1)S(1)}, bf16[128,256]{1,0:T(8,128)(2,1)S(1)}, u32[]{:S(2)}, u32[]{:S(2)}) collective-permute-start(bf16[128,256]{1,0:T(8,128)(2,1)S(1)} %get-tuple-element.96), channel_id=1, source_target_pairs={{0,2},{1,3},{2,0},{3,1},{4,6},{5,7},{6,4},{7,5},{8,10},{9,11},{10,... | collective-permute-start | bytes 196616 | tf_op jit(solution)/shard_map/ppermute | solution.py:24
  90.6 2.2 %collective-permute-done.30.refs_4_ = bf16[128,256]{1,0:T(8,128)(2,1)S(1)} collective-permute-done((bf16[128,256]{1,0:T(8,128)(2,1)S(1)}, bf16[128,256]{1,0:T(8,128)(2,1)S(1)}, u32[]{:S(2)}, u32[]{:S(2)}) %collective-permute-start.30) | collective-permute-done | bytes 65568 | tf_op jit(solution)/shard_map/ppermute | solution.py:24
  92.8 2.3 %collective-permute-done.29.refs_3_ = bf16[128,256]{1,0:T(8,128)(2,1)S(1)} collective-permute-done((bf16[128,256]{1,0:T(8,128)(2,1)S(1)}, bf16[128,256]{1,0:T(8,128)(2,1)S(1)}, u32[]{:S(2)}, u32[]{:S(2)}) %collective-permute-start.29) | collective-permute-done | bytes 65568 | tf_op jit(solution)/shard_map/ppermute | solution.py:24
  95.1 0.7 shard_map.246
  (46 shorter events, 3.3 us)
Async XLA Ops:
  1.8 7.9 %collective-permute-start.4 = (bf16[128,512]{1,0:T(8,128)(2,1)S(1)}, bf16[128,512]{1,0:T(8,128)(2,1)S(1)}, u32[]{:S(2)}, u32[]{:S(2)}) collective-permute-start(bf16[128,512]{1,0:T(8,128)(2,1)S(1)} %get-tuple-element.56), channel_id=1, source_target_pairs={{0,24},{8,16},{16,8},{24,0},{1,25},{9,17},{17,9},{25,1},{2,26},{10... | collective-permute-start | bytes 393224 | tf_op jit(solution)/shard_map/ppermute | solution.py:19
  5.8 6.3 %collective-permute-start.2 = (bf16[128,512]{1,0:T(8,128)(2,1)S(1)}, bf16[128,512]{1,0:T(8,128)(2,1)S(1)}, u32[]{:S(2)}, u32[]{:S(2)}) collective-permute-start(bf16[128,512]{1,0:T(8,128)(2,1)S(1)} %get-tuple-element.55), channel_id=1, source_target_pairs={{0,16},{8,24},{16,0},{24,8},{1,17},{9,25},{17,1},{25,9},{2,18},{10... | collective-permute-start | bytes 393224 | tf_op jit(solution)/shard_map/ppermute | solution.py:19
  6.3 6.1 %collective-permute-start = (bf16[128,512]{1,0:T(8,128)(2,1)S(1)}, bf16[128,512]{1,0:T(8,128)(2,1)S(1)}, u32[]{:S(2)}, u32[]{:S(2)}) collective-permute-start(bf16[128,512]{1,0:T(8,128)(2,1)S(1)} %get-tuple-element.54), channel_id=1, source_target_pairs={{0,8},{8,0},{16,24},{24,16},{1,9},{9,1},{17,25},{25,17},{2,10},{10... | collective-permute-start | bytes 393224 | tf_op jit(solution)/shard_map/ppermute | solution.py:19
  12.4 22.7 %copy-start.4 = (f32[256]{0:T(256)S(1)}, f32[256]{0:T(256)}, u32[]{:S(2)}) copy-start(f32[256]{0:T(256)} %param.30) | copy-start | bytes 3076
  12.7 0.7 copy-start.3
  19.3 15.8 %collective-permute-start.6 = (bf16[256,1024]{1,0:T(8,128)(2,1)S(1)}, bf16[256,1024]{1,0:T(8,128)(2,1)S(1)}, u32[]{:S(2)}, u32[]{:S(2)}) collective-permute-start(bf16[256,1024]{1,0:T(8,128)(2,1)S(1)} %get-tuple-element.61), channel_id=1, source_target_pairs={{0,1},{1,0},{2,3},{3,2},{4,5},{5,4},{6,7},{7,6},{8,9},{9,8},{10,11... | collective-permute-start | bytes 1572872 | tf_op jit(solution)/shard_map/ppermute | solution.py:29
  19.4 9.2 %collective-permute-start.1 = (bf16[128,1024]{1,0:T(8,128)(2,1)S(1)}, bf16[128,1024]{1,0:T(8,128)(2,1)S(1)}, u32[]{:S(2)}, u32[]{:S(2)}) collective-permute-start(bf16[128,1024]{1,0:T(8,128)(2,1)S(1)} %shard_map.231.refs_0_), channel_id=1, source_target_pairs={{0,8},{8,0},{16,24},{24,16},{1,9},{9,1},{17,25},{25,17},{2,10},{10... | collective-permute-start | bytes 786440 | tf_op jit(solution)/shard_map/ppermute | solution.py:19
  21.1 14.0 %collective-permute-start.3 = (bf16[128,1024]{1,0:T(8,128)(2,1)S(1)}, bf16[128,1024]{1,0:T(8,128)(2,1)S(1)}, u32[]{:S(2)}, u32[]{:S(2)}) collective-permute-start(bf16[128,1024]{1,0:T(8,128)(2,1)S(1)} %shard_map.232.refs_1_), channel_id=1, source_target_pairs={{0,16},{8,24},{16,0},{24,8},{1,17},{9,25},{17,1},{25,9},{2,18},{10... | collective-permute-start | bytes 786440 | tf_op jit(solution)/shard_map/ppermute | solution.py:19
  21.8 13.3 %collective-permute-start.5 = (bf16[128,1024]{1,0:T(8,128)(2,1)S(1)}, bf16[128,1024]{1,0:T(8,128)(2,1)S(1)}, u32[]{:S(2)}, u32[]{:S(2)}) collective-permute-start(bf16[128,1024]{1,0:T(8,128)(2,1)S(1)} %shard_map.233.refs_2_), channel_id=1, source_target_pairs={{0,24},{8,16},{16,8},{24,0},{1,25},{9,17},{17,9},{25,1},{2,26},{10... | collective-permute-start | bytes 786440 | tf_op jit(solution)/shard_map/ppermute | solution.py:19
  22.9 41.4 %collective-permute-start.18 = (bf16[2048,128]{1,0:T(8,128)(2,1)S(1)}, bf16[2048,128]{1,0:T(8,128)(2,1)S(1)}, u32[]{:S(2)}, u32[]{:S(2)}) collective-permute-start(bf16[2048,128]{1,0:T(8,128)(2,1)S(1)} %get-tuple-element.77), channel_id=1, source_target_pairs={{0,1},{1,0},{2,3},{3,2},{4,5},{5,4},{6,7},{7,6},{8,9},{9,8},{10,11... | collective-permute-start | bytes 1572872 | tf_op jit(solution)/shard_map/ppermute | solution.py:29
  35.1 26.5 %copy-start.2 = (f32[2048]{0:T(1024)S(1)}, f32[2048]{0:T(1024)}, u32[]{:S(2)}) copy-start(f32[2048]{0:T(1024)} %param.35) | copy-start | bytes 24580
  36.9 1.3 %collective-permute-start.7 = (bf16[128,256]{1,0:T(8,128)(2,1)S(1)}, bf16[128,256]{1,0:T(8,128)(2,1)S(1)}, u32[]{:S(2)}, u32[]{:S(2)}) collective-permute-start(bf16[128,256]{1,0:T(8,128)(2,1)S(1)} %get-tuple-element.62.own_ref), channel_id=1, source_target_pairs={{0,1},{1,0},{2,3},{3,2},{4,5},{5,4},{6,7},{7,6},{8,9},{9,8},{10,11... | collective-permute-start | bytes 196616 | tf_op jit(solution)/shard_map/ppermute | solution.py:29
  38.5 4.5 %collective-permute-start.8 = (bf16[128,256]{1,0:T(8,128)(2,1)S(1)}, bf16[128,256]{1,0:T(8,128)(2,1)S(1)}, u32[]{:S(2)}, u32[]{:S(2)}) collective-permute-start(bf16[128,256]{1,0:T(8,128)(2,1)S(1)} %get-tuple-element.70), channel_id=1, source_target_pairs={{0,2},{1,3},{2,0},{3,1},{4,6},{5,7},{6,4},{7,5},{8,10},{9,11},{10,... | collective-permute-start | bytes 196616 | tf_op jit(solution)/shard_map/ppermute | solution.py:24
  40.1 7.5 %collective-permute-start.9 = (bf16[128,256]{1,0:T(8,128)(2,1)S(1)}, bf16[128,256]{1,0:T(8,128)(2,1)S(1)}, u32[]{:S(2)}, u32[]{:S(2)}) collective-permute-start(bf16[128,256]{1,0:T(8,128)(2,1)S(1)} %get-tuple-element.71), channel_id=1, source_target_pairs={{0,4},{1,5},{2,6},{3,7},{4,0},{5,1},{6,2},{7,3},{8,12},{9,13},{10,... | collective-permute-start | bytes 196616 | tf_op jit(solution)/shard_map/ppermute | solution.py:24
  42.7 6.2 %collective-permute-start.10 = (bf16[128,256]{1,0:T(8,128)(2,1)S(1)}, bf16[128,256]{1,0:T(8,128)(2,1)S(1)}, u32[]{:S(2)}, u32[]{:S(2)}) collective-permute-start(bf16[128,256]{1,0:T(8,128)(2,1)S(1)} %get-tuple-element.64.after_ref), channel_id=1, source_target_pairs={{0,6},{1,7},{2,4},{3,5},{4,2},{5,3},{6,0},{7,1},{8,14},{9,15},{10,... | collective-permute-start | bytes 196616 | tf_op jit(solution)/shard_map/ppermute | solution.py:24
  42.9 22.8 %collective-permute-start.19 = (bf16[2048,128]{1,0:T(8,128)(2,1)S(1)}, bf16[2048,128]{1,0:T(8,128)(2,1)S(1)}, u32[]{:S(2)}, u32[]{:S(2)}) collective-permute-start(bf16[2048,128]{1,0:T(8,128)(2,1)S(1)} %get-tuple-element.78), channel_id=1, source_target_pairs={{0,1},{1,0},{2,3},{3,2},{4,5},{5,4},{6,7},{7,6},{8,9},{9,8},{10,11... | collective-permute-start | bytes 1572872 | tf_op jit(solution)/shard_map/ppermute | solution.py:29
  43.0 22.8 %collective-permute-start.20 = (bf16[128,2048]{1,0:T(8,128)(2,1)S(1)}, bf16[128,2048]{1,0:T(8,128)(2,1)S(1)}, u32[]{:S(2)}, u32[]{:S(2)}) collective-permute-start(bf16[128,2048]{1,0:T(8,128)(2,1)S(1)} %get-tuple-element.79), channel_id=1, source_target_pairs={{0,1},{1,0},{2,3},{3,2},{4,5},{5,4},{6,7},{7,6},{8,9},{9,8},{10,11... | collective-permute-start | bytes 1572872 | tf_op jit(solution)/shard_map/ppermute | solution.py:29
  43.5 34.7 %copy-start = (bf16[2048,8]{0,1:T(8,128)(2,1)S(1)}, bf16[2048,8]{0,1:T(8,128)(2,1)}, u32[]{:S(2)}) copy-start(bf16[2048,8]{0,1:T(8,128)(2,1)} %param.37) | copy-start | bytes 98308
  43.5 34.7 %copy-start.1 = (bf16[2048,4]{0,1:T(4,128)(2,1)S(1)}, bf16[2048,4]{0,1:T(4,128)(2,1)}, u32[]{:S(2)}) copy-start(bf16[2048,4]{0,1:T(4,128)(2,1)} %param.36) | copy-start | bytes 49156
  48.9 2.7 %collective-permute-start.14 = (bf16[128,256]{1,0:T(8,128)(2,1)S(1)}, bf16[128,256]{1,0:T(8,128)(2,1)S(1)}, u32[]{:S(2)}, u32[]{:S(2)}) collective-permute-start(bf16[128,256]{1,0:T(8,128)(2,1)S(1)} %shard_map.238.refs_0_), channel_id=1, source_target_pairs={{0,1},{1,0},{2,3},{3,2},{4,5},{5,4},{6,7},{7,6},{8,9},{9,8},{10,11... | collective-permute-start | bytes 196616 | tf_op jit(solution)/shard_map/ppermute | solution.py:29
  49.0 6.9 %collective-permute-start.13 = (bf16[128,256]{1,0:T(8,128)(2,1)S(1)}, bf16[128,256]{1,0:T(8,128)(2,1)S(1)}, u32[]{:S(2)}, u32[]{:S(2)}) collective-permute-start(bf16[128,256]{1,0:T(8,128)(2,1)S(1)} %shard_map.238.refs_0_), channel_id=1, source_target_pairs={{0,6},{1,7},{2,4},{3,5},{4,2},{5,3},{6,0},{7,1},{8,14},{9,15},{10,... | collective-permute-start | bytes 196616 | tf_op jit(solution)/shard_map/ppermute | solution.py:24
  51.6 6.6 %collective-permute-start.12 = (bf16[128,256]{1,0:T(8,128)(2,1)S(1)}, bf16[128,256]{1,0:T(8,128)(2,1)S(1)}, u32[]{:S(2)}, u32[]{:S(2)}) collective-permute-start(bf16[128,256]{1,0:T(8,128)(2,1)S(1)} %shard_map.238.refs_0_), channel_id=1, source_target_pairs={{0,4},{1,5},{2,6},{3,7},{4,0},{5,1},{6,2},{7,3},{8,12},{9,13},{10,... | collective-permute-start | bytes 196616 | tf_op jit(solution)/shard_map/ppermute | solution.py:24
  55.9 4.3 %collective-permute-start.11 = (bf16[128,256]{1,0:T(8,128)(2,1)S(1)}, bf16[128,256]{1,0:T(8,128)(2,1)S(1)}, u32[]{:S(2)}, u32[]{:S(2)}) collective-permute-start(bf16[128,256]{1,0:T(8,128)(2,1)S(1)} %shard_map.238.refs_0_), channel_id=1, source_target_pairs={{0,2},{1,3},{2,0},{3,1},{4,6},{5,7},{6,4},{7,5},{8,10},{9,11},{10,... | collective-permute-start | bytes 196616 | tf_op jit(solution)/shard_map/ppermute | solution.py:24
  58.2 2.0 %collective-permute-start.17 = (bf16[128,256]{1,0:T(8,128)(2,1)S(1)}, bf16[128,256]{1,0:T(8,128)(2,1)S(1)}, u32[]{:S(2)}, u32[]{:S(2)}) collective-permute-start(bf16[128,256]{1,0:T(8,128)(2,1)S(1)} %collective-permute-done.13.refs_3_), channel_id=1, source_target_pairs={{0,1},{1,0},{2,3},{3,2},{4,5},{5,4},{6,7},{7,6},{8,9},{9,8},{10,11... | collective-permute-start | bytes 196616 | tf_op jit(solution)/shard_map/ppermute | solution.py:29
  60.2 1.3 %collective-permute-start.16 = (bf16[128,256]{1,0:T(8,128)(2,1)S(1)}, bf16[128,256]{1,0:T(8,128)(2,1)S(1)}, u32[]{:S(2)}, u32[]{:S(2)}) collective-permute-start(bf16[128,256]{1,0:T(8,128)(2,1)S(1)} %collective-permute-done.12.refs_2_), channel_id=1, source_target_pairs={{0,1},{1,0},{2,3},{3,2},{4,5},{5,4},{6,7},{7,6},{8,9},{9,8},{10,11... | collective-permute-start | bytes 196616 | tf_op jit(solution)/shard_map/ppermute | solution.py:29
  60.2 1.4 %collective-permute-start.15 = (bf16[128,256]{1,0:T(8,128)(2,1)S(1)}, bf16[128,256]{1,0:T(8,128)(2,1)S(1)}, u32[]{:S(2)}, u32[]{:S(2)}) collective-permute-start(bf16[128,256]{1,0:T(8,128)(2,1)S(1)} %collective-permute-done.11.refs_1_), channel_id=1, source_target_pairs={{0,1},{1,0},{2,3},{3,2},{4,5},{5,4},{6,7},{7,6},{8,9},{9,8},{10,11... | collective-permute-start | bytes 196616 | tf_op jit(solution)/shard_map/ppermute | solution.py:29
  62.2 7.8 %collective-permute-start.21 = (bf16[48,2048]{1,0:T(8,128)(2,1)S(1)}, bf16[48,2048]{1,0:T(8,128)(2,1)S(1)}, u32[]{:S(2)}, u32[]{:S(2)}) collective-permute-start(bf16[48,2048]{1,0:T(8,128)(2,1)S(1)} %get-tuple-element.80), channel_id=1, source_target_pairs={{0,8},{8,0},{16,24},{24,16},{1,9},{9,1},{17,25},{25,17},{2,10},{10... | collective-permute-start | bytes 589832 | tf_op jit(solution)/shard_map/ppermute | solution.py:19
  62.8 9.6 %collective-permute-start.23 = (bf16[48,2048]{1,0:T(8,128)(2,1)S(1)}, bf16[48,2048]{1,0:T(8,128)(2,1)S(1)}, u32[]{:S(2)}, u32[]{:S(2)}) collective-permute-start(bf16[48,2048]{1,0:T(8,128)(2,1)S(1)} %get-tuple-element.81), channel_id=1, source_target_pairs={{0,16},{8,24},{16,0},{24,8},{1,17},{9,25},{17,1},{25,9},{2,18},{10... | collective-permute-start | bytes 589832 | tf_op jit(solution)/shard_map/ppermute | solution.py:19
  64.4 11.8 %collective-permute-start.25 = (bf16[48,2048]{1,0:T(8,128)(2,1)S(1)}, bf16[48,2048]{1,0:T(8,128)(2,1)S(1)}, u32[]{:S(2)}, u32[]{:S(2)}) collective-permute-start(bf16[48,2048]{1,0:T(8,128)(2,1)S(1)} %get-tuple-element.82), channel_id=1, source_target_pairs={{0,24},{8,16},{16,8},{24,0},{1,25},{9,17},{17,9},{25,1},{2,26},{10... | collective-permute-start | bytes 589832 | tf_op jit(solution)/shard_map/ppermute | solution.py:19
  70.8 8.7 %collective-permute-start.22 = (bf16[48,2048]{1,0:T(8,128)(2,1)S(1)}, bf16[48,2048]{1,0:T(8,128)(2,1)S(1)}, u32[]{:S(2)}, u32[]{:S(2)}) collective-permute-start(bf16[48,2048]{1,0:T(8,128)(2,1)S(1)} %shard_map.241), channel_id=1, source_target_pairs={{0,8},{8,0},{16,24},{24,16},{1,9},{9,1},{17,25},{25,17},{2,10},{10... | collective-permute-start | bytes 589832 | tf_op jit(solution)/shard_map/ppermute | solution.py:19
  73.1 10.8 %collective-permute-start.24 = (bf16[48,2048]{1,0:T(8,128)(2,1)S(1)}, bf16[48,2048]{1,0:T(8,128)(2,1)S(1)}, u32[]{:S(2)}, u32[]{:S(2)}) collective-permute-start(bf16[48,2048]{1,0:T(8,128)(2,1)S(1)} %shard_map.242), channel_id=1, source_target_pairs={{0,16},{8,24},{16,0},{24,8},{1,17},{9,25},{17,1},{25,9},{2,18},{10... | collective-permute-start | bytes 589832 | tf_op jit(solution)/shard_map/ppermute | solution.py:19
  76.8 7.2 %collective-permute-start.26 = (bf16[48,2048]{1,0:T(8,128)(2,1)S(1)}, bf16[48,2048]{1,0:T(8,128)(2,1)S(1)}, u32[]{:S(2)}, u32[]{:S(2)}) collective-permute-start(bf16[48,2048]{1,0:T(8,128)(2,1)S(1)} %shard_map.243), channel_id=1, source_target_pairs={{0,24},{8,16},{16,8},{24,0},{1,25},{9,17},{17,9},{25,1},{2,26},{10... | collective-permute-start | bytes 589832 | tf_op jit(solution)/shard_map/ppermute | solution.py:19
  84.4 1.6 %collective-permute-start.27 = (bf16[128,1024]{1,0:T(8,128)(2,1)S(1)}, bf16[128,1024]{1,0:T(8,128)(2,1)S(1)}, u32[]{:S(2)}, u32[]{:S(2)}) collective-permute-start(bf16[128,1024]{1,0:T(8,128)(2,1)S(1)} %get-tuple-element.88), channel_id=1, source_target_pairs={{0,1},{1,0},{2,3},{3,2},{4,5},{5,4},{6,7},{7,6},{8,9},{9,8},{10,11... | collective-permute-start | bytes 786440 | tf_op jit(solution)/shard_map/ppermute | solution.py:29
  86.1 6.7 %collective-permute-start.30 = (bf16[128,256]{1,0:T(8,128)(2,1)S(1)}, bf16[128,256]{1,0:T(8,128)(2,1)S(1)}, u32[]{:S(2)}, u32[]{:S(2)}) collective-permute-start(bf16[128,256]{1,0:T(8,128)(2,1)S(1)} %get-tuple-element.94), channel_id=1, source_target_pairs={{0,6},{1,7},{2,4},{3,5},{4,2},{5,3},{6,0},{7,1},{8,14},{9,15},{10,... | collective-permute-start | bytes 196616 | tf_op jit(solution)/shard_map/ppermute | solution.py:24
  88.5 6.5 %collective-permute-start.29 = (bf16[128,256]{1,0:T(8,128)(2,1)S(1)}, bf16[128,256]{1,0:T(8,128)(2,1)S(1)}, u32[]{:S(2)}, u32[]{:S(2)}) collective-permute-start(bf16[128,256]{1,0:T(8,128)(2,1)S(1)} %get-tuple-element.95), channel_id=1, source_target_pairs={{0,4},{1,5},{2,6},{3,7},{4,0},{5,1},{6,2},{7,3},{8,12},{9,13},{10,... | collective-permute-start | bytes 196616 | tf_op jit(solution)/shard_map/ppermute | solution.py:24
  88.5 6.5 %collective-permute-start.28 = (bf16[128,256]{1,0:T(8,128)(2,1)S(1)}, bf16[128,256]{1,0:T(8,128)(2,1)S(1)}, u32[]{:S(2)}, u32[]{:S(2)}) collective-permute-start(bf16[128,256]{1,0:T(8,128)(2,1)S(1)} %get-tuple-element.96), channel_id=1, source_target_pairs={{0,2},{1,3},{2,0},{3,1},{4,6},{5,7},{6,4},{7,5},{8,10},{9,11},{10,... | collective-permute-start | bytes 196616 | tf_op jit(solution)/shard_map/ppermute | solution.py:24

commit v2 on v1

--- a/solution.py
+++ b/solution.py
@@ -208,7 +208,7 @@
     for ref in got_refs:
         total = total + ref[...].astype(F32)
     total = total * factor_ref[:, :1]
-    turned_ref[...] = total.astype(BF16).astype(F32).T
+    turned_ref[...] = total.astype(BF16).T.astype(F32)
     span = heads * size
     outs = []
     for h in range(heads):
@@ -275,7 +275,7 @@
     total = functools.reduce(lambda x, y: x + y, chosen)
     combine = jnp.zeros((slots, rows), F32)
     for j, (value, share) in enumerate(zip(chosen, shares)):
-        weight = share * value / total
+        weight = share * (value / total)
         combine = combine + jnp.where(slot_iota == at_ref[j : j + 1, :], weight, 0.0)
     combine = combine.T
     high = combine.astype(BF16)
@@ -316,16 +316,16 @@
 
 def combine_kernel(chips, cols, blocks, *refs):
     y_refs = refs[:blocks]
-    high_ref, low_ref, away_ref, keep_ref = refs[blocks:]
+    high_ref, low_ref = refs[blocks : blocks + 2]
+    away_refs, keep_refs = refs[blocks + 2 : blocks + 2 + chips], refs[blocks + 2 + chips :]
     core = lax.axis_index("tp") % CORES
     for k in range(chips):
-        at = slice(k * cols, (k + 1) * cols)
-        for target, out_ref in ((1 - core, away_ref), (core, keep_ref)):
+        for target, out_ref in ((1 - core, away_refs[k]), (core, keep_refs[k])):
             ds = block_cols(k, target, cols)
             y = jnp.concatenate([ref[:, ds] for ref in y_refs], axis=0)
             value = jnp.dot(high_ref[...], y, preferred_element_type=F32)
             value = value + jnp.dot(low_ref[...], y, preferred_element_type=F32)
-            out_ref[:, at] = value.astype(out_ref.dtype)
+            out_ref[...] = value.astype(out_ref.dtype)
 
 
 def per_device(
@@ -524,15 +524,14 @@
         )
         terms.append(part)
     back = [terms[0]] + [ep_send(terms[k], k) for k in others]
-    moe_away, moe_keep = call(
+    moe_blocks = call(
         functools.partial(combine_kernel, chips, cols, ep_count),
-        [((rows, half), BF16), ((rows, half), F32)],
+        [((rows, cols), BF16)] * chips + [((rows, cols), F32)] * chips,
         *back,
         combine_high,
         combine_low,
     )
-    moe = moe_keep + core_send(moe_away).astype(F32)
-    moe_parts = [moe[:, k * cols : (k + 1) * cols] for k in range(chips)]
+    moe_parts = [moe_blocks[chips + k] + core_send(moe_blocks[k]).astype(F32) for k in range(chips)]
     moe_got = [chip_send(moe_parts[k].astype(BF16), k) for k in range(1, chips)]
     (mixed,) = call(
         final_kernel, [((rows, cols), BF16)], after_cols, moe_parts[0], *moe_got, limit=4

time: 95.9 us -> 95.8 us (level)
    ppermute x10 -> x13, starting transfers between devices: 1.24 us -> 2.25 us  [core_send(): return lax.ppermute(value, 'tp', [(i, i ^ 1) for i in range(count)])]
    ppermute x10 -> x13, waiting for transfers between devices: 3.69 us -> 2.82 us  [core_send(): return lax.ppermute(value, 'tp', [(i, i ^ 1) for i in range(count)])]
  transfers between devices with their start and end apart: 31 -> 34, of which waited for: 18 -> 20; matrix products, arithmetic and copies ran while one was open for 0% -> 0% of each run, Pallas kernels for 13% -> 12%
where the time goes in v2:
time: 95.8 us; the launch traced here: 95.6 us
  waiting for transfers between devices  43.1 us (45%)
  starting transfers between devices  30.6 us (32%)
  Pallas kernels  20.3 us (21%)
    ppermute x12, waiting for transfers between devices, ep_send(): return lax.ppermute(value, 'ep', [(i, i ^ step) for i in range(count)])  25.9 us
    pallas_call x19, Pallas kernels, call(): pl.pallas_call(kernel, out_shape=[jax.ShapeDtypeStruct(shape, dtype) for...  20.3 us
    ppermute x12, starting transfers between devices, ep_send(): return lax.ppermute(value, 'ep', [(i, i ^ step) for i in range(count)])  16.7 us
    ppermute x9, waiting for transfers between devices, chip_send(): lax.ppermute(value, 'tp', [(i, i ^ CORES * step) for i in range(count)])  14.4 us
    ppermute x9, starting transfers between devices, chip_send(): lax.ppermute(value, 'tp', [(i, i ^ CORES * step) for i in range(count)])  11.7 us
    ppermute x13, waiting for transfers between devices, core_send(): return lax.ppermute(value, 'tp', [(i, i ^ 1) for i in range(count)])  2.82 us
    ppermute x13, starting transfers between devices, core_send(): return lax.ppermute(value, 'tp', [(i, i ^ 1) for i in range(count)])  2.25 us
  transfers between devices with their start and end apart: 34, of which 20 were waited for; matrix products, arithmetic and copies ran while one was open for 0% of the time, Pallas kernels for 12%

profile of v2, /device:TPU:0, one launch (start us, length us, event | category | flops | bytes accessed | tf_op | source)
XLA Modules:
  0.0 95.6 jit_solution(5454948206890016062)
XLA Ops:
  0.6 1.1 %shard_map.228 = (bf16[128,512]{1,0:T(8,128)(2,1)S(1)}, bf16[128,512]{1,0:T(8,128)(2,1)S(1)}, bf16[128,512]{1,0:T(8,128)(2,1)S(1)}, bf16[128,512]{1,0:T(8,128)(2,1)S(1)}) custom-call(bf16[128,2048]{1,0:T(8,128)(2,1)} %refs_8_.1), custom_call_target="tpu_custom_call" | custom-call | tf_op jit(solution)/shard_map/pallas_call | solution.py:43
  1.8 4.0 %collective-permute-start.4 = (bf16[128,512]{1,0:T(8,128)(2,1)S(1)}, bf16[128,512]{1,0:T(8,128)(2,1)S(1)}, u32[]{:S(2)}, u32[]{:S(2)}) collective-permute-start(bf16[128,512]{1,0:T(8,128)(2,1)S(1)} %get-tuple-element.62), channel_id=1, source_target_pairs={{0,24},{8,16},{16,8},{24,0},{1,25},{9,17},{17,9},{25,1},{2,26},{10... | collective-permute-start | bytes 393224 | tf_op jit(solution)/shard_map/ppermute | solution.py:19
  5.8 0.5 collective-permute-start.2
  6.4 1.2 %shard_map.229 = (bf16[512,256]{1,0:T(8,128)(2,1)S(1)}, bf16[512,256]{1,0:T(8,128)(2,1)S(1)}, bf16[512,256]{1,0:T(8,128)(2,1)S(1)}, bf16[512,256]{1,0:T(8,128)(2,1)S(1)}, f32[1,512]{1,0:T(1,128)S(1)}) custom-call(f32[1,2048]{1,0:T(1,128)} %bitcast.25, bf16[512,256]{1,0:T(8,128)(2,1)} %refs_0_.1, bf16[512,256]{1,0:T(8,128)(2,1)} %refs_1_.1, ...), custom_call_target="tpu_custom_call" | custom-call | tf_op jit(solution)/shard_map/pallas_call | solution.py:43
  7.7 2.0 %collective-permute-done.4.x_ref = bf16[128,512]{1,0:T(8,128)(2,1)S(1)} collective-permute-done((bf16[128,512]{1,0:T(8,128)(2,1)S(1)}, bf16[128,512]{1,0:T(8,128)(2,1)S(1)}, u32[]{:S(2)}, u32[]{:S(2)}) %collective-permute-start.4) | collective-permute-done | bytes 131104 | tf_op jit(solution)/shard_map/ppermute | solution.py:19
  10.0 2.1 %collective-permute-done.2.x_ref = bf16[128,512]{1,0:T(8,128)(2,1)S(1)} collective-permute-done((bf16[128,512]{1,0:T(8,128)(2,1)S(1)}, bf16[128,512]{1,0:T(8,128)(2,1)S(1)}, u32[]{:S(2)}, u32[]{:S(2)}) %collective-permute-start.2) | collective-permute-done | bytes 131104 | tf_op jit(solution)/shard_map/ppermute | solution.py:19
  12.8 0.7 copy-done.3
  13.4 5.8 %shard_map.234 = (bf16[256,1024]{1,0:T(8,128)(2,1)S(1)}, bf16[256,1024]{1,0:T(8,128)(2,1)S(1)}, f32[4,64,64,128]{3,2,1,0:T(8,128)S(1)}, f32[4,64,128]{2,1,0:T(8,...) custom-call(bf16[128,1024]{1,0:T(8,128)(2,1)S(1)} %shard_map.231.ref, ...), custom_call_target="tpu_custom_call" | custom-call | tf_op jit(solution)/shard_map/pallas_call | solution.py:43
  19.4 1.7 %collective-permute-start.1 = (bf16[128,1024]{1,0:T(8,128)(2,1)S(1)}, bf16[128,1024]{1,0:T(8,128)(2,1)S(1)}, u32[]{:S(2)}, u32[]{:S(2)}) collective-permute-start(bf16[128,1024]{1,0:T(8,128)(2,1)S(1)} %shard_map.231.refs_0_), channel_id=1, source_target_pairs={{0,8},{8,0},{16,24},{24,16},{1,9},{9,1},{17,25},{25,17},{2,10},{10... | collective-permute-start | bytes 786440 | tf_op jit(solution)/shard_map/ppermute | solution.py:19
  21.1 0.7 collective-permute-start.3
  21.8 1.1 %collective-permute-start.5 = (bf16[128,1024]{1,0:T(8,128)(2,1)S(1)}, bf16[128,1024]{1,0:T(8,128)(2,1)S(1)}, u32[]{:S(2)}, u32[]{:S(2)}) collective-permute-start(bf16[128,1024]{1,0:T(8,128)(2,1)S(1)} %shard_map.233.refs_2_), channel_id=1, source_target_pairs={{0,24},{8,16},{16,8},{24,0},{1,25},{9,17},{17,9},{25,1},{2,26},{10... | collective-permute-start | bytes 786440 | tf_op jit(solution)/shard_map/ppermute | solution.py:19
  23.2 5.4 %collective-permute-done.1.refs_1_ = bf16[128,1024]{1,0:T(8,128)(2,1)S(1)} collective-permute-done((bf16[128,1024]{1,0:T(8,128)(2,1)S(1)}, bf16[128,1024]{1,0:T(8,128)(2,1)S(1)}, u32[]{:S(2)}, u32[]{:S(2)}) %collective-permute-start.1) | collective-permute-done | bytes 262176 | tf_op jit(solution)/shard_map/ppermute | solution.py:19
  28.6 6.5 %collective-permute-done.3.refs_2_ = bf16[128,1024]{1,0:T(8,128)(2,1)S(1)} collective-permute-done((bf16[128,1024]{1,0:T(8,128)(2,1)S(1)}, bf16[128,1024]{1,0:T(8,128)(2,1)S(1)}, u32[]{:S(2)}, u32[]{:S(2)}) %collective-permute-start.3) | collective-permute-done | bytes 262176 | tf_op jit(solution)/shard_map/ppermute | solution.py:19
  35.1 1.6 %shard_map.235 = (bf16[128,256]{1,0:T(8,128)(2,1)S(1)}, f32[4,64,128]{2,1,0:T(8,128)S(1)}, f32[4,64,128]{2,1,0:T(8,128)S(1)}, f32[4,64,128]{2,1,0:T(8,128)}) custom-call(f32[128,1024]{1,0:T(8,128)S(1)} %shard_map.230.refs_0_, bf16[128,1024]{1,0:T(8,128)(2,1)S(1)} %collective-permute-done.1.refs_1_, bf16[128,1024]{1,0:T(8,128)(2,1)S(1)} %collective-permute-done.3.refs_2_, ...), custom_call_target="tpu_custom_call" | custom-call | tf_op jit(solution)/shard_map/pallas_call | solution.py:43
  36.8 1.3 %collective-permute-done.7.got_ref = bf16[128,256]{1,0:T(8,128)(2,1)S(1)} collective-permute-done((bf16[128,256]{1,0:T(8,128)(2,1)S(1)}, bf16[128,256]{1,0:T(8,128)(2,1)S(1)}, u32[]{:S(2)}, u32[]{:S(2)}) %collective-permute-start.7) | collective-permute-done | bytes 65568 | tf_op jit(solution)/shard_map/ppermute | solution.py:29
  38.3 1.6 %collective-permute-start.8 = (bf16[128,256]{1,0:T(8,128)(2,1)S(1)}, bf16[128,256]{1,0:T(8,128)(2,1)S(1)}, u32[]{:S(2)}, u32[]{:S(2)}) collective-permute-start(bf16[128,256]{1,0:T(8,128)(2,1)S(1)} %get-tuple-element.76), channel_id=1, source_target_pairs={{0,2},{1,3},{2,0},{3,1},{4,6},{5,7},{6,4},{7,5},{8,10},{9,11},{10,... | collective-permute-start | bytes 196616 | tf_op jit(solution)/shard_map/ppermute | solution.py:24
  40.0 2.6 %collective-permute-start.9 = (bf16[128,256]{1,0:T(8,128)(2,1)S(1)}, bf16[128,256]{1,0:T(8,128)(2,1)S(1)}, u32[]{:S(2)}, u32[]{:S(2)}) collective-permute-start(bf16[128,256]{1,0:T(8,128)(2,1)S(1)} %get-tuple-element.77), channel_id=1, source_target_pairs={{0,4},{1,5},{2,6},{3,7},{4,0},{5,1},{6,2},{7,3},{8,12},{9,13},{10,... | collective-permute-start | bytes 196616 | tf_op jit(solution)/shard_map/ppermute | solution.py:24
  42.8 0.5 collective-permute-start.20
  43.3 3.8 %shard_map.237 = (f32[4,64,64,128]{3,2,1,0:T(8,128)}, f32[8,128]{1,0:T(8,128)S(1)}) custom-call(bf16[128,256]{1,0:T(8,128)(2,1)S(1)} %get-tuple-element.70.after_ref, f32[4,64,64,128]{3,2,1,0:T(8,128)S(1)} %get-tuple-element.64.refs_5_.matrix_ref, f32[4,64,128]{2,1,0:T(8,128)S(1)} %get-tuple-element.71.key_ref, ...), custom_call_target="tpu_custom_call" | custom-call | tf_op jit(solution)/shard_map/pallas_call | solution.py:43
  47.5 1.2 %collective-permute-done.10.refs_4_ = bf16[128,256]{1,0:T(8,128)(2,1)S(1)} collective-permute-done((bf16[128,256]{1,0:T(8,128)(2,1)S(1)}, bf16[128,256]{1,0:T(8,128)(2,1)S(1)}, u32[]{:S(2)}, u32[]{:S(2)}) %collective-permute-start.10) | collective-permute-done | bytes 65568 | tf_op jit(solution)/shard_map/ppermute | solution.py:24
  48.9 2.6 %collective-permute-start.13 = (bf16[128,256]{1,0:T(8,128)(2,1)S(1)}, bf16[128,256]{1,0:T(8,128)(2,1)S(1)}, u32[]{:S(2)}, u32[]{:S(2)}) collective-permute-start(bf16[128,256]{1,0:T(8,128)(2,1)S(1)} %shard_map.238.refs_0_), channel_id=1, source_target_pairs={{0,6},{1,7},{2,4},{3,5},{4,2},{5,3},{6,0},{7,1},{8,14},{9,15},{10,... | collective-permute-start | bytes 196616 | tf_op jit(solution)/shard_map/ppermute | solution.py:24
  51.9 3.9 %collective-permute-done.13.refs_3_ = bf16[128,256]{1,0:T(8,128)(2,1)S(1)} collective-permute-done((bf16[128,256]{1,0:T(8,128)(2,1)S(1)}, bf16[128,256]{1,0:T(8,128)(2,1)S(1)}, u32[]{:S(2)}, u32[]{:S(2)}) %collective-permute-start.13) | collective-permute-done | bytes 65568 | tf_op jit(solution)/shard_map/ppermute | solution.py:24
  55.8 2.2 %collective-permute-done.12.refs_2_ = bf16[128,256]{1,0:T(8,128)(2,1)S(1)} collective-permute-done((bf16[128,256]{1,0:T(8,128)(2,1)S(1)}, bf16[128,256]{1,0:T(8,128)(2,1)S(1)}, u32[]{:S(2)}, u32[]{:S(2)}) %collective-permute-start.12) | collective-permute-done | bytes 65568 | tf_op jit(solution)/shard_map/ppermute | solution.py:24
  58.0 2.0 %collective-permute-done.11.refs_1_ = bf16[128,256]{1,0:T(8,128)(2,1)S(1)} collective-permute-done((bf16[128,256]{1,0:T(8,128)(2,1)S(1)}, bf16[128,256]{1,0:T(8,128)(2,1)S(1)}, u32[]{:S(2)}, u32[]{:S(2)}) %collective-permute-start.11) | collective-permute-done | bytes 65568 | tf_op jit(solution)/shard_map/ppermute | solution.py:24
  60.1 0.5 collective-permute-start.15
  60.6 0.7 collective-permute-done.16.refs_6_
  61.5 0.6 shard_map.239
  62.1 0.6 collective-permute-start.21
  62.7 1.5 %collective-permute-start.23 = (bf16[48,2048]{1,0:T(8,128)(2,1)S(1)}, bf16[48,2048]{1,0:T(8,128)(2,1)S(1)}, u32[]{:S(2)}, u32[]{:S(2)}) collective-permute-start(bf16[48,2048]{1,0:T(8,128)(2,1)S(1)} %get-tuple-element.87), channel_id=1, source_target_pairs={{0,16},{8,24},{16,0},{24,8},{1,17},{9,25},{17,1},{25,9},{2,18},{10... | collective-permute-start | bytes 589832 | tf_op jit(solution)/shard_map/ppermute | solution.py:19
  64.2 1.4 %collective-permute-start.25 = (bf16[48,2048]{1,0:T(8,128)(2,1)S(1)}, bf16[48,2048]{1,0:T(8,128)(2,1)S(1)}, u32[]{:S(2)}, u32[]{:S(2)}) collective-permute-start(bf16[48,2048]{1,0:T(8,128)(2,1)S(1)} %get-tuple-element.88), channel_id=1, source_target_pairs={{0,24},{8,16},{16,8},{24,0},{1,25},{9,17},{17,9},{25,1},{2,26},{10... | collective-permute-start | bytes 589832 | tf_op jit(solution)/shard_map/ppermute | solution.py:19
  65.6 4.3 %collective-permute-done.21.x_ref = bf16[48,2048]{1,0:T(8,128)(2,1)S(1)} collective-permute-done((bf16[48,2048]{1,0:T(8,128)(2,1)S(1)}, bf16[48,2048]{1,0:T(8,128)(2,1)S(1)}, u32[]{:S(2)}, u32[]{:S(2)}) %collective-permute-start.21) | collective-permute-done | bytes 196640 | tf_op jit(solution)/shard_map/ppermute | solution.py:19
  69.9 0.7 shard_map.241
  70.6 0.6 collective-permute-start.22
  71.2 1.1 %collective-permute-done.23.x_ref = bf16[48,2048]{1,0:T(8,128)(2,1)S(1)} collective-permute-done((bf16[48,2048]{1,0:T(8,128)(2,1)S(1)}, bf16[48,2048]{1,0:T(8,128)(2,1)S(1)}, u32[]{:S(2)}, u32[]{:S(2)}) %collective-permute-start.23) | collective-permute-done | bytes 196640 | tf_op jit(solution)/shard_map/ppermute | solution.py:19
  72.3 0.7 shard_map.242
  73.0 2.9 %collective-permute-start.24 = (bf16[48,2048]{1,0:T(8,128)(2,1)S(1)}, bf16[48,2048]{1,0:T(8,128)(2,1)S(1)}, u32[]{:S(2)}, u32[]{:S(2)}) collective-permute-start(bf16[48,2048]{1,0:T(8,128)(2,1)S(1)} %shard_map.242), channel_id=1, source_target_pairs={{0,16},{8,24},{16,0},{24,8},{1,17},{9,25},{17,1},{25,9},{2,18},{10... | collective-permute-start | bytes 589832 | tf_op jit(solution)/shard_map/ppermute | solution.py:19
  75.9 0.7 shard_map.243
  76.6 1.4 %collective-permute-start.26 = (bf16[48,2048]{1,0:T(8,128)(2,1)S(1)}, bf16[48,2048]{1,0:T(8,128)(2,1)S(1)}, u32[]{:S(2)}, u32[]{:S(2)}) collective-permute-start(bf16[48,2048]{1,0:T(8,128)(2,1)S(1)} %shard_map.243), channel_id=1, source_target_pairs={{0,24},{8,16},{16,8},{24,0},{1,25},{9,17},{17,9},{25,1},{2,26},{10... | collective-permute-start | bytes 589832 | tf_op jit(solution)/shard_map/ppermute | solution.py:19
  78.1 0.5 shard_map.244
  78.6 0.7 shard_map.240.refs_0_
  79.3 4.5 %collective-permute-done.24.refs_2_ = bf16[48,2048]{1,0:T(8,128)(2,1)S(1)} collective-permute-done((bf16[48,2048]{1,0:T(8,128)(2,1)S(1)}, bf16[48,2048]{1,0:T(8,128)(2,1)S(1)}, u32[]{:S(2)}, u32[]{:S(2)}) %collective-permute-start.24) | collective-permute-done | bytes 196640 | tf_op jit(solution)/shard_map/ppermute | solution.py:19
  83.8 0.4 shard_map.245
  84.3 0.5 collective-permute-start.27
  86.1 2.6 %collective-permute-start.31 = (bf16[128,256]{1,0:T(8,128)(2,1)S(1)}, bf16[128,256]{1,0:T(8,128)(2,1)S(1)}, u32[]{:S(2)}, u32[]{:S(2)}) collective-permute-start(bf16[128,256]{1,0:T(8,128)(2,1)S(1)} %add_convert_fusion.1), channel_id=1, source_target_pairs={{0,4},{1,5},{2,6},{3,7},{4,0},{5,1},{6,2},{7,3},{8,12},{9,13},{10,... | collective-permute-start | bytes 196616 | tf_op jit(solution)/shard_map/ppermute | solution.py:24
  88.7 1.5 %collective-permute-start.33 = (bf16[128,256]{1,0:T(8,128)(2,1)S(1)}, bf16[128,256]{1,0:T(8,128)(2,1)S(1)}, u32[]{:S(2)}, u32[]{:S(2)}) collective-permute-start(bf16[128,256]{1,0:T(8,128)(2,1)S(1)} %add_convert_fusion), channel_id=1, source_target_pairs={{0,6},{1,7},{2,4},{3,5},{4,2},{5,3},{6,0},{7,1},{8,14},{9,15},{10,... | collective-permute-start | bytes 196616 | tf_op jit(solution)/shard_map/ppermute | solution.py:24
  90.6 3.0 %collective-permute-done.31.refs_3_ = bf16[128,256]{1,0:T(8,128)(2,1)S(1)} collective-permute-done((bf16[128,256]{1,0:T(8,128)(2,1)S(1)}, bf16[128,256]{1,0:T(8,128)(2,1)S(1)}, u32[]{:S(2)}, u32[]{:S(2)}) %collective-permute-start.31) | collective-permute-done | bytes 65568 | tf_op jit(solution)/shard_map/ppermute | solution.py:24
  93.6 1.3 %collective-permute-done.33.refs_4_ = bf16[128,256]{1,0:T(8,128)(2,1)S(1)} collective-permute-done((bf16[128,256]{1,0:T(8,128)(2,1)S(1)}, bf16[128,256]{1,0:T(8,128)(2,1)S(1)}, u32[]{:S(2)}, u32[]{:S(2)}) %collective-permute-start.33) | collective-permute-done | bytes 65568 | tf_op jit(solution)/shard_map/ppermute | solution.py:24
  94.9 0.7 shard_map.246
  (53 shorter events, 4.9 us)
Async XLA Ops:
  1.8 7.9 %collective-permute-start.4 = (bf16[128,512]{1,0:T(8,128)(2,1)S(1)}, bf16[128,512]{1,0:T(8,128)(2,1)S(1)}, u32[]{:S(2)}, u32[]{:S(2)}) collective-permute-start(bf16[128,512]{1,0:T(8,128)(2,1)S(1)} %get-tuple-element.62), channel_id=1, source_target_pairs={{0,24},{8,16},{16,8},{24,0},{1,25},{9,17},{17,9},{25,1},{2,26},{10... | collective-permute-start | bytes 393224 | tf_op jit(solution)/shard_map/ppermute | solution.py:19
  5.8 6.3 %collective-permute-start.2 = (bf16[128,512]{1,0:T(8,128)(2,1)S(1)}, bf16[128,512]{1,0:T(8,128)(2,1)S(1)}, u32[]{:S(2)}, u32[]{:S(2)}) collective-permute-start(bf16[128,512]{1,0:T(8,128)(2,1)S(1)} %get-tuple-element.61), channel_id=1, source_target_pairs={{0,16},{8,24},{16,0},{24,8},{1,17},{9,25},{17,1},{25,9},{2,18},{10... | collective-permute-start | bytes 393224 | tf_op jit(solution)/shard_map/ppermute | solution.py:19
  6.3 6.1 %collective-permute-start = (bf16[128,512]{1,0:T(8,128)(2,1)S(1)}, bf16[128,512]{1,0:T(8,128)(2,1)S(1)}, u32[]{:S(2)}, u32[]{:S(2)}) collective-permute-start(bf16[128,512]{1,0:T(8,128)(2,1)S(1)} %get-tuple-element.60), channel_id=1, source_target_pairs={{0,8},{8,0},{16,24},{24,16},{1,9},{9,1},{17,25},{25,17},{2,10},{10... | collective-permute-start | bytes 393224 | tf_op jit(solution)/shard_map/ppermute | solution.py:19
  12.4 22.7 %copy-start.4 = (f32[256]{0:T(256)S(1)}, f32[256]{0:T(256)}, u32[]{:S(2)}) copy-start(f32[256]{0:T(256)} %param.30) | copy-start | bytes 3076
  12.7 0.7 copy-start.3
  19.3 15.8 %collective-permute-start.6 = (bf16[256,1024]{1,0:T(8,128)(2,1)S(1)}, bf16[256,1024]{1,0:T(8,128)(2,1)S(1)}, u32[]{:S(2)}, u32[]{:S(2)}) collective-permute-start(bf16[256,1024]{1,0:T(8,128)(2,1)S(1)} %get-tuple-element.67), channel_id=1, source_target_pairs={{0,1},{1,0},{2,3},{3,2},{4,5},{5,4},{6,7},{7,6},{8,9},{9,8},{10,11... | collective-permute-start | bytes 1572872 | tf_op jit(solution)/shard_map/ppermute | solution.py:29
  19.4 9.2 %collective-permute-start.1 = (bf16[128,1024]{1,0:T(8,128)(2,1)S(1)}, bf16[128,1024]{1,0:T(8,128)(2,1)S(1)}, u32[]{:S(2)}, u32[]{:S(2)}) collective-permute-start(bf16[128,1024]{1,0:T(8,128)(2,1)S(1)} %shard_map.231.refs_0_), channel_id=1, source_target_pairs={{0,8},{8,0},{16,24},{24,16},{1,9},{9,1},{17,25},{25,17},{2,10},{10... | collective-permute-start | bytes 786440 | tf_op jit(solution)/shard_map/ppermute | solution.py:19
  21.1 14.0 %collective-permute-start.3 = (bf16[128,1024]{1,0:T(8,128)(2,1)S(1)}, bf16[128,1024]{1,0:T(8,128)(2,1)S(1)}, u32[]{:S(2)}, u32[]{:S(2)}) collective-permute-start(bf16[128,1024]{1,0:T(8,128)(2,1)S(1)} %shard_map.232.refs_1_), channel_id=1, source_target_pairs={{0,16},{8,24},{16,0},{24,8},{1,17},{9,25},{17,1},{25,9},{2,18},{10... | collective-permute-start | bytes 786440 | tf_op jit(solution)/shard_map/ppermute | solution.py:19
  21.8 13.3 %collective-permute-start.5 = (bf16[128,1024]{1,0:T(8,128)(2,1)S(1)}, bf16[128,1024]{1,0:T(8,128)(2,1)S(1)}, u32[]{:S(2)}, u32[]{:S(2)}) collective-permute-start(bf16[128,1024]{1,0:T(8,128)(2,1)S(1)} %shard_map.233.refs_2_), channel_id=1, source_target_pairs={{0,24},{8,16},{16,8},{24,0},{1,25},{9,17},{17,9},{25,1},{2,26},{10... | collective-permute-start | bytes 786440 | tf_op jit(solution)/shard_map/ppermute | solution.py:19
  22.9 41.3 %collective-permute-start.18 = (bf16[2048,128]{1,0:T(8,128)(2,1)S(1)}, bf16[2048,128]{1,0:T(8,128)(2,1)S(1)}, u32[]{:S(2)}, u32[]{:S(2)}) collective-permute-start(bf16[2048,128]{1,0:T(8,128)(2,1)S(1)} %get-tuple-element.83), channel_id=1, source_target_pairs={{0,1},{1,0},{2,3},{3,2},{4,5},{5,4},{6,7},{7,6},{8,9},{9,8},{10,11... | collective-permute-start | bytes 1572872 | tf_op jit(solution)/shard_map/ppermute | solution.py:29
  35.1 26.4 %copy-start.2 = (f32[2048]{0:T(1024)S(1)}, f32[2048]{0:T(1024)}, u32[]{:S(2)}) copy-start(f32[2048]{0:T(1024)} %param.35) | copy-start | bytes 24580
  36.8 1.3 %collective-permute-start.7 = (bf16[128,256]{1,0:T(8,128)(2,1)S(1)}, bf16[128,256]{1,0:T(8,128)(2,1)S(1)}, u32[]{:S(2)}, u32[]{:S(2)}) collective-permute-start(bf16[128,256]{1,0:T(8,128)(2,1)S(1)} %get-tuple-element.68.own_ref), channel_id=1, source_target_pairs={{0,1},{1,0},{2,3},{3,2},{4,5},{5,4},{6,7},{7,6},{8,9},{9,8},{10,11... | collective-permute-start | bytes 196616 | tf_op jit(solution)/shard_map/ppermute | solution.py:29
  38.3 4.5 %collective-permute-start.8 = (bf16[128,256]{1,0:T(8,128)(2,1)S(1)}, bf16[128,256]{1,0:T(8,128)(2,1)S(1)}, u32[]{:S(2)}, u32[]{:S(2)}) collective-permute-start(bf16[128,256]{1,0:T(8,128)(2,1)S(1)} %get-tuple-element.76), channel_id=1, source_target_pairs={{0,2},{1,3},{2,0},{3,1},{4,6},{5,7},{6,4},{7,5},{8,10},{9,11},{10,... | collective-permute-start | bytes 196616 | tf_op jit(solution)/shard_map/ppermute | solution.py:24
  40.0 7.5 %collective-permute-start.9 = (bf16[128,256]{1,0:T(8,128)(2,1)S(1)}, bf16[128,256]{1,0:T(8,128)(2,1)S(1)}, u32[]{:S(2)}, u32[]{:S(2)}) collective-permute-start(bf16[128,256]{1,0:T(8,128)(2,1)S(1)} %get-tuple-element.77), channel_id=1, source_target_pairs={{0,4},{1,5},{2,6},{3,7},{4,0},{5,1},{6,2},{7,3},{8,12},{9,13},{10,... | collective-permute-start | bytes 196616 | tf_op jit(solution)/shard_map/ppermute | solution.py:24
  42.6 6.2 %collective-permute-start.10 = (bf16[128,256]{1,0:T(8,128)(2,1)S(1)}, bf16[128,256]{1,0:T(8,128)(2,1)S(1)}, u32[]{:S(2)}, u32[]{:S(2)}) collective-permute-start(bf16[128,256]{1,0:T(8,128)(2,1)S(1)} %get-tuple-element.70.after_ref), channel_id=1, source_target_pairs={{0,6},{1,7},{2,4},{3,5},{4,2},{5,3},{6,0},{7,1},{8,14},{9,15},{10,... | collective-permute-start | bytes 196616 | tf_op jit(solution)/shard_map/ppermute | solution.py:24
  42.8 22.8 %collective-permute-start.19 = (bf16[2048,128]{1,0:T(8,128)(2,1)S(1)}, bf16[2048,128]{1,0:T(8,128)(2,1)S(1)}, u32[]{:S(2)}, u32[]{:S(2)}) collective-permute-start(bf16[2048,128]{1,0:T(8,128)(2,1)S(1)} %get-tuple-element.84), channel_id=1, source_target_pairs={{0,1},{1,0},{2,3},{3,2},{4,5},{5,4},{6,7},{7,6},{8,9},{9,8},{10,11... | collective-permute-start | bytes 1572872 | tf_op jit(solution)/shard_map/ppermute | solution.py:29
  42.8 22.8 %collective-permute-start.20 = (bf16[128,2048]{1,0:T(8,128)(2,1)S(1)}, bf16[128,2048]{1,0:T(8,128)(2,1)S(1)}, u32[]{:S(2)}, u32[]{:S(2)}) collective-permute-start(bf16[128,2048]{1,0:T(8,128)(2,1)S(1)} %get-tuple-element.85), channel_id=1, source_target_pairs={{0,1},{1,0},{2,3},{3,2},{4,5},{5,4},{6,7},{7,6},{8,9},{9,8},{10,11... | collective-permute-start | bytes 1572872 | tf_op jit(solution)/shard_map/ppermute | solution.py:29
  43.3 34.7 %copy-start = (bf16[2048,8]{0,1:T(8,128)(2,1)S(1)}, bf16[2048,8]{0,1:T(8,128)(2,1)}, u32[]{:S(2)}) copy-start(bf16[2048,8]{0,1:T(8,128)(2,1)} %param.37) | copy-start | bytes 98308
  43.3 34.7 %copy-start.1 = (bf16[2048,4]{0,1:T(4,128)(2,1)S(1)}, bf16[2048,4]{0,1:T(4,128)(2,1)}, u32[]{:S(2)}) copy-start(bf16[2048,4]{0,1:T(4,128)(2,1)} %param.36) | copy-start | bytes 49156
  48.8 2.7 %collective-permute-start.14 = (bf16[128,256]{1,0:T(8,128)(2,1)S(1)}, bf16[128,256]{1,0:T(8,128)(2,1)S(1)}, u32[]{:S(2)}, u32[]{:S(2)}) collective-permute-start(bf16[128,256]{1,0:T(8,128)(2,1)S(1)} %shard_map.238.refs_0_), channel_id=1, source_target_pairs={{0,1},{1,0},{2,3},{3,2},{4,5},{5,4},{6,7},{7,6},{8,9},{9,8},{10,11... | collective-permute-start | bytes 196616 | tf_op jit(solution)/shard_map/ppermute | solution.py:29
  48.9 6.9 %collective-permute-start.13 = (bf16[128,256]{1,0:T(8,128)(2,1)S(1)}, bf16[128,256]{1,0:T(8,128)(2,1)S(1)}, u32[]{:S(2)}, u32[]{:S(2)}) collective-permute-start(bf16[128,256]{1,0:T(8,128)(2,1)S(1)} %shard_map.238.refs_0_), channel_id=1, source_target_pairs={{0,6},{1,7},{2,4},{3,5},{4,2},{5,3},{6,0},{7,1},{8,14},{9,15},{10,... | collective-permute-start | bytes 196616 | tf_op jit(solution)/shard_map/ppermute | solution.py:24
  51.5 6.6 %collective-permute-start.12 = (bf16[128,256]{1,0:T(8,128)(2,1)S(1)}, bf16[128,256]{1,0:T(8,128)(2,1)S(1)}, u32[]{:S(2)}, u32[]{:S(2)}) collective-permute-start(bf16[128,256]{1,0:T(8,128)(2,1)S(1)} %shard_map.238.refs_0_), channel_id=1, source_target_pairs={{0,4},{1,5},{2,6},{3,7},{4,0},{5,1},{6,2},{7,3},{8,12},{9,13},{10,... | collective-permute-start | bytes 196616 | tf_op jit(solution)/shard_map/ppermute | solution.py:24
  55.8 4.3 %collective-permute-start.11 = (bf16[128,256]{1,0:T(8,128)(2,1)S(1)}, bf16[128,256]{1,0:T(8,128)(2,1)S(1)}, u32[]{:S(2)}, u32[]{:S(2)}) collective-permute-start(bf16[128,256]{1,0:T(8,128)(2,1)S(1)} %shard_map.238.refs_0_), channel_id=1, source_target_pairs={{0,2},{1,3},{2,0},{3,1},{4,6},{5,7},{6,4},{7,5},{8,10},{9,11},{10,... | collective-permute-start | bytes 196616 | tf_op jit(solution)/shard_map/ppermute | solution.py:24
  58.0 2.0 %collective-permute-start.17 = (bf16[128,256]{1,0:T(8,128)(2,1)S(1)}, bf16[128,256]{1,0:T(8,128)(2,1)S(1)}, u32[]{:S(2)}, u32[]{:S(2)}) collective-permute-start(bf16[128,256]{1,0:T(8,128)(2,1)S(1)} %collective-permute-done.13.refs_3_), channel_id=1, source_target_pairs={{0,1},{1,0},{2,3},{3,2},{4,5},{5,4},{6,7},{7,6},{8,9},{9,8},{10,11... | collective-permute-start | bytes 196616 | tf_op jit(solution)/shard_map/ppermute | solution.py:29
  60.1 1.3 %collective-permute-start.16 = (bf16[128,256]{1,0:T(8,128)(2,1)S(1)}, bf16[128,256]{1,0:T(8,128)(2,1)S(1)}, u32[]{:S(2)}, u32[]{:S(2)}) collective-permute-start(bf16[128,256]{1,0:T(8,128)(2,1)S(1)} %collective-permute-done.12.refs_2_), channel_id=1, source_target_pairs={{0,1},{1,0},{2,3},{3,2},{4,5},{5,4},{6,7},{7,6},{8,9},{9,8},{10,11... | collective-permute-start | bytes 196616 | tf_op jit(solution)/shard_map/ppermute | solution.py:29
  60.1 1.4 %collective-permute-start.15 = (bf16[128,256]{1,0:T(8,128)(2,1)S(1)}, bf16[128,256]{1,0:T(8,128)(2,1)S(1)}, u32[]{:S(2)}, u32[]{:S(2)}) collective-permute-start(bf16[128,256]{1,0:T(8,128)(2,1)S(1)} %collective-permute-done.11.refs_1_), channel_id=1, source_target_pairs={{0,1},{1,0},{2,3},{3,2},{4,5},{5,4},{6,7},{7,6},{8,9},{9,8},{10,11... | collective-permute-start | bytes 196616 | tf_op jit(solution)/shard_map/ppermute | solution.py:29
  62.1 7.8 %collective-permute-start.21 = (bf16[48,2048]{1,0:T(8,128)(2,1)S(1)}, bf16[48,2048]{1,0:T(8,128)(2,1)S(1)}, u32[]{:S(2)}, u32[]{:S(2)}) collective-permute-start(bf16[48,2048]{1,0:T(8,128)(2,1)S(1)} %get-tuple-element.86), channel_id=1, source_target_pairs={{0,8},{8,0},{16,24},{24,16},{1,9},{9,1},{17,25},{25,17},{2,10},{10... | collective-permute-start | bytes 589832 | tf_op jit(solution)/shard_map/ppermute | solution.py:19
  62.7 9.6 %collective-permute-start.23 = (bf16[48,2048]{1,0:T(8,128)(2,1)S(1)}, bf16[48,2048]{1,0:T(8,128)(2,1)S(1)}, u32[]{:S(2)}, u32[]{:S(2)}) collective-permute-start(bf16[48,2048]{1,0:T(8,128)(2,1)S(1)} %get-tuple-element.87), channel_id=1, source_target_pairs={{0,16},{8,24},{16,0},{24,8},{1,17},{9,25},{17,1},{25,9},{2,18},{10... | collective-permute-start | bytes 589832 | tf_op jit(solution)/shard_map/ppermute | solution.py:19
  64.2 11.7 %collective-permute-start.25 = (bf16[48,2048]{1,0:T(8,128)(2,1)S(1)}, bf16[48,2048]{1,0:T(8,128)(2,1)S(1)}, u32[]{:S(2)}, u32[]{:S(2)}) collective-permute-start(bf16[48,2048]{1,0:T(8,128)(2,1)S(1)} %get-tuple-element.88), channel_id=1, source_target_pairs={{0,24},{8,16},{16,8},{24,0},{1,25},{9,17},{17,9},{25,1},{2,26},{10... | collective-permute-start | bytes 589832 | tf_op jit(solution)/shard_map/ppermute | solution.py:19
  70.6 8.7 %collective-permute-start.22 = (bf16[48,2048]{1,0:T(8,128)(2,1)S(1)}, bf16[48,2048]{1,0:T(8,128)(2,1)S(1)}, u32[]{:S(2)}, u32[]{:S(2)}) collective-permute-start(bf16[48,2048]{1,0:T(8,128)(2,1)S(1)} %shard_map.241), channel_id=1, source_target_pairs={{0,8},{8,0},{16,24},{24,16},{1,9},{9,1},{17,25},{25,17},{2,10},{10... | collective-permute-start | bytes 589832 | tf_op jit(solution)/shard_map/ppermute | solution.py:19
  73.0 10.8 %collective-permute-start.24 = (bf16[48,2048]{1,0:T(8,128)(2,1)S(1)}, bf16[48,2048]{1,0:T(8,128)(2,1)S(1)}, u32[]{:S(2)}, u32[]{:S(2)}) collective-permute-start(bf16[48,2048]{1,0:T(8,128)(2,1)S(1)} %shard_map.242), channel_id=1, source_target_pairs={{0,16},{8,24},{16,0},{24,8},{1,17},{9,25},{17,1},{25,9},{2,18},{10... | collective-permute-start | bytes 589832 | tf_op jit(solution)/shard_map/ppermute | solution.py:19
  76.6 7.2 %collective-permute-start.26 = (bf16[48,2048]{1,0:T(8,128)(2,1)S(1)}, bf16[48,2048]{1,0:T(8,128)(2,1)S(1)}, u32[]{:S(2)}, u32[]{:S(2)}) collective-permute-start(bf16[48,2048]{1,0:T(8,128)(2,1)S(1)} %shard_map.243), channel_id=1, source_target_pairs={{0,24},{8,16},{16,8},{24,0},{1,25},{9,17},{17,9},{25,1},{2,26},{10... | collective-permute-start | bytes 589832 | tf_op jit(solution)/shard_map/ppermute | solution.py:19
  84.2 1.3 %collective-permute-start.28 = (bf16[128,256]{1,0:T(8,128)(2,1)S(1)}, bf16[128,256]{1,0:T(8,128)(2,1)S(1)}, u32[]{:S(2)}, u32[]{:S(2)}) collective-permute-start(bf16[128,256]{1,0:T(8,128)(2,1)S(1)} %get-tuple-element.96), channel_id=1, source_target_pairs={{0,1},{1,0},{2,3},{3,2},{4,5},{5,4},{6,7},{7,6},{8,9},{9,8},{10,11... | collective-permute-start | bytes 196616 | tf_op jit(solution)/shard_map/ppermute | solution.py:29
  84.3 5.9 %collective-permute-start.27 = (bf16[128,256]{1,0:T(8,128)(2,1)S(1)}, bf16[128,256]{1,0:T(8,128)(2,1)S(1)}, u32[]{:S(2)}, u32[]{:S(2)}) collective-permute-start(bf16[128,256]{1,0:T(8,128)(2,1)S(1)} %get-tuple-element.94), channel_id=1, source_target_pairs={{0,1},{1,0},{2,3},{3,2},{4,5},{5,4},{6,7},{7,6},{8,9},{9,8},{10,11... | collective-permute-start | bytes 196616 | tf_op jit(solution)/shard_map/ppermute | solution.py:29
  84.8 1.3 %collective-permute-start.30 = (bf16[128,256]{1,0:T(8,128)(2,1)S(1)}, bf16[128,256]{1,0:T(8,128)(2,1)S(1)}, u32[]{:S(2)}, u32[]{:S(2)}) collective-permute-start(bf16[128,256]{1,0:T(8,128)(2,1)S(1)} %get-tuple-element.98), channel_id=1, source_target_pairs={{0,1},{1,0},{2,3},{3,2},{4,5},{5,4},{6,7},{7,6},{8,9},{9,8},{10,11... | collective-permute-start | bytes 196616 | tf_op jit(solution)/shard_map/ppermute | solution.py:29
  84.9 3.8 %collective-permute-start.32 = (bf16[128,256]{1,0:T(8,128)(2,1)S(1)}, bf16[128,256]{1,0:T(8,128)(2,1)S(1)}, u32[]{:S(2)}, u32[]{:S(2)}) collective-permute-start(bf16[128,256]{1,0:T(8,128)(2,1)S(1)} %get-tuple-element.100), channel_id=1, source_target_pairs={{0,1},{1,0},{2,3},{3,2},{4,5},{5,4},{6,7},{7,6},{8,9},{9,8},{10,11... | collective-permute-start | bytes 196616 | tf_op jit(solution)/shard_map/ppermute | solution.py:29
  85.6 5.0 %collective-permute-start.29 = (bf16[128,256]{1,0:T(8,128)(2,1)S(1)}, bf16[128,256]{1,0:T(8,128)(2,1)S(1)}, u32[]{:S(2)}, u32[]{:S(2)}) collective-permute-start(bf16[128,256]{1,0:T(8,128)(2,1)S(1)} %add_convert_fusion.2), channel_id=1, source_target_pairs={{0,2},{1,3},{2,0},{3,1},{4,6},{5,7},{6,4},{7,5},{8,10},{9,11},{10,... | collective-permute-start | bytes 196616 | tf_op jit(solution)/shard_map/ppermute | solution.py:24
  86.1 7.5 %collective-permute-start.31 = (bf16[128,256]{1,0:T(8,128)(2,1)S(1)}, bf16[128,256]{1,0:T(8,128)(2,1)S(1)}, u32[]{:S(2)}, u32[]{:S(2)}) collective-permute-start(bf16[128,256]{1,0:T(8,128)(2,1)S(1)} %add_convert_fusion.1), channel_id=1, source_target_pairs={{0,4},{1,5},{2,6},{3,7},{4,0},{5,1},{6,2},{7,3},{8,12},{9,13},{10,... | collective-permute-start | bytes 196616 | tf_op jit(solution)/shard_map/ppermute | solution.py:24
  88.7 6.2 %collective-permute-start.33 = (bf16[128,256]{1,0:T(8,128)(2,1)S(1)}, bf16[128,256]{1,0:T(8,128)(2,1)S(1)}, u32[]{:S(2)}, u32[]{:S(2)}) collective-permute-start(bf16[128,256]{1,0:T(8,128)(2,1)S(1)} %add_convert_fusion), channel_id=1, source_target_pairs={{0,6},{1,7},{2,4},{3,5},{4,2},{5,3},{6,0},{7,1},{8,14},{9,15},{10,... | collective-permute-start | bytes 196616 | tf_op jit(solution)/shard_map/ppermute | solution.py:24

commit v3 on v2

--- a/solution.py
+++ b/solution.py
@@ -197,6 +197,13 @@
         out_ref[:, i * cols : (i + 1) * cols] = jnp.dot(
             x, w_ref[...], preferred_element_type=F32
         ).astype(out_ref.dtype)
+
+
+def sum_kernel(*refs):
+    total = refs[0][...]
+    for ref in refs[1:-1]:
+        total = total + ref[...].astype(F32)
+    refs[-1][...] = total
 
 
 def cell_kernel(heads, size, received, *refs):
@@ -437,18 +444,19 @@
     w_got = core_send(w_sent)
     expert_got = [core_send(value) for value in expert_sent]
 
+    (early,) = call(sum_kernel, [((rows, span), F32)], own, *sent[1:])
     head_out, key_rows, value_rows, new_normer = call(
-        functools.partial(cell_kernel, heads, size, ep_count - 1),
+        functools.partial(cell_kernel, heads, size, 1),
         [((rows, heads * size), BF16)] + [((heads, size, rows), F32)] * 3,
-        own,
-        *sent,
+        early,
+        sent[0],
         gates,
         matrix,
         normer,
         head_gain[None, :],
         factor,
         w_got,
-        unread=(ep_count + 5,),
+        unread=(7,),
         scratch=[pltpu.VMEM((span, rows), F32)],
         limit=20,
     )

time: 95.8 us -> 98.5 us (1.028)
  waiting for transfers between devices: 43.1 us -> 47.3 us
  starting transfers between devices: 30.6 us -> 29.1 us
    ppermute x12, waiting for transfers between devices: 25.9 us -> 30.1 us  [ep_send(): return lax.ppermute(value, 'ep', [(i, i ^ step) for i in range(count)])]
    ppermute x12, starting transfers between devices: 16.7 us -> 15.2 us  [ep_send(): return lax.ppermute(value, 'ep', [(i, i ^ step) for i in range(count)])]
    pallas_call x19 -> x20, Pallas kernels: 20.3 us -> 20.3 us  [call(): pl.pallas_call(kernel, out_shape=[jax.ShapeDtypeStruct(shape, dtype) for...]
  transfers between devices with their start and end apart: 34 -> 34, of which waited for: 20 -> 21; matrix products, arithmetic and copies ran while one was open for 0% -> 0% of each run, Pallas kernels for 12% -> 12%
where the time goes in v3:
time: 98.5 us; the launch traced here: 98.3 us
  waiting for transfers between devices  47.3 us (48%)
  starting transfers between devices  29.1 us (30%)
  Pallas kernels  20.3 us (21%)
    ppermute x12, waiting for transfers between devices, ep_send(): return lax.ppermute(value, 'ep', [(i, i ^ step) for i in range(count)])  30.1 us
    pallas_call x20, Pallas kernels, call(): pl.pallas_call(kernel, out_shape=[jax.ShapeDtypeStruct(shape, dtype) for...  20.3 us
    ppermute x12, starting transfers between devices, ep_send(): return lax.ppermute(value, 'ep', [(i, i ^ step) for i in range(count)])  15.2 us
    ppermute x9, waiting for transfers between devices, chip_send(): lax.ppermute(value, 'tp', [(i, i ^ CORES * step) for i in range(count)])  14.4 us
    ppermute x9, starting transfers between devices, chip_send(): lax.ppermute(value, 'tp', [(i, i ^ CORES * step) for i in range(count)])  11.7 us
    ppermute x13, waiting for transfers between devices, core_send(): return lax.ppermute(value, 'tp', [(i, i ^ 1) for i in range(count)])  2.82 us
    ppermute x13, starting transfers between devices, core_send(): return lax.ppermute(value, 'tp', [(i, i ^ 1) for i in range(count)])  2.25 us
  transfers between devices with their start and end apart: 34, of which 21 were waited for; matrix products, arithmetic and copies ran while one was open for 0% of the time, Pallas kernels for 12%

profile of v3, /device:TPU:0, one launch (start us, length us, event | category | flops | bytes accessed | tf_op | source)
XLA Modules:
  0.0 98.3 jit_solution(1875774100096615618)
XLA Ops:
  0.6 1.1 %shard_map.228 = (bf16[128,512]{1,0:T(8,128)(2,1)S(1)}, bf16[128,512]{1,0:T(8,128)(2,1)S(1)}, bf16[128,512]{1,0:T(8,128)(2,1)S(1)}, bf16[128,512]{1,0:T(8,128)(2,1)S(1)}) custom-call(bf16[128,2048]{1,0:T(8,128)(2,1)} %refs_8_.1), custom_call_target="tpu_custom_call" | custom-call | tf_op jit(solution)/shard_map/pallas_call | solution.py:43
  1.8 3.0 %collective-permute-start.4 = (bf16[128,512]{1,0:T(8,128)(2,1)S(1)}, bf16[128,512]{1,0:T(8,128)(2,1)S(1)}, u32[]{:S(2)}, u32[]{:S(2)}) collective-permute-start(bf16[128,512]{1,0:T(8,128)(2,1)S(1)} %get-tuple-element.62), channel_id=1, source_target_pairs={{0,8},{8,0},{16,24},{24,16},{1,9},{9,1},{17,25},{25,17},{2,10},{10... | collective-permute-start | bytes 393224 | tf_op jit(solution)/shard_map/ppermute | solution.py:19
  4.8 1.5 %collective-permute-start.2 = (bf16[128,512]{1,0:T(8,128)(2,1)S(1)}, bf16[128,512]{1,0:T(8,128)(2,1)S(1)}, u32[]{:S(2)}, u32[]{:S(2)}) collective-permute-start(bf16[128,512]{1,0:T(8,128)(2,1)S(1)} %get-tuple-element.61), channel_id=1, source_target_pairs={{0,24},{8,16},{16,8},{24,0},{1,25},{9,17},{17,9},{25,1},{2,26},{10... | collective-permute-start | bytes 393224 | tf_op jit(solution)/shard_map/ppermute | solution.py:19
  6.4 1.2 %shard_map.229 = (bf16[512,256]{1,0:T(8,128)(2,1)S(1)}, bf16[512,256]{1,0:T(8,128)(2,1)S(1)}, bf16[512,256]{1,0:T(8,128)(2,1)S(1)}, bf16[512,256]{1,0:T(8,128)(2,1)S(1)}, f32[1,512]{1,0:T(1,128)S(1)}) custom-call(f32[1,2048]{1,0:T(1,128)} %bitcast.25, bf16[512,256]{1,0:T(8,128)(2,1)} %refs_0_.1, bf16[512,256]{1,0:T(8,128)(2,1)} %refs_1_.1, ...), custom_call_target="tpu_custom_call" | custom-call | tf_op jit(solution)/shard_map/pallas_call | solution.py:43
  7.6 1.1 %collective-permute-done.4.x_ref = bf16[128,512]{1,0:T(8,128)(2,1)S(1)} collective-permute-done((bf16[128,512]{1,0:T(8,128)(2,1)S(1)}, bf16[128,512]{1,0:T(8,128)(2,1)S(1)}, u32[]{:S(2)}, u32[]{:S(2)}) %collective-permute-start.4) | collective-permute-done | bytes 131104 | tf_op jit(solution)/shard_map/ppermute | solution.py:19
  9.0 3.4 %collective-permute-done.2.x_ref = bf16[128,512]{1,0:T(8,128)(2,1)S(1)} collective-permute-done((bf16[128,512]{1,0:T(8,128)(2,1)S(1)}, bf16[128,512]{1,0:T(8,128)(2,1)S(1)}, u32[]{:S(2)}, u32[]{:S(2)}) %collective-permute-start.2) | collective-permute-done | bytes 131104 | tf_op jit(solution)/shard_map/ppermute | solution.py:19
  12.7 1.0 %collective-permute-done.x_ref = bf16[128,512]{1,0:T(8,128)(2,1)S(1)} collective-permute-done((bf16[128,512]{1,0:T(8,128)(2,1)S(1)}, bf16[128,512]{1,0:T(8,128)(2,1)S(1)}, u32[]{:S(2)}, u32[]{:S(2)}) %collective-permute-start) | collective-permute-done | bytes 131104 | tf_op jit(solution)/shard_map/ppermute | solution.py:19
  14.1 0.7 copy-done.3
  14.8 5.8 %shard_map.235 = (bf16[256,1024]{1,0:T(8,128)(2,1)S(1)}, bf16[256,1024]{1,0:T(8,128)(2,1)S(1)}, f32[4,64,64,128]{3,2,1,0:T(8,128)S(1)}, f32[4,64,128]{2,1,0:T(8,...) custom-call(bf16[128,1024]{1,0:T(8,128)(2,1)S(1)} %shard_map.234.ref, ...), custom_call_target="tpu_custom_call" | custom-call | tf_op jit(solution)/shard_map/pallas_call | solution.py:43
  21.1 2.6 %collective-permute-start.3 = (bf16[128,1024]{1,0:T(8,128)(2,1)S(1)}, bf16[128,1024]{1,0:T(8,128)(2,1)S(1)}, u32[]{:S(2)}, u32[]{:S(2)}) collective-permute-start(bf16[128,1024]{1,0:T(8,128)(2,1)S(1)} %shard_map.232.refs_2_), channel_id=1, source_target_pairs={{0,24},{8,16},{16,8},{24,0},{1,25},{9,17},{17,9},{25,1},{2,26},{10... | collective-permute-start | bytes 786440 | tf_op jit(solution)/shard_map/ppermute | solution.py:19
  23.7 0.5 collective-permute-start.5
  24.6 10.5 %collective-permute-done.1.refs_1_ = bf16[128,1024]{1,0:T(8,128)(2,1)S(1)} collective-permute-done((bf16[128,1024]{1,0:T(8,128)(2,1)S(1)}, bf16[128,1024]{1,0:T(8,128)(2,1)S(1)}, u32[]{:S(2)}, u32[]{:S(2)}) %collective-permute-start.1) | collective-permute-done | bytes 262176 | tf_op jit(solution)/shard_map/ppermute | solution.py:19
  35.1 1.2 %collective-permute-done.5.refs_1_ = bf16[128,1024]{1,0:T(8,128)(2,1)S(1)} collective-permute-done((bf16[128,1024]{1,0:T(8,128)(2,1)S(1)}, bf16[128,1024]{1,0:T(8,128)(2,1)S(1)}, u32[]{:S(2)}, u32[]{:S(2)}) %collective-permute-start.5) | collective-permute-done | bytes 262176 | tf_op jit(solution)/shard_map/ppermute | solution.py:19
  36.3 1.6 %shard_map.236 = (bf16[128,256]{1,0:T(8,128)(2,1)S(1)}, f32[4,64,128]{2,1,0:T(8,128)S(1)}, f32[4,64,128]{2,1,0:T(8,128)S(1)}, f32[4,64,128]{2,1,0:T(8,128)}) custom-call(f32[128,1024]{1,0:T(8,128)S(1)} %shard_map.233.refs_0_, bf16[128,1024]{1,0:T(8,128)(2,1)S(1)} %collective-permute-done.5.refs_1_, f32[8,128]{1,0:T(8,128)S(1)} %get-tuple-element.63.refs_2_.gates_ref, ...), custom_call_target="tpu_custom_call" | custom-call | tf_op jit(solution)/shard_map/pallas_call | solution.py:43
  37.9 1.3 %collective-permute-done.7.got_ref = bf16[128,256]{1,0:T(8,128)(2,1)S(1)} collective-permute-done((bf16[128,256]{1,0:T(8,128)(2,1)S(1)}, bf16[128,256]{1,0:T(8,128)(2,1)S(1)}, u32[]{:S(2)}, u32[]{:S(2)}) %collective-permute-start.7) | collective-permute-done | bytes 65568 | tf_op jit(solution)/shard_map/ppermute | solution.py:29
  39.5 1.6 %collective-permute-start.8 = (bf16[128,256]{1,0:T(8,128)(2,1)S(1)}, bf16[128,256]{1,0:T(8,128)(2,1)S(1)}, u32[]{:S(2)}, u32[]{:S(2)}) collective-permute-start(bf16[128,256]{1,0:T(8,128)(2,1)S(1)} %get-tuple-element.76), channel_id=1, source_target_pairs={{0,2},{1,3},{2,0},{3,1},{4,6},{5,7},{6,4},{7,5},{8,10},{9,11},{10,... | collective-permute-start | bytes 196616 | tf_op jit(solution)/shard_map/ppermute | solution.py:24
  41.1 2.6 %collective-permute-start.9 = (bf16[128,256]{1,0:T(8,128)(2,1)S(1)}, bf16[128,256]{1,0:T(8,128)(2,1)S(1)}, u32[]{:S(2)}, u32[]{:S(2)}) collective-permute-start(bf16[128,256]{1,0:T(8,128)(2,1)S(1)} %get-tuple-element.77), channel_id=1, source_target_pairs={{0,4},{1,5},{2,6},{3,7},{4,0},{5,1},{6,2},{7,3},{8,12},{9,13},{10,... | collective-permute-start | bytes 196616 | tf_op jit(solution)/shard_map/ppermute | solution.py:24
  44.0 0.5 collective-permute-start.20
  44.5 3.8 %shard_map.238 = (f32[4,64,64,128]{3,2,1,0:T(8,128)}, f32[8,128]{1,0:T(8,128)S(1)}) custom-call(bf16[128,256]{1,0:T(8,128)(2,1)S(1)} %get-tuple-element.70.after_ref, f32[4,64,64,128]{3,2,1,0:T(8,128)S(1)} %get-tuple-element.64.refs_3_.matrix_ref, f32[4,64,128]{2,1,0:T(8,128)S(1)} %get-tuple-element.71.key_ref, ...), custom_call_target="tpu_custom_call" | custom-call | tf_op jit(solution)/shard_map/pallas_call | solution.py:43
  48.7 1.2 %collective-permute-done.10.refs_4_ = bf16[128,256]{1,0:T(8,128)(2,1)S(1)} collective-permute-done((bf16[128,256]{1,0:T(8,128)(2,1)S(1)}, bf16[128,256]{1,0:T(8,128)(2,1)S(1)}, u32[]{:S(2)}, u32[]{:S(2)}) %collective-permute-start.10) | collective-permute-done | bytes 65568 | tf_op jit(solution)/shard_map/ppermute | solution.py:24
  50.0 2.6 %collective-permute-start.13 = (bf16[128,256]{1,0:T(8,128)(2,1)S(1)}, bf16[128,256]{1,0:T(8,128)(2,1)S(1)}, u32[]{:S(2)}, u32[]{:S(2)}) collective-permute-start(bf16[128,256]{1,0:T(8,128)(2,1)S(1)} %shard_map.239.refs_0_), channel_id=1, source_target_pairs={{0,6},{1,7},{2,4},{3,5},{4,2},{5,3},{6,0},{7,1},{8,14},{9,15},{10,... | collective-permute-start | bytes 196616 | tf_op jit(solution)/shard_map/ppermute | solution.py:24
  52.6 0.4 collective-permute-start.12
  53.1 3.9 %collective-permute-done.13.refs_3_ = bf16[128,256]{1,0:T(8,128)(2,1)S(1)} collective-permute-done((bf16[128,256]{1,0:T(8,128)(2,1)S(1)}, bf16[128,256]{1,0:T(8,128)(2,1)S(1)}, u32[]{:S(2)}, u32[]{:S(2)}) %collective-permute-start.13) | collective-permute-done | bytes 65568 | tf_op jit(solution)/shard_map/ppermute | solution.py:24
  57.0 2.2 %collective-permute-done.12.refs_2_ = bf16[128,256]{1,0:T(8,128)(2,1)S(1)} collective-permute-done((bf16[128,256]{1,0:T(8,128)(2,1)S(1)}, bf16[128,256]{1,0:T(8,128)(2,1)S(1)}, u32[]{:S(2)}, u32[]{:S(2)}) %collective-permute-start.12) | collective-permute-done | bytes 65568 | tf_op jit(solution)/shard_map/ppermute | solution.py:24
  59.2 2.0 %collective-permute-done.11.refs_1_ = bf16[128,256]{1,0:T(8,128)(2,1)S(1)} collective-permute-done((bf16[128,256]{1,0:T(8,128)(2,1)S(1)}, bf16[128,256]{1,0:T(8,128)(2,1)S(1)}, u32[]{:S(2)}, u32[]{:S(2)}) %collective-permute-start.11) | collective-permute-done | bytes 65568 | tf_op jit(solution)/shard_map/ppermute | solution.py:24
  61.2 0.5 collective-permute-start.15
  61.7 0.7 collective-permute-done.16.refs_6_
  62.6 0.6 shard_map.240
  63.2 1.6 %collective-permute-start.21 = (bf16[48,2048]{1,0:T(8,128)(2,1)S(1)}, bf16[48,2048]{1,0:T(8,128)(2,1)S(1)}, u32[]{:S(2)}, u32[]{:S(2)}) collective-permute-start(bf16[48,2048]{1,0:T(8,128)(2,1)S(1)} %get-tuple-element.86), channel_id=1, source_target_pairs={{0,8},{8,0},{16,24},{24,16},{1,9},{9,1},{17,25},{25,17},{2,10},{10... | collective-permute-start | bytes 589832 | tf_op jit(solution)/shard_map/ppermute | solution.py:19
  64.8 0.5 collective-permute-start.23
  65.3 1.5 %collective-permute-start.25 = (bf16[48,2048]{1,0:T(8,128)(2,1)S(1)}, bf16[48,2048]{1,0:T(8,128)(2,1)S(1)}, u32[]{:S(2)}, u32[]{:S(2)}) collective-permute-start(bf16[48,2048]{1,0:T(8,128)(2,1)S(1)} %get-tuple-element.88), channel_id=1, source_target_pairs={{0,24},{8,16},{16,8},{24,0},{1,25},{9,17},{17,9},{25,1},{2,26},{10... | collective-permute-start | bytes 589832 | tf_op jit(solution)/shard_map/ppermute | solution.py:19
  66.8 4.3 %collective-permute-done.21.x_ref = bf16[48,2048]{1,0:T(8,128)(2,1)S(1)} collective-permute-done((bf16[48,2048]{1,0:T(8,128)(2,1)S(1)}, bf16[48,2048]{1,0:T(8,128)(2,1)S(1)}, u32[]{:S(2)}, u32[]{:S(2)}) %collective-permute-start.21) | collective-permute-done | bytes 196640 | tf_op jit(solution)/shard_map/ppermute | solution.py:19
  71.1 0.7 shard_map.242
  71.8 1.5 %collective-permute-start.22 = (bf16[48,2048]{1,0:T(8,128)(2,1)S(1)}, bf16[48,2048]{1,0:T(8,128)(2,1)S(1)}, u32[]{:S(2)}, u32[]{:S(2)}) collective-permute-start(bf16[48,2048]{1,0:T(8,128)(2,1)S(1)} %shard_map.242), channel_id=1, source_target_pairs={{0,8},{8,0},{16,24},{24,16},{1,9},{9,1},{17,25},{25,17},{2,10},{10... | collective-permute-start | bytes 589832 | tf_op jit(solution)/shard_map/ppermute | solution.py:19
  73.3 2.6 %collective-permute-done.23.x_ref = bf16[48,2048]{1,0:T(8,128)(2,1)S(1)} collective-permute-done((bf16[48,2048]{1,0:T(8,128)(2,1)S(1)}, bf16[48,2048]{1,0:T(8,128)(2,1)S(1)}, u32[]{:S(2)}, u32[]{:S(2)}) %collective-permute-start.23) | collective-permute-done | bytes 196640 | tf_op jit(solution)/shard_map/ppermute | solution.py:19
  75.9 0.7 shard_map.243
  76.7 0.7 shard_map.244
  77.4 1.8 %collective-permute-start.26 = (bf16[48,2048]{1,0:T(8,128)(2,1)S(1)}, bf16[48,2048]{1,0:T(8,128)(2,1)S(1)}, u32[]{:S(2)}, u32[]{:S(2)}) collective-permute-start(bf16[48,2048]{1,0:T(8,128)(2,1)S(1)} %shard_map.244), channel_id=1, source_target_pairs={{0,24},{8,16},{16,8},{24,0},{1,25},{9,17},{17,9},{25,1},{2,26},{10... | collective-permute-start | bytes 589832 | tf_op jit(solution)/shard_map/ppermute | solution.py:19
  79.3 0.5 shard_map.245
  79.8 0.7 shard_map.241.refs_0_
  80.5 6.1 %collective-permute-done.24.refs_2_ = bf16[48,2048]{1,0:T(8,128)(2,1)S(1)} collective-permute-done((bf16[48,2048]{1,0:T(8,128)(2,1)S(1)}, bf16[48,2048]{1,0:T(8,128)(2,1)S(1)}, u32[]{:S(2)}, u32[]{:S(2)}) %collective-permute-start.24) | collective-permute-done | bytes 196640 | tf_op jit(solution)/shard_map/ppermute | solution.py:19
  86.6 0.4 shard_map.246
  87.1 0.5 collective-permute-start.27
  88.9 2.5 %collective-permute-start.31 = (bf16[128,256]{1,0:T(8,128)(2,1)S(1)}, bf16[128,256]{1,0:T(8,128)(2,1)S(1)}, u32[]{:S(2)}, u32[]{:S(2)}) collective-permute-start(bf16[128,256]{1,0:T(8,128)(2,1)S(1)} %add_convert_fusion.1), channel_id=1, source_target_pairs={{0,4},{1,5},{2,6},{3,7},{4,0},{5,1},{6,2},{7,3},{8,12},{9,13},{10,... | collective-permute-start | bytes 196616 | tf_op jit(solution)/shard_map/ppermute | solution.py:24
  91.4 1.6 %collective-permute-start.33 = (bf16[128,256]{1,0:T(8,128)(2,1)S(1)}, bf16[128,256]{1,0:T(8,128)(2,1)S(1)}, u32[]{:S(2)}, u32[]{:S(2)}) collective-permute-start(bf16[128,256]{1,0:T(8,128)(2,1)S(1)} %add_convert_fusion), channel_id=1, source_target_pairs={{0,6},{1,7},{2,4},{3,5},{4,2},{5,3},{6,0},{7,1},{8,14},{9,15},{10,... | collective-permute-start | bytes 196616 | tf_op jit(solution)/shard_map/ppermute | solution.py:24
  93.4 3.0 %collective-permute-done.31.refs_3_ = bf16[128,256]{1,0:T(8,128)(2,1)S(1)} collective-permute-done((bf16[128,256]{1,0:T(8,128)(2,1)S(1)}, bf16[128,256]{1,0:T(8,128)(2,1)S(1)}, u32[]{:S(2)}, u32[]{:S(2)}) %collective-permute-start.31) | collective-permute-done | bytes 65568 | tf_op jit(solution)/shard_map/ppermute | solution.py:24
  96.4 1.2 %collective-permute-done.33.refs_4_ = bf16[128,256]{1,0:T(8,128)(2,1)S(1)} collective-permute-done((bf16[128,256]{1,0:T(8,128)(2,1)S(1)}, bf16[128,256]{1,0:T(8,128)(2,1)S(1)}, u32[]{:S(2)}, u32[]{:S(2)}) %collective-permute-start.33) | collective-permute-done | bytes 65568 | tf_op jit(solution)/shard_map/ppermute | solution.py:24
  97.7 0.7 shard_map.247
  (54 shorter events, 5.0 us)
Async XLA Ops:
  1.8 6.9 %collective-permute-start.4 = (bf16[128,512]{1,0:T(8,128)(2,1)S(1)}, bf16[128,512]{1,0:T(8,128)(2,1)S(1)}, u32[]{:S(2)}, u32[]{:S(2)}) collective-permute-start(bf16[128,512]{1,0:T(8,128)(2,1)S(1)} %get-tuple-element.62), channel_id=1, source_target_pairs={{0,8},{8,0},{16,24},{24,16},{1,9},{9,1},{17,25},{25,17},{2,10},{10... | collective-permute-start | bytes 393224 | tf_op jit(solution)/shard_map/ppermute | solution.py:19
  4.8 7.6 %collective-permute-start.2 = (bf16[128,512]{1,0:T(8,128)(2,1)S(1)}, bf16[128,512]{1,0:T(8,128)(2,1)S(1)}, u32[]{:S(2)}, u32[]{:S(2)}) collective-permute-start(bf16[128,512]{1,0:T(8,128)(2,1)S(1)} %get-tuple-element.61), channel_id=1, source_target_pairs={{0,24},{8,16},{16,8},{24,0},{1,25},{9,17},{17,9},{25,1},{2,26},{10... | collective-permute-start | bytes 393224 | tf_op jit(solution)/shard_map/ppermute | solution.py:19
  6.3 7.5 %collective-permute-start = (bf16[128,512]{1,0:T(8,128)(2,1)S(1)}, bf16[128,512]{1,0:T(8,128)(2,1)S(1)}, u32[]{:S(2)}, u32[]{:S(2)}) collective-permute-start(bf16[128,512]{1,0:T(8,128)(2,1)S(1)} %get-tuple-element.60), channel_id=1, source_target_pairs={{0,16},{8,24},{16,0},{24,8},{1,17},{9,25},{17,1},{25,9},{2,18},{10... | collective-permute-start | bytes 393224 | tf_op jit(solution)/shard_map/ppermute | solution.py:19
  14.1 0.7 copy-start.3
  14.8 21.5 %copy-start.4 = (f32[256]{0:T(256)S(1)}, f32[256]{0:T(256)}, u32[]{:S(2)}) copy-start(f32[256]{0:T(256)} %param.30) | copy-start | bytes 3076
  20.6 15.6 %collective-permute-start.6 = (bf16[256,1024]{1,0:T(8,128)(2,1)S(1)}, bf16[256,1024]{1,0:T(8,128)(2,1)S(1)}, u32[]{:S(2)}, u32[]{:S(2)}) collective-permute-start(bf16[256,1024]{1,0:T(8,128)(2,1)S(1)} %get-tuple-element.67), channel_id=1, source_target_pairs={{0,1},{1,0},{2,3},{3,2},{4,5},{5,4},{6,7},{7,6},{8,9},{9,8},{10,11... | collective-permute-start | bytes 1572872 | tf_op jit(solution)/shard_map/ppermute | solution.py:29
  20.7 14.3 %collective-permute-start.1 = (bf16[128,1024]{1,0:T(8,128)(2,1)S(1)}, bf16[128,1024]{1,0:T(8,128)(2,1)S(1)}, u32[]{:S(2)}, u32[]{:S(2)}) collective-permute-start(bf16[128,1024]{1,0:T(8,128)(2,1)S(1)} %shard_map.231.refs_1_), channel_id=1, source_target_pairs={{0,16},{8,24},{16,0},{24,8},{1,17},{9,25},{17,1},{25,9},{2,18},{10... | collective-permute-start | bytes 786440 | tf_op jit(solution)/shard_map/ppermute | solution.py:19
  21.1 13.9 %collective-permute-start.3 = (bf16[128,1024]{1,0:T(8,128)(2,1)S(1)}, bf16[128,1024]{1,0:T(8,128)(2,1)S(1)}, u32[]{:S(2)}, u32[]{:S(2)}) collective-permute-start(bf16[128,1024]{1,0:T(8,128)(2,1)S(1)} %shard_map.232.refs_2_), channel_id=1, source_target_pairs={{0,24},{8,16},{16,8},{24,0},{1,25},{9,17},{17,9},{25,1},{2,26},{10... | collective-permute-start | bytes 786440 | tf_op jit(solution)/shard_map/ppermute | solution.py:19
  23.7 12.5 %collective-permute-start.5 = (bf16[128,1024]{1,0:T(8,128)(2,1)S(1)}, bf16[128,1024]{1,0:T(8,128)(2,1)S(1)}, u32[]{:S(2)}, u32[]{:S(2)}) collective-permute-start(bf16[128,1024]{1,0:T(8,128)(2,1)S(1)} %shard_map.234.refs_0_), channel_id=1, source_target_pairs={{0,8},{8,0},{16,24},{24,16},{1,9},{9,1},{17,25},{25,17},{2,10},{10... | collective-permute-start | bytes 786440 | tf_op jit(solution)/shard_map/ppermute | solution.py:19
  24.3 41.0 %collective-permute-start.18 = (bf16[2048,128]{1,0:T(8,128)(2,1)S(1)}, bf16[2048,128]{1,0:T(8,128)(2,1)S(1)}, u32[]{:S(2)}, u32[]{:S(2)}) collective-permute-start(bf16[2048,128]{1,0:T(8,128)(2,1)S(1)} %get-tuple-element.83), channel_id=1, source_target_pairs={{0,1},{1,0},{2,3},{3,2},{4,5},{5,4},{6,7},{7,6},{8,9},{9,8},{10,11... | collective-permute-start | bytes 1572872 | tf_op jit(solution)/shard_map/ppermute | solution.py:29
  36.3 26.3 %copy-start.2 = (f32[2048]{0:T(1024)S(1)}, f32[2048]{0:T(1024)}, u32[]{:S(2)}) copy-start(f32[2048]{0:T(1024)} %param.35) | copy-start | bytes 24580
  37.9 1.3 %collective-permute-start.7 = (bf16[128,256]{1,0:T(8,128)(2,1)S(1)}, bf16[128,256]{1,0:T(8,128)(2,1)S(1)}, u32[]{:S(2)}, u32[]{:S(2)}) collective-permute-start(bf16[128,256]{1,0:T(8,128)(2,1)S(1)} %get-tuple-element.68.own_ref), channel_id=1, source_target_pairs={{0,1},{1,0},{2,3},{3,2},{4,5},{5,4},{6,7},{7,6},{8,9},{9,8},{10,11... | collective-permute-start | bytes 196616 | tf_op jit(solution)/shard_map/ppermute | solution.py:29
  39.5 4.5 %collective-permute-start.8 = (bf16[128,256]{1,0:T(8,128)(2,1)S(1)}, bf16[128,256]{1,0:T(8,128)(2,1)S(1)}, u32[]{:S(2)}, u32[]{:S(2)}) collective-permute-start(bf16[128,256]{1,0:T(8,128)(2,1)S(1)} %get-tuple-element.76), channel_id=1, source_target_pairs={{0,2},{1,3},{2,0},{3,1},{4,6},{5,7},{6,4},{7,5},{8,10},{9,11},{10,... | collective-permute-start | bytes 196616 | tf_op jit(solution)/shard_map/ppermute | solution.py:24
  41.1 7.5 %collective-permute-start.9 = (bf16[128,256]{1,0:T(8,128)(2,1)S(1)}, bf16[128,256]{1,0:T(8,128)(2,1)S(1)}, u32[]{:S(2)}, u32[]{:S(2)}) collective-permute-start(bf16[128,256]{1,0:T(8,128)(2,1)S(1)} %get-tuple-element.77), channel_id=1, source_target_pairs={{0,4},{1,5},{2,6},{3,7},{4,0},{5,1},{6,2},{7,3},{8,12},{9,13},{10,... | collective-permute-start | bytes 196616 | tf_op jit(solution)/shard_map/ppermute | solution.py:24
  43.7 6.2 %collective-permute-start.10 = (bf16[128,256]{1,0:T(8,128)(2,1)S(1)}, bf16[128,256]{1,0:T(8,128)(2,1)S(1)}, u32[]{:S(2)}, u32[]{:S(2)}) collective-permute-start(bf16[128,256]{1,0:T(8,128)(2,1)S(1)} %get-tuple-element.70.after_ref), channel_id=1, source_target_pairs={{0,6},{1,7},{2,4},{3,5},{4,2},{5,3},{6,0},{7,1},{8,14},{9,15},{10,... | collective-permute-start | bytes 196616 | tf_op jit(solution)/shard_map/ppermute | solution.py:24
  44.0 22.8 %collective-permute-start.19 = (bf16[2048,128]{1,0:T(8,128)(2,1)S(1)}, bf16[2048,128]{1,0:T(8,128)(2,1)S(1)}, u32[]{:S(2)}, u32[]{:S(2)}) collective-permute-start(bf16[2048,128]{1,0:T(8,128)(2,1)S(1)} %get-tuple-element.84), channel_id=1, source_target_pairs={{0,1},{1,0},{2,3},{3,2},{4,5},{5,4},{6,7},{7,6},{8,9},{9,8},{10,11... | collective-permute-start | bytes 1572872 | tf_op jit(solution)/shard_map/ppermute | solution.py:29
  44.0 22.8 %collective-permute-start.20 = (bf16[128,2048]{1,0:T(8,128)(2,1)S(1)}, bf16[128,2048]{1,0:T(8,128)(2,1)S(1)}, u32[]{:S(2)}, u32[]{:S(2)}) collective-permute-start(bf16[128,2048]{1,0:T(8,128)(2,1)S(1)} %get-tuple-element.85), channel_id=1, source_target_pairs={{0,1},{1,0},{2,3},{3,2},{4,5},{5,4},{6,7},{7,6},{8,9},{9,8},{10,11... | collective-permute-start | bytes 1572872 | tf_op jit(solution)/shard_map/ppermute | solution.py:29
  44.5 34.8 %copy-start = (bf16[2048,8]{0,1:T(8,128)(2,1)S(1)}, bf16[2048,8]{0,1:T(8,128)(2,1)}, u32[]{:S(2)}) copy-start(bf16[2048,8]{0,1:T(8,128)(2,1)} %param.37) | copy-start | bytes 98308
  44.5 34.8 %copy-start.1 = (bf16[2048,4]{0,1:T(4,128)(2,1)S(1)}, bf16[2048,4]{0,1:T(4,128)(2,1)}, u32[]{:S(2)}) copy-start(bf16[2048,4]{0,1:T(4,128)(2,1)} %param.36) | copy-start | bytes 49156
  49.9 2.7 %collective-permute-start.14 = (bf16[128,256]{1,0:T(8,128)(2,1)S(1)}, bf16[128,256]{1,0:T(8,128)(2,1)S(1)}, u32[]{:S(2)}, u32[]{:S(2)}) collective-permute-start(bf16[128,256]{1,0:T(8,128)(2,1)S(1)} %shard_map.239.refs_0_), channel_id=1, source_target_pairs={{0,1},{1,0},{2,3},{3,2},{4,5},{5,4},{6,7},{7,6},{8,9},{9,8},{10,11... | collective-permute-start | bytes 196616 | tf_op jit(solution)/shard_map/ppermute | solution.py:29
  50.0 6.9 %collective-permute-start.13 = (bf16[128,256]{1,0:T(8,128)(2,1)S(1)}, bf16[128,256]{1,0:T(8,128)(2,1)S(1)}, u32[]{:S(2)}, u32[]{:S(2)}) collective-permute-start(bf16[128,256]{1,0:T(8,128)(2,1)S(1)} %shard_map.239.refs_0_), channel_id=1, source_target_pairs={{0,6},{1,7},{2,4},{3,5},{4,2},{5,3},{6,0},{7,1},{8,14},{9,15},{10,... | collective-permute-start | bytes 196616 | tf_op jit(solution)/shard_map/ppermute | solution.py:24
  52.6 6.6 %collective-permute-start.12 = (bf16[128,256]{1,0:T(8,128)(2,1)S(1)}, bf16[128,256]{1,0:T(8,128)(2,1)S(1)}, u32[]{:S(2)}, u32[]{:S(2)}) collective-permute-start(bf16[128,256]{1,0:T(8,128)(2,1)S(1)} %shard_map.239.refs_0_), channel_id=1, source_target_pairs={{0,4},{1,5},{2,6},{3,7},{4,0},{5,1},{6,2},{7,3},{8,12},{9,13},{10,... | collective-permute-start | bytes 196616 | tf_op jit(solution)/shard_map/ppermute | solution.py:24
  56.9 4.3 %collective-permute-start.11 = (bf16[128,256]{1,0:T(8,128)(2,1)S(1)}, bf16[128,256]{1,0:T(8,128)(2,1)S(1)}, u32[]{:S(2)}, u32[]{:S(2)}) collective-permute-start(bf16[128,256]{1,0:T(8,128)(2,1)S(1)} %shard_map.239.refs_0_), channel_id=1, source_target_pairs={{0,2},{1,3},{2,0},{3,1},{4,6},{5,7},{6,4},{7,5},{8,10},{9,11},{10,... | collective-permute-start | bytes 196616 | tf_op jit(solution)/shard_map/ppermute | solution.py:24
  59.2 2.0 %collective-permute-start.17 = (bf16[128,256]{1,0:T(8,128)(2,1)S(1)}, bf16[128,256]{1,0:T(8,128)(2,1)S(1)}, u32[]{:S(2)}, u32[]{:S(2)}) collective-permute-start(bf16[128,256]{1,0:T(8,128)(2,1)S(1)} %collective-permute-done.13.refs_3_), channel_id=1, source_target_pairs={{0,1},{1,0},{2,3},{3,2},{4,5},{5,4},{6,7},{7,6},{8,9},{9,8},{10,11... | collective-permute-start | bytes 196616 | tf_op jit(solution)/shard_map/ppermute | solution.py:29
  61.2 1.3 %collective-permute-start.16 = (bf16[128,256]{1,0:T(8,128)(2,1)S(1)}, bf16[128,256]{1,0:T(8,128)(2,1)S(1)}, u32[]{:S(2)}, u32[]{:S(2)}) collective-permute-start(bf16[128,256]{1,0:T(8,128)(2,1)S(1)} %collective-permute-done.12.refs_2_), channel_id=1, source_target_pairs={{0,1},{1,0},{2,3},{3,2},{4,5},{5,4},{6,7},{7,6},{8,9},{9,8},{10,11... | collective-permute-start | bytes 196616 | tf_op jit(solution)/shard_map/ppermute | solution.py:29
  61.2 1.4 %collective-permute-start.15 = (bf16[128,256]{1,0:T(8,128)(2,1)S(1)}, bf16[128,256]{1,0:T(8,128)(2,1)S(1)}, u32[]{:S(2)}, u32[]{:S(2)}) collective-permute-start(bf16[128,256]{1,0:T(8,128)(2,1)S(1)} %collective-permute-done.11.refs_1_), channel_id=1, source_target_pairs={{0,1},{1,0},{2,3},{3,2},{4,5},{5,4},{6,7},{7,6},{8,9},{9,8},{10,11... | collective-permute-start | bytes 196616 | tf_op jit(solution)/shard_map/ppermute | solution.py:29
  63.2 7.8 %collective-permute-start.21 = (bf16[48,2048]{1,0:T(8,128)(2,1)S(1)}, bf16[48,2048]{1,0:T(8,128)(2,1)S(1)}, u32[]{:S(2)}, u32[]{:S(2)}) collective-permute-start(bf16[48,2048]{1,0:T(8,128)(2,1)S(1)} %get-tuple-element.86), channel_id=1, source_target_pairs={{0,8},{8,0},{16,24},{24,16},{1,9},{9,1},{17,25},{25,17},{2,10},{10... | collective-permute-start | bytes 589832 | tf_op jit(solution)/shard_map/ppermute | solution.py:19
  64.8 11.1 %collective-permute-start.23 = (bf16[48,2048]{1,0:T(8,128)(2,1)S(1)}, bf16[48,2048]{1,0:T(8,128)(2,1)S(1)}, u32[]{:S(2)}, u32[]{:S(2)}) collective-permute-start(bf16[48,2048]{1,0:T(8,128)(2,1)S(1)} %get-tuple-element.87), channel_id=1, source_target_pairs={{0,16},{8,24},{16,0},{24,8},{1,17},{9,25},{17,1},{25,9},{2,18},{10... | collective-permute-start | bytes 589832 | tf_op jit(solution)/shard_map/ppermute | solution.py:19
  65.3 11.4 %collective-permute-start.25 = (bf16[48,2048]{1,0:T(8,128)(2,1)S(1)}, bf16[48,2048]{1,0:T(8,128)(2,1)S(1)}, u32[]{:S(2)}, u32[]{:S(2)}) collective-permute-start(bf16[48,2048]{1,0:T(8,128)(2,1)S(1)} %get-tuple-element.88), channel_id=1, source_target_pairs={{0,24},{8,16},{16,8},{24,0},{1,25},{9,17},{17,9},{25,1},{2,26},{10... | collective-permute-start | bytes 589832 | tf_op jit(solution)/shard_map/ppermute | solution.py:19
  71.8 8.7 %collective-permute-start.22 = (bf16[48,2048]{1,0:T(8,128)(2,1)S(1)}, bf16[48,2048]{1,0:T(8,128)(2,1)S(1)}, u32[]{:S(2)}, u32[]{:S(2)}) collective-permute-start(bf16[48,2048]{1,0:T(8,128)(2,1)S(1)} %shard_map.242), channel_id=1, source_target_pairs={{0,8},{8,0},{16,24},{24,16},{1,9},{9,1},{17,25},{25,17},{2,10},{10... | collective-permute-start | bytes 589832 | tf_op jit(solution)/shard_map/ppermute | solution.py:19
  76.6 10.0 %collective-permute-start.24 = (bf16[48,2048]{1,0:T(8,128)(2,1)S(1)}, bf16[48,2048]{1,0:T(8,128)(2,1)S(1)}, u32[]{:S(2)}, u32[]{:S(2)}) collective-permute-start(bf16[48,2048]{1,0:T(8,128)(2,1)S(1)} %shard_map.243), channel_id=1, source_target_pairs={{0,16},{8,24},{16,0},{24,8},{1,17},{9,25},{17,1},{25,9},{2,18},{10... | collective-permute-start | bytes 589832 | tf_op jit(solution)/shard_map/ppermute | solution.py:19
  77.4 9.2 %collective-permute-start.26 = (bf16[48,2048]{1,0:T(8,128)(2,1)S(1)}, bf16[48,2048]{1,0:T(8,128)(2,1)S(1)}, u32[]{:S(2)}, u32[]{:S(2)}) collective-permute-start(bf16[48,2048]{1,0:T(8,128)(2,1)S(1)} %shard_map.244), channel_id=1, source_target_pairs={{0,24},{8,16},{16,8},{24,0},{1,25},{9,17},{17,9},{25,1},{2,26},{10... | collective-permute-start | bytes 589832 | tf_op jit(solution)/shard_map/ppermute | solution.py:19
  87.0 1.3 %collective-permute-start.28 = (bf16[128,256]{1,0:T(8,128)(2,1)S(1)}, bf16[128,256]{1,0:T(8,128)(2,1)S(1)}, u32[]{:S(2)}, u32[]{:S(2)}) collective-permute-start(bf16[128,256]{1,0:T(8,128)(2,1)S(1)} %get-tuple-element.96), channel_id=1, source_target_pairs={{0,1},{1,0},{2,3},{3,2},{4,5},{5,4},{6,7},{7,6},{8,9},{9,8},{10,11... | collective-permute-start | bytes 196616 | tf_op jit(solution)/shard_map/ppermute | solution.py:29
  87.1 5.9 %collective-permute-start.27 = (bf16[128,256]{1,0:T(8,128)(2,1)S(1)}, bf16[128,256]{1,0:T(8,128)(2,1)S(1)}, u32[]{:S(2)}, u32[]{:S(2)}) collective-permute-start(bf16[128,256]{1,0:T(8,128)(2,1)S(1)} %get-tuple-element.94), channel_id=1, source_target_pairs={{0,1},{1,0},{2,3},{3,2},{4,5},{5,4},{6,7},{7,6},{8,9},{9,8},{10,11... | collective-permute-start | bytes 196616 | tf_op jit(solution)/shard_map/ppermute | solution.py:29
  87.6 1.3 %collective-permute-start.30 = (bf16[128,256]{1,0:T(8,128)(2,1)S(1)}, bf16[128,256]{1,0:T(8,128)(2,1)S(1)}, u32[]{:S(2)}, u32[]{:S(2)}) collective-permute-start(bf16[128,256]{1,0:T(8,128)(2,1)S(1)} %get-tuple-element.98), channel_id=1, source_target_pairs={{0,1},{1,0},{2,3},{3,2},{4,5},{5,4},{6,7},{7,6},{8,9},{9,8},{10,11... | collective-permute-start | bytes 196616 | tf_op jit(solution)/shard_map/ppermute | solution.py:29
  87.7 3.7 %collective-permute-start.32 = (bf16[128,256]{1,0:T(8,128)(2,1)S(1)}, bf16[128,256]{1,0:T(8,128)(2,1)S(1)}, u32[]{:S(2)}, u32[]{:S(2)}) collective-permute-start(bf16[128,256]{1,0:T(8,128)(2,1)S(1)} %get-tuple-element.100), channel_id=1, source_target_pairs={{0,1},{1,0},{2,3},{3,2},{4,5},{5,4},{6,7},{7,6},{8,9},{9,8},{10,11... | collective-permute-start | bytes 196616 | tf_op jit(solution)/shard_map/ppermute | solution.py:29
  88.4 5.0 %collective-permute-start.29 = (bf16[128,256]{1,0:T(8,128)(2,1)S(1)}, bf16[128,256]{1,0:T(8,128)(2,1)S(1)}, u32[]{:S(2)}, u32[]{:S(2)}) collective-permute-start(bf16[128,256]{1,0:T(8,128)(2,1)S(1)} %add_convert_fusion.2), channel_id=1, source_target_pairs={{0,2},{1,3},{2,0},{3,1},{4,6},{5,7},{6,4},{7,5},{8,10},{9,11},{10,... | collective-permute-start | bytes 196616 | tf_op jit(solution)/shard_map/ppermute | solution.py:24
  88.9 7.5 %collective-permute-start.31 = (bf16[128,256]{1,0:T(8,128)(2,1)S(1)}, bf16[128,256]{1,0:T(8,128)(2,1)S(1)}, u32[]{:S(2)}, u32[]{:S(2)}) collective-permute-start(bf16[128,256]{1,0:T(8,128)(2,1)S(1)} %add_convert_fusion.1), channel_id=1, source_target_pairs={{0,4},{1,5},{2,6},{3,7},{4,0},{5,1},{6,2},{7,3},{8,12},{9,13},{10,... | collective-permute-start | bytes 196616 | tf_op jit(solution)/shard_map/ppermute | solution.py:24
  91.4 6.2 %collective-permute-start.33 = (bf16[128,256]{1,0:T(8,128)(2,1)S(1)}, bf16[128,256]{1,0:T(8,128)(2,1)S(1)}, u32[]{:S(2)}, u32[]{:S(2)}) collective-permute-start(bf16[128,256]{1,0:T(8,128)(2,1)S(1)} %add_convert_fusion), channel_id=1, source_target_pairs={{0,6},{1,7},{2,4},{3,5},{4,2},{5,3},{6,0},{7,1},{8,14},{9,15},{10,... | collective-permute-start | bytes 196616 | tf_op jit(solution)/shard_map/ppermute | solution.py:24
